TPU v7x, 32 devices: a whole 2x2x4 slice. The times are simulated.
32 devices in a mesh: sp: 8 (over z, x), tp: 4 (over y, core).
Axes of the slice: x: 2, y: 2, z: 4, core: 2. Of those that a mesh axis runs over, the one named last changes fastest.
Arguments:
- lane_source_signal: bfloat16 [1024, 1024], P('tp', 'sp'), may hold values from -6 to 6
- spectral_damping_part: float32 [64, 64], P('tp'), may hold values from -3 to -0.0002
- spectral_angular_part: float32 [64, 64], P('tp'), may hold values from 0.31 to 201.0624
- interval_exponent: float32 [64], P('tp'), may hold values from -3.9 to -1.6
- entry_matrix_inphase: float32 [64, 64, 16], P('tp'), may hold values from -1 to 1
- entry_matrix_quadrature: float32 [64, 64, 16], P('tp'), may hold values from -1 to 1
- emission_inphase: float32 [64, 16, 64], P('tp'), may hold values from -0.75 to 0.75
- emission_quadrature: float32 [64, 16, 64], P('tp'), may hold values from -0.75 to 0.75
- lane_bypass_factor: float32 [1024], P('tp'), may hold values from -5 to 5
- spike_shrink_offset: float32 [64, 1024], P('tp', 'sp'), may hold values from -1.4 to 0
- lane_exit_matrix: bfloat16 [1024, 4096], P('tp'), may hold values from -0.1875 to 0.1875
- skipline_stream: bfloat16 [1024, 4096], P('sp'), may hold values from -6 to 6
- specialist_scaling_vector: float32 [4096], replicated, may hold values from 0.1 to 1.9
- selected_specialists: int32 [1024, 2], P('sp'), may hold values from 0 to 7, all different within a row; in each aligned block of 128 rows (0 to 127, 128 to 255, ...) at most 64 rows name the same one
- dispatcher_scores: float32 [1024, 2], P('sp'), may hold values from 0.1 to 1
- specialist_valve_matrix: bfloat16 [8, 4096, 2048], P('sp', None, 'tp'), may hold values from -0.09375 to 0.09375
- specialist_widen_matrix: bfloat16 [8, 4096, 2048], P('sp', None, 'tp'), may hold values from -0.09375 to 0.09375
- specialist_shrink_matrix: bfloat16 [8, 2048, 4096], P('sp', 'tp'), may hold values from -0.1875 to 0.1875
Outputs:
- updated: bfloat16 [1024, 4096], P('sp', 'tp')
Inputs may be any that keep to these rules, and one draw needn't show every extreme that they name: `selected_specialists`: each row names 2 different experts. Among the rows of each aligned block of 128 positions no expert is named more than 64 times, and in every block some expert is named exactly 64 times.
All inputs are finite; a program needn't handle non-finite values.
Results may differ from a plain program's by a relative error of at most 0.019.
Values may be sent and summed in bfloat16 or wider, within the bound.
No kernel may reach another device: no remote copies, remote signals or barrier semaphores. Data moves between devices by JAX's collectives and lax.ppermute only.
A program may use at most 64 MiB of HBM per device.

v0:
```python
import jax
import jax.numpy as jnp
from jax import lax
from jax.sharding import PartitionSpec as P

EPS = 1e-06
PRECISE_MODE = lax.Precision.HIGHEST


def carried_in(value, axis, join, neutral):
    count, mine = (lax.axis_size(axis), lax.axis_index(axis))
    pieces = jax.tree.map(lambda part: lax.all_gather(part, axis), value)
    running = jax.tree.map(
        lambda part, zero: jnp.full_like(part, 0) + jnp.asarray(zero, part.dtype), value, neutral
    )

    def lap(position, running):
        longer = join(running, jax.tree.map(lambda part: part[position], pieces))
        return jax.tree.map(lambda new, old: jnp.where(position < mine, new, old), longer, running)

    return lax.fori_loop(0, count - 1, lap, running)


def affine_pair(earlier, latter):
    mul_re = earlier[0] * latter[0] - earlier[1] * latter[1]
    mul_im = earlier[0] * latter[1] + earlier[1] * latter[0]
    add_re = latter[0] * earlier[2] - latter[1] * earlier[3] + latter[2]
    add_im = latter[0] * earlier[3] + latter[1] * earlier[2] + latter[3]
    return (mul_re, mul_im, add_re, add_im)


def local_prefix(elements):
    length = elements[0].shape[2]
    fills = (1.0, 0.0, 0.0, 0.0)
    offset = 1
    while offset < length:
        earlier = tuple(
            (
                jnp.pad(
                    item[:, :, : length - offset],
                    ((0, 0), (0, 0), (offset, 0)),
                    constant_values=fill,
                )
                for item, fill in zip(elements, fills)
            )
        )
        elements = affine_pair(earlier, elements)
        offset = offset * 2
    return elements


def full_norm(projected, skipline_stream, specialist_scaling_vector, col_start, d_local):
    stream = (
        skipline_stream.astype(jnp.float32)
        + lax.optimization_barrier(projected).astype(jnp.float32)
    ).astype(jnp.bfloat16)
    stream_f = lax.optimization_barrier(stream).astype(jnp.float32)
    inv_rms = lax.rsqrt(jnp.mean(stream_f * stream_f, axis=-1, keepdims=True) + EPS)
    normed = (stream_f * inv_rms * specialist_scaling_vector).astype(jnp.bfloat16)
    own_stream = lax.dynamic_slice_in_dim(stream_f, col_start, d_local, 1)
    own_cols = lax.dynamic_slice_in_dim(normed, col_start, d_local, 1)
    return (own_stream, normed, own_cols)


def per_device(
    lane_source_signal,
    spectral_damping_part,
    spectral_angular_part,
    interval_exponent,
    entry_matrix_inphase,
    entry_matrix_quadrature,
    emission_inphase,
    emission_quadrature,
    lane_bypass_factor,
    spike_shrink_offset,
    lane_exit_matrix,
    skipline_stream,
    specialist_scaling_vector,
    selected_specialists,
    dispatcher_scores,
    specialist_valve_matrix,
    specialist_widen_matrix,
    specialist_shrink_matrix,
):
    f32 = jnp.float32
    bf16 = jnp.bfloat16
    groups_here = spectral_damping_part.shape[0]
    lanes_within_bundle = entry_matrix_inphase.shape[2]
    tok_local = lane_source_signal.shape[1]
    bundled_signal = lane_source_signal.astype(f32).reshape(
        groups_here, lanes_within_bundle, tok_local
    )
    step_size = jnp.exp(interval_exponent)[:, None]
    natural_pace_exponent = spectral_damping_part * step_size
    angle = spectral_angular_part * step_size
    num_re = jnp.expm1(natural_pace_exponent) * jnp.cos(angle) - 2.0 * jnp.sin(0.5 * angle) ** 2
    num_im = jnp.exp(natural_pace_exponent) * jnp.sin(angle)
    denom = (
        spectral_damping_part * spectral_damping_part
        + spectral_angular_part * spectral_angular_part
    )
    fac_re = (num_re * spectral_damping_part + num_im * spectral_angular_part) / denom
    fac_im = (num_im * spectral_damping_part - num_re * spectral_angular_part) / denom
    map_re = (
        fac_re[:, :, None] * entry_matrix_inphase - fac_im[:, :, None] * entry_matrix_quadrature
    )
    map_im = (
        fac_re[:, :, None] * entry_matrix_quadrature + fac_im[:, :, None] * entry_matrix_inphase
    )
    drive_re = jnp.einsum("gpc,gct->gpt", map_re, bundled_signal, precision=PRECISE_MODE)
    drive_im = jnp.einsum("gpc,gct->gpt", map_im, bundled_signal, precision=PRECISE_MODE)
    recurrence_modulus = jnp.exp(
        natural_pace_exponent[:, :, None] + spike_shrink_offset[:, None, :]
    )
    trans_re = recurrence_modulus * jnp.cos(angle)[:, :, None]
    trans_im = recurrence_modulus * jnp.sin(angle)[:, :, None]
    cum_re, cum_im, state_real, state_imaginary = local_prefix(
        (trans_re, trans_im, drive_re, drive_im)
    )
    summary = (cum_re[:, :, -1], cum_im[:, :, -1], state_real[:, :, -1], state_imaginary[:, :, -1])
    unit = jnp.ones_like(summary[0])
    blank = jnp.zeros_like(summary[0])
    carried = carried_in(summary, "sp", affine_pair, (unit, blank, blank, blank))
    enter_re = carried[2][:, :, None]
    enter_im = carried[3][:, :, None]
    state_real = state_real + cum_re * enter_re - cum_im * enter_im
    state_imaginary = state_imaginary + cum_re * enter_im + cum_im * enter_re
    value = (
        jnp.einsum("nef,nfi->nei", emission_inphase, state_real, precision=PRECISE_MODE)
        - jnp.einsum("nef,nfi->nei", emission_quadrature, state_imaginary, precision=PRECISE_MODE)
        + lane_bypass_factor.reshape(groups_here, lanes_within_bundle)[:, :, None] * bundled_signal
    )
    recurrence_result = (
        jax.nn.gelu(value).astype(bf16).reshape(groups_here * lanes_within_bundle, tok_local)
    )
    width = specialist_scaling_vector.shape[0]
    d_local = width // lax.axis_size("tp")
    col_start = lax.axis_index("tp") * d_local
    partial_rows = jnp.einsum(
        "ct,cd->td", recurrence_result, lane_exit_matrix, preferred_element_type=f32
    )
    projected = lax.psum(partial_rows.astype(jnp.bfloat16), "tp").astype(jnp.float32).astype(bf16)
    own_stream, normed, own_cols = full_norm(
        projected, skipline_stream, specialist_scaling_vector, col_start, d_local
    )
    share = dispatcher_scores / jnp.sum(dispatcher_scores, axis=1, keepdims=True)
    experts = lax.axis_size("sp")
    top = selected_specialists.shape[1]
    capacity = 2 * tok_local * top // experts
    flat_routes = selected_specialists.reshape(-1)
    hits = (flat_routes[:, None] == jnp.arange(experts, dtype=jnp.int32)[None, :]).astype(jnp.int32)
    ranks = jnp.sum((jnp.cumsum(hits, axis=0) - hits) * hits, axis=1)
    slot_ids = flat_routes * capacity + ranks
    slot_grid = jnp.arange(experts * capacity, dtype=jnp.int32)
    matched = slot_grid[:, None] == slot_ids[None, :]
    token_of = jnp.arange(tok_local * top, dtype=jnp.int32) // top
    slot_token = jnp.sum(jnp.where(matched, token_of[None, :], 0), axis=1)
    slot_live = jnp.any(matched, axis=1)
    gate_w = specialist_valve_matrix[0]
    up_w = specialist_widen_matrix[0]
    down_w = specialist_shrink_matrix[0]
    bf_zero = jnp.zeros((), bf16)
    dispatch = jnp.where(slot_live[:, None], own_cols[slot_token], bf_zero).reshape(
        experts, capacity, d_local
    )
    arrived = lax.all_to_all(dispatch, "sp", split_axis=0, concat_axis=0, tiled=True)
    piece = lax.all_gather(arrived, "tp", axis=2, tiled=True)
    gate_part = jnp.einsum("snd,df->snf", piece, gate_w, preferred_element_type=f32)
    up_part = jnp.einsum("snd,df->snf", piece, up_w, preferred_element_type=f32)
    hidden = (jax.nn.silu(gate_part) * up_part).astype(bf16)
    flat_hidden = hidden.reshape(experts * capacity, hidden.shape[2])
    down_part = jnp.dot(flat_hidden, down_w, preferred_element_type=f32).astype(bf16)
    summed = lax.psum_scatter(
        down_part.astype(f32).astype(jnp.bfloat16), "tp", scatter_dimension=1, tiled=True
    ).astype(jnp.float32)
    expert_out = summed.astype(bf16).reshape(experts, capacity, d_local)
    returned = lax.all_to_all(expert_out, "sp", split_axis=0, concat_axis=0, tiled=True).reshape(
        experts * capacity, d_local
    )
    picked = returned[slot_ids].reshape(tok_local, top, d_local)
    combined = jnp.sum(lax.optimization_barrier(picked).astype(f32) * share[:, :, None], axis=1)
    return (own_stream + combined).astype(bf16)


def solution(mesh):
    placed = (
        P("tp", "sp"),
        P("tp", None),
        P("tp", None),
        P("tp"),
        P("tp", None, None),
        P("tp", None, None),
        P("tp", None, None),
        P("tp", None, None),
        P("tp"),
        P("tp", "sp"),
        P("tp", None),
        P("sp", None),
        P(),
        P("sp", None),
        P("sp", None),
        P("sp", None, "tp"),
        P("sp", None, "tp"),
        P("sp", "tp", None),
    )
    return jax.shard_map(
        per_device, mesh=mesh, in_specs=placed, out_specs=P("sp", "tp"), check_vma=False
    )
```

profile of v0, /device:TPU:0, one launch (start us, length us, event | category | flops | bytes accessed | tf_op | source)
XLA Modules:
  0.0 370.3 jit_solution(14271177628407040252)
XLA Ops:
  6.5 0.8 exp.13
  7.4 0.9 fusion.59
  8.2 1.6 fusion.45
  9.8 1.6 fusion.49
  11.4 1.4 subtract_add_fusion.6
  12.9 1.0 add_add_fusion.5
  13.9 0.3 subtract_add_fusion.5
  14.3 0.6 add_add_fusion.4
  14.9 0.3 subtract_add_fusion.4
  15.2 0.6 add_add_fusion.3
  15.8 0.3 subtract_add_fusion.3
  16.2 0.6 add_add_fusion.2
  16.8 0.3 subtract_add_fusion.2
  17.2 0.6 add_add_fusion.1
  18.1 1.4 add_add_fusion
  19.5 1.4 multiply_subtract_fusion
  20.9 1.0 slice.168
  21.9 1.3 copy.32
  23.2 32.4 %all-gather = f32[128,64,1]{1,2,0:T(1,128)S(1)} all-gather(f32[16,64,1]{1,2,0:T(1,128)S(1)} %copy.32), channel_id=2, replica_groups=mesh['sp'=8,'tp'=4] {'sp'}, dimensions={0}, use_global_device_ids=true | all-gather | bytes 36864 | tf_op jit(solution)/shard_map/all_gather | solution.py:12
  55.5 1.0 slice.169
  56.5 1.2 copy.33
  57.8 30.5 %all-gather.1 = f32[128,64,1]{1,2,0:T(1,128)S(1)} all-gather(f32[16,64,1]{1,2,0:T(1,128)S(1)} %copy.33), channel_id=3, replica_groups=mesh['sp'=8,'tp'=4] {'sp'}, dimensions={0}, use_global_device_ids=true | all-gather | bytes 36864 | tf_op jit(solution)/shard_map/all_gather | solution.py:12
  88.3 2.0 slice.170
  90.4 1.2 copy.34
  91.6 30.5 %all-gather.2 = f32[128,64,1]{1,2,0:T(1,128)S(1)} all-gather(f32[16,64,1]{1,2,0:T(1,128)S(1)} %copy.34), channel_id=4, replica_groups=mesh['sp'=8,'tp'=4] {'sp'}, dimensions={0}, use_global_device_ids=true | all-gather | bytes 36864 | tf_op jit(solution)/shard_map/all_gather | solution.py:12
  122.2 2.0 slice.171
  124.2 1.2 copy.35
  125.4 30.5 %all-gather.3 = f32[128,64,1]{1,2,0:T(1,128)S(1)} all-gather(f32[16,64,1]{1,2,0:T(1,128)S(1)} %copy.35), channel_id=5, replica_groups=mesh['sp'=8,'tp'=4] {'sp'}, dimensions={0}, use_global_device_ids=true | all-gather | bytes 36864 | tf_op jit(solution)/shard_map/all_gather | solution.py:12
  156.4 1.9 fusion.22
  158.2 1.9 fusion.42
  160.1 1.5 convolution_convert_fusion.1
  162.3 0.6 reduce-window.6
  163.7 35.4 %all-reduce.30.cloned.1.call-done = bf16[128,4096]{1,0:T(8,128)(2,1)} async-done(((bf16[128,4096]{1,0:T(8,128)(2,1)}), bf16[128,4096]{1,0:T(8,128)(2,1)}) %all-reduce.30.cloned.1.call-update) | async-done | bytes 1048592 | tf_op jit(solution)/shard_map/psum | solution.py:142
  199.0 1.8 add_convert_fusion
  201.3 1.0 copy-done.1
  202.5 2.1 gather_fusion
  204.7 30.6 %all_to_all.10 = bf16[8,64,1024]{2,1,0:T(8,128)(2,1)} all-to-all(bf16[8,64,1024]{2,1,0:T(8,128)(2,1)S(1)} %broadcast_select_fusion), channel_id=1, replica_groups=mesh['sp'=8,'tp'=4] {'sp'}, dimensions={0} | all-to-all | bytes 2097152 | tf_op jit(solution)/shard_map/all_to_all | solution.py:166
  235.4 33.4 %all-gather.6.cloned.1.call-done = bf16[8,64,4096]{2,1,0:T(8,128)(2,1)} async-done(((bf16[8,64,1024]{2,1,0:T(8,128)(2,1)}), bf16[8,64,4096]{2,1,0:T(8,128)(2,1)}) %all-gather.6.cloned.1.call-update) | async-done | bytes 4194320 | tf_op jit(solution)/shard_map/all_gather | solution.py:167
  268.9 5.9 %fusion.7 = f32[8,64,512]{2,1,0:T(8,128)S(1)} fusion(bf16[8,64,4096]{2,1,0:T(8,128)(2,1)} %all-gather.6.cloned.1.call-done, bf16[1,4096,512]{2,1,0:T(8,128)(2,1)} %param.35), kind=kOutput, calls=%fused_computation.17 | convolution fusion | flops 2147483648 | bytes 9437184 | tf_op jit(solution)/shard_map/snd,df->snf/dot_general | solution.py:168
  274.8 2.4 fusion.12
  277.3 4.3 %convolution_convert_fusion = bf16[512,4096]{1,0:T(8,128)(2,1)} fusion(bf16[512,512]{1,0:T(8,128)(2,1)S(1)} %bitcast.169, bf16[1,512,4096]{2,1,0:T(8,128)(2,1)S(1)} %copy-done.8), kind=kOutput, calls=%fused_computation.12 | convolution fusion | flops 2149580800 | bytes 8912896 | tf_op jit(solution)/shard_map/dot_general | solution.py:172
  281.6 44.6 %reduce-scatter.2.cloned.1.call-done = bf16[512,1024]{1,0:T(8,128)(2,1)} async-done(((bf16[512,4096]{1,0:T(8,128)(2,1)}), bf16[512,1024]{1,0:T(8,128)(2,1)}) %reduce-scatter.2.cloned.1.call-update) | async-done | bytes 1048592 | tf_op jit(solution)/shard_map/reduce_scatter | solution.py:173
  326.1 5.5 %all-to-all-start.1 = ((bf16[8,64,1024]{2,1,0:T(8,128)(2,1)}), bf16[8,64,1024]{2,1,0:T(8,128)(2,1)S(1)}, u32[]{:S(2)}, u32[]{:S(2)}) async-start(bf16[8,64,1024]{2,1,0:T(8,128)(2,1)} %bitcast.156), calls=%async_computation.2 | async-start | bytes 2097152 | tf_op jit(solution)/shard_map/all_to_all | solution.py:177
  332.1 25.2 %all-to-all-done.1 = bf16[8,64,1024]{2,1,0:T(8,128)(2,1)S(1)} async-done(((bf16[8,64,1024]{2,1,0:T(8,128)(2,1)}), bf16[8,64,1024]{2,1,0:T(8,128)(2,1)S(1)}, u32[]{:S(2)}, u32[]{:S(2)}) %all-to-all-start.1) | async-done | bytes 1048608 | tf_op jit(solution)/shard_map/all_to_all | solution.py:177
  357.3 2.0 gather_fusion.1
  359.3 1.2 reshape.140
  360.5 1.4 multiply_reduce_fusion.1
  361.9 1.8 add_convert_fusion.1
  (66 shorter events, 3.4 us)
Async XLA Ops:
  6.5 153.6 %copy-start = (bf16[256,4096]{1,0:T(8,128)(2,1)S(1)}, bf16[256,4096]{1,0:T(8,128)(2,1)}, u32[]{:S(2)}) copy-start(bf16[256,4096]{1,0:T(8,128)(2,1)} %param.30) | copy-start | bytes 6291460
  6.5 6.3 %copy-start.3 = (f32[16,128]{1,0:T(8,128)S(1)}, f32[16,128]{1,0:T(8,128)}, u32[]{:S(2)}) copy-start(f32[16,128]{1,0:T(8,128)} %param.29) | copy-start | bytes 24580
  6.5 192.5 %all-reduce.30.cloned.1.call-start = ((), (), s32[]{:S(2)}) async-start(), calls=%async_computation.3 | async-start | bytes 2097152 | tf_op jit(solution)/shard_map/psum | solution.py:142
  20.9 135.3 %copy-start.6 = (f32[256]{0:T(256)S(1)}, f32[256]{0:T(256)}, u32[]{:S(2)}) copy-start(f32[256]{0:T(256)} %param.28) | copy-start | bytes 3076
  21.9 136.3 %copy-start.2 = (bf16[256,128]{1,0:T(8,128)(2,1)S(1)}, bf16[256,128]{1,0:T(8,128)(2,1)}, u32[]{:S(2)}) copy-start(bf16[256,128]{1,0:T(8,128)(2,1)} %param.20) | copy-start | bytes 196612
  156.3 5.6 %copy-start.4 = (s32[128,2]{0,1:T(2,128)S(1)}, s32[128,2]{0,1:T(2,128)}, u32[]{:S(2)}) copy-start(s32[128,2]{0,1:T(2,128)} %param.33) | copy-start | bytes 3076
  161.6 107.2 %all-gather.6.cloned.1.call-start = ((), (), s32[]{:S(2)}) async-start(), calls=%async_computation.4 | async-start | bytes 5242880 | tf_op jit(solution)/shard_map/all_gather | solution.py:167
  163.5 38.9 %dynamic-slice-start = ((f32[4096]{0:T(1024)}, s32[]{:T(128)}), f32[1024]{0:T(1024)S(1)}, s32[]{:S(2)}) async-start(f32[4096]{0:T(1024)} %param.32, s32[]{:T(128)} %select_n.74), calls=%async_computation.6 | async-start | bytes 8704 | tf_op jit(solution)/shard_map/dynamic_slice | solution.py:61
  201.0 1.3 copy-start.1
  235.4 90.8 %reduce-scatter.2.cloned.1.call-start = ((), (), s32[]{:S(2)}) async-start(), calls=%async_computation.5 | async-start | bytes 5242880 | tf_op jit(solution)/shard_map/reduce_scatter | solution.py:173
  268.8 5.9 %copy-start.7 = (bf16[1,4096,512]{2,1,0:T(8,128)(2,1)S(1)}, bf16[1,4096,512]{2,1,0:T(8,128)(2,1)}, u32[]{:S(2)}) copy-start(bf16[1,4096,512]{2,1,0:T(8,128)(2,1)} %param.36) | copy-start | bytes 12582916
  268.9 5.9 %copy-start.9 = (bf16[8,64,4096]{2,1,0:T(8,128)(2,1)S(1)}, bf16[8,64,4096]{2,1,0:T(8,128)(2,1)}, u32[]{:S(2)}) copy-start(bf16[8,64,4096]{2,1,0:T(8,128)(2,1)} %all-gather.6.cloned.1.call-done) | copy-start | bytes 12582916
  274.8 2.5 copy-start.8
  281.6 50.4 %copy-start.5 = (f32[128,2]{0,1:T(2,128)S(1)}, f32[128,2]{0,1:T(2,128)}, u32[]{:S(2)}) copy-start(f32[128,2]{0,1:T(2,128)} %param.34) | copy-start | bytes 3076
  326.1 31.2 %all-to-all-start.1 = ((bf16[8,64,1024]{2,1,0:T(8,128)(2,1)}), bf16[8,64,1024]{2,1,0:T(8,128)(2,1)S(1)}, u32[]{:S(2)}, u32[]{:S(2)}) async-start(bf16[8,64,1024]{2,1,0:T(8,128)(2,1)} %bitcast.156), calls=%async_computation.2 | async-start | bytes 2097152 | tf_op jit(solution)/shard_map/all_to_all | solution.py:177
Sparse Core Ops, SparseCore 0:
  161.8 37.2 all-reduce.29
  235.5 33.3 all-gather.5
  281.7 44.3 reduce-scatter.1
where the time goes:
time: 371 us; the launch traced here: 370 us
  blocking collectives  155 us (42%)
  waiting for transfers between devices  139 us (37%)
  matrix products  21 us (6%)
  local copies, waits for them, and re-layouts  19.4 us (5%)
  other arithmetic  17.3 us (5%)
  between operations  13.5 us (4%)
  starting transfers between devices  5.77 us (2%)
    all_gather x4, blocking collectives, carried_in(): pieces = jax.tree.map(lambda part: lax.all_gather(part, axis), value)  124 us
    reduce_scatter x1, waiting for transfers between devices, per_device(): lax.psum_scatter(down_part.astype(f32).astype(jnp.bfloat16), 'tp', scatte...  44.6 us
    psum x1, waiting for transfers between devices, per_device(): lax.psum(partial_rows.astype(jnp.bfloat16), 'tp').astype(jnp.float32)  35.4 us
    all_gather x1, waiting for transfers between devices, per_device(): piece = lax.all_gather(arrived, 'tp', axis=2, tiled=True)  33.4 us
    all_to_all x1, blocking collectives, per_device(): lax.all_to_all(dispatch, 'sp', split_axis=0, concat_axis=0, tiled=True)  30.6 us
    all_to_all x1, waiting for transfers between devices, per_device(): lax.all_to_all(expert_out, 'sp', split_axis=0, concat_axis=0, tiled=True)  25.2 us
  transfers between devices with their start and end apart: 4, of which 4 were waited for; matrix products, arithmetic and copies ran while one was open for 1% of the time, Pallas kernels for 0%

commit v1 on v0

v1 whole, which is shorter than its diff:
```python
import jax
import jax.numpy as jnp
from jax import lax
from jax.experimental import pallas as pl
from jax.experimental.pallas import tpu as pltpu
from jax.sharding import PartitionSpec as P

EPS = 1e-06
F32 = jnp.float32
BF16 = jnp.bfloat16


def swap(value, axis, bits):
    count = lax.axis_size(axis)
    return lax.ppermute(value, axis, [(i, i ^ bits) for i in range(count)])


def expanded(columns, wide):
    return jnp.concatenate(
        [
            jnp.broadcast_to(columns[:, g : g + 1], (columns.shape[0], wide))
            for g in range(columns.shape[1])
        ],
        axis=1,
    )


def later(value, offset):
    if offset % 8:
        return pltpu.roll(value, offset, axis=0)
    return jnp.concatenate([value[-offset:], value[:-offset]], axis=0)


def block_rows(matrix, copies, inner):
    _, wide = matrix.shape
    spread = (
        lax.broadcasted_iota(jnp.int32, (wide, copies * wide), 1) % wide
        == lax.broadcasted_iota(jnp.int32, (wide, copies * wide), 0)
    ).astype(BF16)
    tiled = jnp.dot(matrix.astype(BF16), spread, preferred_element_type=F32)
    keep = (
        lax.broadcasted_iota(jnp.int32, tiled.shape, 0) // inner
        == lax.broadcasted_iota(jnp.int32, tiled.shape, 1) // wide
    )
    return jnp.where(keep, tiled, 0.0).astype(BF16)


def across(left, right):
    return lax.dot_general(left, right, (((1,), (1,)), ((), ())), preferred_element_type=F32)


def scan_kernel(
    signal_ref, damp_ref, turn_ref, pace_ref, ent_re_ref, ent_im_ref, shrink_ref,
    emit_re_ref, emit_im_ref, bypass_ref,
    summary_ref, local_ref, powers_ref, gone_ref,
):
    groups, states = damp_ref.shape
    length = shrink_ref.shape[1]
    lanes = ent_re_ref.shape[1]
    total = groups * states
    square = (groups, groups)
    step = jnp.where(
        lax.broadcasted_iota(jnp.int32, square, 0) == lax.broadcasted_iota(jnp.int32, square, 1),
        jnp.broadcast_to(pace_ref[...], square),
        0.0,
    )
    step = jnp.exp(jnp.sum(step, axis=1, keepdims=True))
    damp, turn = damp_ref[...], turn_ref[...]
    rate, angle = damp * step, turn * step
    size, cosine, sine = jnp.exp(rate), jnp.cos(angle), jnp.sin(angle)
    half = jnp.sin(0.5 * angle)
    series = rate * (1.0 + rate * 0.5 * (1.0 + rate * (1.0 / 3.0) * (1.0 + rate * 0.25)))
    less_one = jnp.where(jnp.abs(rate) < 0.05, series, size - 1.0)
    num_re = less_one * cosine - 2.0 * half * half
    num_im = size * sine
    denom = damp * damp + turn * turn
    own_group = (
        lax.broadcasted_iota(jnp.int32, (groups, total), 1) // states
        == lax.broadcasted_iota(jnp.int32, (groups, total), 0)
    )

    def row(value):
        spread = jnp.concatenate([value] * groups, axis=1)
        return jnp.sum(jnp.where(own_group, spread, 0.0), axis=0, keepdims=True)

    fac_re = row((num_re * damp + num_im * turn) / denom)
    fac_im = row((num_im * damp - num_re * turn) / denom)
    pow_re, pow_im = [row(size * cosine)], [row(num_im)]
    while 2 ** len(pow_re) < length:
        re, im = pow_re[-1], pow_im[-1]
        pow_re.append(re * re - im * im)
        pow_im.append(2.0 * re * im)
    for i, value in enumerate(pow_re + pow_im):
        powers_ref[i : i + 1, :] = value
    last = pow_re[-1], pow_im[-1]
    full_re = last[0] * last[0] - last[1] * last[1]
    full_im = 2.0 * last[0] * last[1]

    shrink = shrink_ref[...]
    summed = shrink
    position = lax.broadcasted_iota(jnp.int32, shrink.shape, 1)
    offset = 1
    while offset < length:
        summed = summed + jnp.where(
            position >= offset, pltpu.roll(summed, offset, axis=1), 0.0
        )
        offset *= 2
    columns = jnp.transpose(jnp.exp(jnp.concatenate([shrink, summed], axis=0)))
    gone_ref[...] = columns[:, groups:]
    all_gone = expanded(columns[length - 8 :, groups:], states)[7:8]
    flipped = jnp.transpose(signal_ref[...].astype(F32))
    local = bypass_ref[...] * flipped
    flipped = flipped.astype(BF16)
    ent_re = block_rows(ent_re_ref[...].reshape(groups * lanes, states), groups, lanes)
    ent_im = block_rows(ent_im_ref[...].reshape(groups * lanes, states), groups, lanes)
    emit_re = block_rows(emit_re_ref[...].reshape(groups * lanes, states), groups, lanes)
    emit_im = block_rows(emit_im_ref[...].reshape(groups * lanes, states), groups, lanes)
    wide = min(128, total)
    time = lax.broadcasted_iota(jnp.int32, (length, wide), 0)
    each = wide // states
    xs_re, xs_im = [], []
    for block in range(total // wide):
        cut = slice(block * wide, (block + 1) * wide)
        raw_re = jnp.dot(flipped, ent_re[:, cut], preferred_element_type=F32)
        raw_im = jnp.dot(flipped, ent_im[:, cut], preferred_element_type=F32)
        f_re, f_im = fac_re[:, cut], fac_im[:, cut]
        x_re = f_re * raw_re - f_im * raw_im
        x_im = f_re * raw_im + f_im * raw_re
        first = block * each
        decay = expanded(columns[:, first : first + each], states)
        decay = jnp.where(time >= 1, decay, 0.0)
        offset = 1
        for p_re, p_im in zip(pow_re, pow_im):
            a_re, a_im = p_re[:, cut], p_im[:, cut]
            s_re, s_im = later(x_re, offset), later(x_im, offset)
            x_re = x_re + decay * (a_re * s_re - a_im * s_im)
            x_im = x_im + decay * (a_re * s_im + a_im * s_re)
            if 2 * offset < length:
                decay = decay * later(decay, offset)
            offset *= 2
        local = local + across(x_re.astype(BF16), emit_re[:, cut])
        local = local - across(x_im.astype(BF16), emit_im[:, cut])
        xs_re.append(x_re[length - 8 :])
        xs_im.append(x_im[length - 8 :])
    local_ref[...] = local
    ends = []
    for value in (
        full_re * all_gone,
        full_im * all_gone,
        jnp.concatenate(xs_re, axis=1)[7:8],
        jnp.concatenate(xs_im, axis=1)[7:8],
    ):
        ends += [value[:, : total // 2], value[:, total // 2 :]]
    ends = jnp.concatenate(ends, axis=0)
    for s in range(summary_ref.shape[0]):
        summary_ref[s] = ends


def readout_kernel(
    mine_ref, pieces_ref, local_ref, powers_ref, gone_ref, emit_re_ref, emit_im_ref, mixed_ref
):
    groups, lanes, states = emit_re_ref.shape
    length, total = local_ref.shape[0], powers_ref.shape[1]
    mine = mine_ref[0]
    re = jnp.zeros((2, pieces_ref.shape[2]), F32)
    im = re
    for s in range(pieces_ref.shape[0] - 1):
        piece = pieces_ref[s]
        m_re, m_im, a_re, a_im = piece[0:2], piece[2:4], piece[4:6], piece[6:8]
        new_re = m_re * re - m_im * im + a_re
        new_im = m_re * im + m_im * re + a_im
        re = jnp.where(s < mine, new_re, re)
        im = jnp.where(s < mine, new_im, im)
    re = jnp.concatenate([re[0:1], re[1:2]], axis=1)
    im = jnp.concatenate([im[0:1], im[1:2]], axis=1)
    emit_re = block_rows(emit_re_ref[...].reshape(groups * lanes, states), groups, lanes)
    emit_im = block_rows(emit_im_ref[...].reshape(groups * lanes, states), groups, lanes)
    value = local_ref[...]
    bits = powers_ref.shape[0] // 2
    wide = min(128, total)
    each = wide // states
    near = lax.broadcasted_iota(jnp.int32, (8, wide), 0) + 1
    for block in range(total // wide):
        cut = slice(block * wide, (block + 1) * wide)
        p_re = [powers_ref[i : i + 1, cut] for i in range(bits)]
        p_im = [powers_ref[bits + i : bits + i + 1, cut] for i in range(bits)]
        c_re = jnp.broadcast_to(re[:, cut], (8, wide))
        c_im = jnp.broadcast_to(im[:, cut], (8, wide))
        for bit in range(4):
            a_re, a_im = p_re[bit], p_im[bit]
            on = (near >> bit) & 1 == 1
            c_re, c_im = (
                jnp.where(on, c_re * a_re - c_im * a_im, c_re),
                jnp.where(on, c_re * a_im + c_im * a_re, c_im),
            )
        bit = 3
        while c_re.shape[0] < length:
            a_re, a_im = p_re[bit], p_im[bit]
            c_re, c_im = (
                jnp.concatenate([c_re, c_re * a_re - c_im * a_im], axis=0),
                jnp.concatenate([c_im, c_re * a_im + c_im * a_re], axis=0),
            )
            bit += 1
        gone = expanded(gone_ref[:, block * each : (block + 1) * each], states)
        value = value + across((c_re * gone).astype(BF16), emit_re[:, cut])
        value = value - across((c_im * gone).astype(BF16), emit_im[:, cut])
    mixed_ref[...] = jax.nn.gelu(value).astype(BF16)


def vmem(count):
    return [pl.BlockSpec(memory_space=pltpu.VMEM)] * count


def hbm(count):
    return [pl.BlockSpec(memory_space=pltpu.HBM)] * count


def staged(kernel, first, count):
    def run(*refs):
        sources, buffers, sems = refs[first : first + count], refs[-count - 1 : -1], refs[-1]
        copies = [
            pltpu.make_async_copy(source, buffer, sems.at[i])
            for i, (source, buffer) in enumerate(zip(sources, buffers))
        ]
        for copy in copies:
            copy.start()
        for copy in copies:
            copy.wait()
        kernel(*refs[:first], *buffers, *refs[first + count : -count - 1])

    return run


def stage(args):
    return [pltpu.VMEM(arg.shape, arg.dtype) for arg in args] + [
        pltpu.SemaphoreType.DMA((len(args),))
    ]


def mixer(place, signal, damp, turn, pace, ent_re, ent_im, emit_re, emit_im, bypass, shrink):
    groups, states = damp.shape
    channels, length = signal.shape
    total = groups * states
    count = lax.axis_size("sp")
    bits = (length - 1).bit_length()
    args = (
        signal, damp, turn, pace.reshape(1, groups), ent_re.transpose(0, 2, 1),
        ent_im.transpose(0, 2, 1), shrink, emit_re, emit_im, bypass.reshape(1, channels),
    )
    summary, local, powers, gone = pl.pallas_call(
        staged(scan_kernel, 0, len(args)),
        in_specs=hbm(len(args)),
        out_specs=vmem(4),
        out_shape=[
            jax.ShapeDtypeStruct((count, 8, total // 2), F32),
            jax.ShapeDtypeStruct((length, channels), F32),
            jax.ShapeDtypeStruct((2 * bits, total), F32),
            jax.ShapeDtypeStruct((length, groups), F32),
        ],
        scratch_shapes=stage(args),
        compiler_params=pltpu.CompilerParams(vmem_limit_bytes=16 * 2**20),
        name="mixer_scan",
    )(*args)
    pieces = lax.all_to_all(summary, "sp", 0, 0, tiled=True)
    args = (emit_re, emit_im)
    return pl.pallas_call(
        staged(readout_kernel, 5, len(args)),
        in_specs=[pl.BlockSpec(memory_space=pltpu.SMEM)] + vmem(4) + hbm(len(args)),
        out_specs=vmem(1)[0],
        out_shape=jax.ShapeDtypeStruct((length, channels), BF16),
        scratch_shapes=stage(args),
        compiler_params=pltpu.CompilerParams(vmem_limit_bytes=16 * 2**20),
        name="mixer_readout",
    )(place, pieces, local, powers, gone, *args)


def cut_kernel(n_tp, place_ref, exit_ref, skip_ref, *refs):
    outs, sems = refs[: n_tp + 1], refs[n_tp + 1]
    me = place_ref[1]
    wide = outs[0].shape[1]
    copies = []
    for k in range(n_tp):
        source = exit_ref.at[:, pl.ds(pl.multiple_of((me ^ k) * wide, wide), wide)]
        copies.append(pltpu.make_async_copy(source, outs[k], sems.at[k]))
    source = skip_ref.at[:, pl.ds(pl.multiple_of(me * wide, wide), wide)]
    copies.append(pltpu.make_async_copy(source, outs[n_tp], sems.at[n_tp]))
    for copy in copies:
        copy.start()
    for copy in copies:
        copy.wait()


def cut_blocks(place, exit_matrix, skip, n_tp):
    wide = skip.shape[1] // n_tp
    block = jax.ShapeDtypeStruct((exit_matrix.shape[0], wide), BF16)
    anywhere = pl.BlockSpec(memory_space=pl.ANY)
    *exits, own_skip = pl.pallas_call(
        lambda *refs: cut_kernel(n_tp, *refs),
        in_specs=[pl.BlockSpec(memory_space=pltpu.SMEM)] + hbm(2),
        out_specs=[anywhere] * (n_tp + 1),
        out_shape=[block] * n_tp + [jax.ShapeDtypeStruct((skip.shape[0], wide), BF16)],
        scratch_shapes=[pltpu.SemaphoreType.DMA((n_tp + 1,))],
        compiler_params=pltpu.CompilerParams(vmem_limit_bytes=2**20),
        name="cut_blocks",
    )(place, exit_matrix, skip)
    return exits, own_skip


def route_kernel(experts, capacity, place_ref, chosen_ref, score_ref, pick_ref, high_ref, low_ref):
    chosen, score = chosen_ref[...], score_ref[...]
    length, top = chosen.shape
    share = score / jnp.sum(score, axis=1, keepdims=True)
    lane = lax.broadcasted_iota(jnp.int32, (length, experts), 1)
    named = [chosen[:, k : k + 1] == lane for k in range(top)]
    counted = sum(jnp.where(one, 1.0, 0.0) for one in named)
    before = (
        lax.broadcasted_iota(jnp.int32, (length, length), 0)
        > lax.broadcasted_iota(jnp.int32, (length, length), 1)
    )
    ranks = jnp.dot(
        jnp.where(before, 1.0, 0.0).astype(BF16), counted.astype(BF16),
        preferred_element_type=F32,
    )
    grid = lax.broadcasted_iota(jnp.int32, (length, experts * capacity), 1)
    pick = weight = 0.0
    for k, one in enumerate(named):
        rank = jnp.sum(jnp.where(one, ranks, 0.0), axis=1, keepdims=True).astype(jnp.int32)
        hit = grid == (chosen[:, k : k + 1] ^ place_ref[0]) * capacity + rank
        pick = pick + jnp.where(hit, 1.0, 0.0)
        weight = weight + jnp.where(hit, share[:, k : k + 1], 0.0)
    pick_ref[...] = jnp.transpose(pick).astype(BF16)
    high = weight.astype(BF16)
    high_ref[...] = high
    low_ref[...] = (weight - high.astype(F32)).astype(BF16)


def route(place, chosen, score, experts, capacity):
    length = chosen.shape[0]
    weight = jax.ShapeDtypeStruct((length, experts * capacity), BF16)
    return pl.pallas_call(
        lambda *refs: route_kernel(experts, capacity, *refs),
        in_specs=[pl.BlockSpec(memory_space=pltpu.SMEM)] + vmem(2),
        out_specs=vmem(3),
        out_shape=[jax.ShapeDtypeStruct((experts * capacity, length), BF16), weight, weight],
        compiler_params=pltpu.CompilerParams(vmem_limit_bytes=8 * 2**20),
        name="route",
    )(place, chosen, score)


def pack_kernel(*refs):
    height = refs[0].shape[0]
    for i, ref in enumerate(refs[:-1]):
        refs[-1][i * height : (i + 1) * height] = ref[...]


def pack(parts):
    height, wide = parts[0].shape
    return pl.pallas_call(
        pack_kernel,
        in_specs=vmem(len(parts)),
        out_specs=vmem(1)[0],
        out_shape=jax.ShapeDtypeStruct((height * len(parts), wide), BF16),
        compiler_params=pltpu.CompilerParams(vmem_limit_bytes=4 * 2**20),
        name="pack",
    )(*parts)


def project_kernel(n_tp, *refs):
    mixed, exits = refs[:n_tp], refs[n_tp : 2 * n_tp]
    skip_ref, pick_ref, stream_ref, *rows = refs[2 * n_tp :]
    total = 0.0
    for k in range(n_tp):
        total = total + jnp.dot(mixed[k][...], exits[k][...], preferred_element_type=F32)
    stream = (skip_ref[...].astype(F32) + total.astype(BF16).astype(F32)).astype(BF16)
    stream_ref[...] = stream
    picked = jnp.dot(pick_ref[...], stream, preferred_element_type=F32).astype(BF16)
    height = rows[0].shape[0]
    for k, ref in enumerate(rows):
        ref[...] = picked[k * height : (k + 1) * height]


def project(mixed, exits, skip, pick, experts):
    length, d_local = skip.shape
    n_tp = len(mixed)
    return pl.pallas_call(
        lambda *refs: project_kernel(n_tp, *refs),
        in_specs=vmem(2 * n_tp + 2),
        out_specs=vmem(1 + experts),
        out_shape=[jax.ShapeDtypeStruct((length, d_local), BF16)]
        + [jax.ShapeDtypeStruct((pick.shape[0] // experts, d_local), BF16)] * experts,
        compiler_params=pltpu.CompilerParams(vmem_limit_bytes=12 * 2**20),
        name="project",
    )(*mixed, *exits, skip, pick)


def fold_kernel(pairs, *refs):
    outs = refs[2 * pairs :]
    share = len(outs) // pairs
    for i in range(pairs):
        total = (refs[i][...].astype(F32) + refs[pairs + i][...].astype(F32)).astype(BF16)
        height = outs[i * share].shape[0]
        for j in range(share):
            outs[i * share + j][...] = total[j * height : (j + 1) * height]


def fold(kept, moved, share):
    rows, wide = kept[0].shape
    return pl.pallas_call(
        lambda *refs: fold_kernel(len(kept), *refs),
        in_specs=vmem(2 * len(kept)),
        out_specs=vmem(len(kept) * share),
        out_shape=[jax.ShapeDtypeStruct((rows // share, wide), BF16)] * (len(kept) * share),
        compiler_params=pltpu.CompilerParams(vmem_limit_bytes=6 * 2**20),
        name="fold",
    )(*kept, *moved)


def combine_kernel(stream_ref, high_ref, low_ref, *refs):
    out_ref = refs[-1]
    total = stream_ref[...].astype(F32)
    back = jnp.concatenate([ref[...] for ref in refs[:-1]], axis=0)
    total = total + jnp.dot(high_ref[...], back, preferred_element_type=F32)
    total = total + jnp.dot(low_ref[...], back, preferred_element_type=F32)
    out_ref[...] = total.astype(BF16)


def combine(stream, high, low, back):
    return pl.pallas_call(
        combine_kernel,
        in_specs=vmem(3 + len(back)),
        out_specs=vmem(1)[0],
        out_shape=jax.ShapeDtypeStruct(stream.shape, BF16),
        compiler_params=pltpu.CompilerParams(vmem_limit_bytes=8 * 2**20),
        name="combine",
    )(stream, high, low, *back)


def ffn_kernel(n_tp, width, place_ref, *refs):
    pieces = refs[:n_tp]
    scale_ref, gate_ref, up_ref, down_ref = refs[n_tp : n_tp + 4]
    outs = refs[n_tp + 4 :]
    me = place_ref[1]
    d_local = pieces[0].shape[1]
    square = gate = up = 0.0
    for k in range(n_tp):
        rows = pieces[k][...].astype(F32)
        square = square + jnp.sum(rows * rows, axis=1, keepdims=True)
        place = pl.multiple_of((me ^ k) * d_local, d_local)
        scaled = (rows * scale_ref[me ^ k]).astype(BF16)
        gate = gate + jnp.dot(
            scaled, gate_ref[pl.ds(place, d_local), :], preferred_element_type=F32
        )
        up = up + jnp.dot(scaled, up_ref[pl.ds(place, d_local), :], preferred_element_type=F32)
    inv_rms = lax.rsqrt(square / width + EPS)
    gate = gate * inv_rms
    hidden = (gate * jax.nn.sigmoid(gate) * (up * inv_rms)).astype(BF16)
    for k in range(n_tp):
        place = pl.multiple_of((me ^ k) * d_local, d_local)
        outs[k][...] = jnp.dot(
            hidden, down_ref[:, pl.ds(place, d_local)], preferred_element_type=F32
        ).astype(BF16)


def load_kernel(*refs):
    half = len(refs) // 2
    sems = refs[-1]
    copies = [
        pltpu.make_async_copy(refs[i], refs[half + i], sems.at[i]) for i in range(half)
    ]
    for copy in copies:
        copy.start()
    for copy in copies:
        copy.wait()


def load(*weights):
    return pl.pallas_call(
        load_kernel,
        in_specs=hbm(len(weights)),
        out_specs=vmem(len(weights)),
        out_shape=[jax.ShapeDtypeStruct(w.shape, w.dtype) for w in weights],
        scratch_shapes=[pltpu.SemaphoreType.DMA((len(weights),))],
        compiler_params=pltpu.CompilerParams(vmem_limit_bytes=16 * 2**20),
        name="load",
    )(*weights)


def ffn(place, pieces, scale, gate_w, up_w, down_w):
    n_tp = len(pieces)
    rows, d_local = pieces[0].shape
    width, units = gate_w.shape
    return pl.pallas_call(
        lambda *refs: ffn_kernel(n_tp, width, *refs),
        in_specs=[pl.BlockSpec(memory_space=pltpu.SMEM)] + vmem(n_tp + 4),
        out_specs=vmem(n_tp),
        out_shape=[jax.ShapeDtypeStruct((rows, d_local), BF16)] * n_tp,
        compiler_params=pltpu.CompilerParams(vmem_limit_bytes=24 * 2**20),
        cost_estimate=pl.CostEstimate(
            flops=6 * rows * width * units,
            bytes_accessed=6 * width * units + 4 * rows * width,
            transcendentals=rows * units,
        ),
        name="expert_ffn",
    )(place, *pieces, scale, gate_w, up_w, down_w)


def gather_pieces(own, n_tp):
    pieces = {0: own}
    bit = n_tp // 2
    while bit:
        for k in list(pieces):
            pieces[k ^ bit] = swap(pieces[k], "tp", bit)
        bit //= 2
    return [pieces[k] for k in range(n_tp)]


def scatter_sum(parts, n_tp, share):
    held = {k: parts[k] for k in range(n_tp)}
    bit = 1
    while bit < n_tp:
        sent = sorted((k for k in held if k & bit), reverse=True)
        moved = []
        for k in sent:
            moved.append(swap(held[k], "tp", bit))
        last = 2 * bit == n_tp
        sums = fold([held[k ^ bit] for k in sent], moved, share if last else 1)
        if last:
            return sums
        held = {k ^ bit: total for k, total in zip(sent, sums)}
        bit *= 2
    return [parts[0]]


def layer(
    lane_source_signal,
    spectral_damping_part,
    spectral_angular_part,
    interval_exponent,
    entry_matrix_inphase,
    entry_matrix_quadrature,
    emission_inphase,
    emission_quadrature,
    lane_bypass_factor,
    spike_shrink_offset,
    lane_exit_matrix,
    skipline_stream,
    specialist_scaling_vector,
    selected_specialists,
    dispatcher_scores,
    specialist_valve_matrix,
    specialist_widen_matrix,
    specialist_shrink_matrix,
):
    n_tp, experts = lax.axis_size("tp"), lax.axis_size("sp")
    d_local = specialist_scaling_vector.shape[0] // n_tp
    tok_local, top = selected_specialists.shape
    capacity = 2 * tok_local * top // experts
    place = jnp.stack([lax.axis_index("sp"), lax.axis_index("tp")]).astype(jnp.int32)
    exits, own_skip = cut_blocks(place, lane_exit_matrix, skipline_stream, n_tp)
    for k in range(1, n_tp):
        exits[k] = swap(exits[k], "tp", k)

    mixed = mixer(
        place,
        lane_source_signal,
        spectral_damping_part,
        spectral_angular_part,
        interval_exponent,
        entry_matrix_inphase,
        entry_matrix_quadrature,
        emission_inphase,
        emission_quadrature,
        lane_bypass_factor,
        spike_shrink_offset,
    )
    others = [mixed]
    for k in range(1, n_tp):
        others.append(swap(mixed, "tp", k))
    pick, high, low = route(place, selected_specialists, dispatcher_scores, experts, capacity)
    gate_w, up_w, down_w = load(
        specialist_valve_matrix[0], specialist_widen_matrix[0], specialist_shrink_matrix[0]
    )
    scale = specialist_scaling_vector.reshape(n_tp, 1, d_local)

    stream, *rows = project(others, exits, own_skip, pick, experts)
    arrived = {}
    for k in range(experts):
        arrived[k] = swap(rows[k], "sp", k) if k else rows[k]
    back = {}
    for chunk in chunks_of(experts):
        pieces = gather_pieces(pack([arrived[k] for k in chunk]), n_tp)
        parts = ffn(place, pieces, scale, gate_w, up_w, down_w)
        sums = scatter_sum(parts, n_tp, len(chunk))
        for k, total in zip(chunk, sums):
            back[k] = swap(total, "sp", k) if k else total
    return combine(stream, high, low, [back[k] for k in range(experts)])


def chunks_of(experts):
    near = list(range(experts // 2))
    far = list(range(experts // 2, experts))
    return near, far[: experts // 4], far[experts // 4 :]


def solution(mesh):
    placed = (
        P("tp", "sp"),
        P("tp", None),
        P("tp", None),
        P("tp"),
        P("tp", None, None),
        P("tp", None, None),
        P("tp", None, None),
        P("tp", None, None),
        P("tp"),
        P("tp", "sp"),
        P("tp", None),
        P("sp", None),
        P(),
        P("sp", None),
        P("sp", None),
        P("sp", None, "tp"),
        P("sp", None, "tp"),
        P("sp", "tp", None),
    )
    return jax.shard_map(
        layer, mesh=mesh, in_specs=placed, out_specs=P("sp", "tp"), check_vma=False
    )
```

time: 371 us -> 157 us (0.42)
  blocking collectives: 155 us -> 13.3 us
  waiting for transfers between devices: 139 us -> 69.4 us
  starting transfers between devices: 5.77 us -> 34 us
  Pallas kernels: 0 us -> 22.4 us
  matrix products: 21 us -> 0 us
  other arithmetic: 17.3 us -> 0.07 us
  between operations: 13.5 us -> 0.22 us
    all_gather x4 -> x0, blocking collectives: 124 us -> none  [carried_in(): pieces = jax.tree.map(lambda part: lax.all_gather(part, axis), value)]
    ppermute x0 -> x38, waiting for transfers between devices: none -> 69.4 us  [swap(): return lax.ppermute(value, axis, [(i, i ^ bits) for i in range(count)])]
    reduce_scatter x1 -> x0, waiting for transfers between devices: 44.6 us -> none  [per_device(): lax.psum_scatter(down_part.astype(f32).astype(jnp.bfloat16), 'tp', scatte...]
    psum x1 -> x0, waiting for transfers between devices: 35.4 us -> none  [per_device(): lax.psum(partial_rows.astype(jnp.bfloat16), 'tp').astype(jnp.float32)]
    ppermute x0 -> x38, starting transfers between devices: none -> 34 us  [swap(): return lax.ppermute(value, axis, [(i, i ^ bits) for i in range(count)])]
    all_gather x1 -> x0, waiting for transfers between devices: 33.4 us -> none  [per_device(): piece = lax.all_gather(arrived, 'tp', axis=2, tiled=True)]
    all_to_all x1 -> x0, waiting for transfers between devices: 25.2 us -> none  [per_device(): lax.all_to_all(expert_out, 'sp', split_axis=0, concat_axis=0, tiled=True)]
    pallas_call x0 -> x19, Pallas kernels: none -> 22.4 us  [the longest x3 9.52 us: ffn(): pl.pallas_call(lambda *refs: ffn_kernel(n_tp, width, *refs), in_specs=[pl...]
  transfers between devices with their start and end apart: 4 -> 38, of which waited for: 4 -> 16; matrix products, arithmetic and copies ran while one was open for 1% -> 0% of each run, Pallas kernels for 0% -> 12%
where the time goes in v1:
time: 157 us
  waiting for transfers between devices  69.4 us (44%)
  starting transfers between devices  34 us (22%)
  Pallas kernels  22.4 us (14%)
  local copies, waits for them, and re-layouts  17.1 us (11%)
  blocking collectives  13.3 us (8%)
    ppermute x38, waiting for transfers between devices, swap(): return lax.ppermute(value, axis, [(i, i ^ bits) for i in range(count)])  69.4 us
    ppermute x38, starting transfers between devices, swap(): return lax.ppermute(value, axis, [(i, i ^ bits) for i in range(count)])  34 us
    unnamed x42, local copies, waits for them, and re-layouts  17.1 us
    all_to_all x1, blocking collectives, mixer(): pieces = lax.all_to_all(summary, 'sp', 0, 0, tiled=True)  13.3 us
    pallas_call x3, Pallas kernels, ffn(): pl.pallas_call(lambda *refs: ffn_kernel(n_tp, width, *refs), in_specs=[pl...  9.52 us
    pallas_call x1, Pallas kernels, mixer(): pl.pallas_call(staged(scan_kernel, 0, len(args)), in_specs=hbm(len(args))...  4.43 us
  transfers between devices with their start and end apart: 38, of which 16 were waited for; matrix products, arithmetic and copies ran while one was open for 0% of the time, Pallas kernels for 12%

profile of v1, /device:TPU:0, one launch (start us, length us, event | category | flops | bytes accessed | tf_op | source)
XLA Modules:
  0.0 156.5 jit_solution(6954088224401051985)
XLA Ops:
  0.1 1.6 %copy-done.3 = bf16[256,4096]{1,0:T(8,128)(2,1)S(1)} copy-done((bf16[256,4096]{1,0:T(8,128)(2,1)S(1)}, bf16[256,4096]{1,0:T(8,128)(2,1)}, u32[]{:S(2)}) %copy-start.3) | copy-done | bytes 2097176
  1.7 1.2 copy-done.4
  2.9 1.7 %cut_blocks.1 = (bf16[256,1024]{1,0:T(8,128)(2,1)S(1)}, bf16[256,1024]{1,0:T(8,128)(2,1)}, bf16[256,1024]{1,0:T(8,128)(2,1)}, bf16[256,1024]{1,0:T(8,128)(2,1)S(1)}, bf16[128,1024]{1,0:T(8,128)(2,1)S(1)}) custom-call(s32[2]{0:T(128)S(1)} %pad_add_fusion.refs_0_, bf16[256,4096]{1,0:T(8,128)(2,1)S(1)} %copy-done.3, bf16[128,4096]{1,0:T(8,128)(2,1)S(1)} %copy-done.4), custom_call_target="tpu_custom_call" | custom-call | tf_op jit(solution)/shard_map/cut_blocks/pallas_call | solution.py:297
  5.1 2.6 %collective-permute-start.4 = (bf16[256,1024]{1,0:T(8,128)(2,1)}, bf16[256,1024]{1,0:T(8,128)(2,1)S(1)}, u32[]{:S(2)}, u32[]{:S(2)}) collective-permute-start(bf16[256,1024]{1,0:T(8,128)(2,1)} %get-tuple-element.61), channel_id=1, source_target_pairs={{0,2},{1,3},{2,0},{3,1},{4,6},{5,7},{6,4},{7,5},{8,10},{9,11},{10,... | collective-permute-start | bytes 1572872 | tf_op jit(solution)/shard_map/ppermute | solution.py:15
  7.8 0.9 copy-done.5
  8.7 0.9 copy-done.7
  9.6 0.9 copy-done.10
  10.5 0.9 copy-done.11
  15.6 4.4 %mixer_scan.1 = (f32[8,8,512]{2,1,0:T(8,128)S(1)}, f32[128,256]{1,0:T(8,128)S(1)}, f32[14,1024]{1,0:T(8,128)S(1)}, f32[128,16]{1,0:T(8,128)S(1)}) custom-call(bf16[256,128]{1,0:T(8,128)(2,1)S(1)} %copy-done.12, f32[16,64]{1,0:T(8,128)S(1)} %copy-done.13, f32[16,64]{1,0:T(8,128)S(1)} %copy-done.14, f32[1,16]{1,0:T(1,128)S(1)} %bitcast.19, ...), custom_call_target="tpu_custom_call" | custom-call | tf_op jit(solution)/shard_map/mixer_scan/pallas_call | solution.py:250
  20.1 13.3 %all_to_all.5.refs_1_ = f32[8,8,512]{2,1,0:T(8,128)S(1)} all-to-all(f32[8,8,512]{2,1,0:T(8,128)S(1)} %get-tuple-element.55), channel_id=1, replica_groups=mesh['sp'=8,'tp'=4] {'sp'}, dimensions={0} | all-to-all | bytes 262144 | tf_op jit(solution)/shard_map/all_to_all | solution.py:264
  33.4 0.9 copy-done.6
  35.2 1.8 %mixer_readout.1.refs_0_ = bf16[128,256]{1,0:T(8,128)(2,1)S(1)} custom-call(s32[2]{0:T(128)S(1)} %pad_add_fusion.refs_0_, f32[8,8,512]{2,1,0:T(8,128)S(1)} %all_to_all.5.refs_1_, f32[128,256]{1,0:T(8,128)S(1)} %get-tuple-element.56.refs_2_, f32[14,1024]{1,0:T(8,128)S(1)} %get-tuple-element.57.refs_3_, f32[128,16]{1,0:T(8,128)S(1)} %get-tuple-element.58.refs_4_, ...), custom_call_target="tpu_custom_call" | custom-call | tf_op jit(solution)/shard_map/mixer_readout/pallas_call | solution.py:266
  37.1 1.6 %collective-permute-start.1 = (bf16[128,256]{1,0:T(8,128)(2,1)S(1)}, bf16[128,256]{1,0:T(8,128)(2,1)S(1)}, u32[]{:S(2)}, u32[]{:S(2)}) collective-permute-start(bf16[128,256]{1,0:T(8,128)(2,1)S(1)} %mixer_readout.1.refs_0_), channel_id=1, source_target_pairs={{0,2},{1,3},{2,0},{3,1},{4,6},{5,7},{6,4},{7,5},{8,10},{9,11},{10,... | collective-permute-start | bytes 196616 | tf_op jit(solution)/shard_map/ppermute | solution.py:15
  38.6 0.9 collective-permute-start.2
  39.8 1.1 route.1
  41.6 1.1 collective-permute-done.2.refs_3_
  44.0 0.9 collective-permute-start.7
  44.9 2.2 %collective-permute-start.8 = (bf16[64,1024]{1,0:T(8,128)(2,1)S(1)}, bf16[64,1024]{1,0:T(8,128)(2,1)S(1)}, u32[]{:S(2)}, u32[]{:S(2)}) collective-permute-start(bf16[64,1024]{1,0:T(8,128)(2,1)S(1)} %get-tuple-element.71), channel_id=1, source_target_pairs={{0,12},{4,8},{8,4},{12,0},{16,28},{20,24},{24,20},{28,16},{1,13},{... | collective-permute-start | bytes 393224 | tf_op jit(solution)/shard_map/ppermute | solution.py:15
  47.1 2.1 %collective-permute-done.6.refs_1_ = bf16[64,1024]{1,0:T(8,128)(2,1)S(1)} collective-permute-done((bf16[64,1024]{1,0:T(8,128)(2,1)S(1)}, bf16[64,1024]{1,0:T(8,128)(2,1)S(1)}, u32[]{:S(2)}, u32[]{:S(2)}) %collective-permute-start.6) | collective-permute-done | bytes 131104 | tf_op jit(solution)/shard_map/ppermute | solution.py:15
  49.2 1.2 collective-permute-done.7.refs_2_
  50.4 2.8 %collective-permute-done.8.refs_3_ = bf16[64,1024]{1,0:T(8,128)(2,1)S(1)} collective-permute-done((bf16[64,1024]{1,0:T(8,128)(2,1)S(1)}, bf16[64,1024]{1,0:T(8,128)(2,1)S(1)}, u32[]{:S(2)}, u32[]{:S(2)}) %collective-permute-start.8) | collective-permute-done | bytes 131104 | tf_op jit(solution)/shard_map/ppermute | solution.py:15
  53.2 1.5 collective-permute-start.10
  54.8 11.4 %collective-permute-done.10.refs_3_ = bf16[256,1024]{1,0:T(8,128)(2,1)S(1)} collective-permute-done((bf16[256,1024]{1,0:T(8,128)(2,1)S(1)}, bf16[256,1024]{1,0:T(8,128)(2,1)S(1)}, u32[]{:S(2)}, u32[]{:S(2)}) %collective-permute-start.10) | collective-permute-done | bytes 524320 | tf_op jit(solution)/shard_map/ppermute | solution.py:15
  66.7 2.2 %collective-permute-start.19 = (bf16[64,1024]{1,0:T(8,128)(2,1)S(1)}, bf16[64,1024]{1,0:T(8,128)(2,1)S(1)}, u32[]{:S(2)}, u32[]{:S(2)}) collective-permute-start(bf16[64,1024]{1,0:T(8,128)(2,1)S(1)} %get-tuple-element.86), channel_id=1, source_target_pairs={{0,20},{4,16},{8,28},{12,24},{16,4},{20,0},{24,12},{28,8},{1,21},{... | collective-permute-start | bytes 393224 | tf_op jit(solution)/shard_map/ppermute | solution.py:15
  68.9 9.7 %collective-permute-done.18.refs_0_ = bf16[64,1024]{1,0:T(8,128)(2,1)S(1)} collective-permute-done((bf16[64,1024]{1,0:T(8,128)(2,1)S(1)}, bf16[64,1024]{1,0:T(8,128)(2,1)S(1)}, u32[]{:S(2)}, u32[]{:S(2)}) %collective-permute-start.18) | collective-permute-done | bytes 131104 | tf_op jit(solution)/shard_map/ppermute | solution.py:15
  78.6 2.6 %collective-permute-done.19.refs_1_ = bf16[64,1024]{1,0:T(8,128)(2,1)S(1)} collective-permute-done((bf16[64,1024]{1,0:T(8,128)(2,1)S(1)}, bf16[64,1024]{1,0:T(8,128)(2,1)S(1)}, u32[]{:S(2)}, u32[]{:S(2)}) %collective-permute-start.19) | collective-permute-done | bytes 131104 | tf_op jit(solution)/shard_map/ppermute | solution.py:15
  81.2 1.5 collective-permute-start.21
  82.7 1.6 %collective-permute-start.28 = (bf16[64,1024]{1,0:T(8,128)(2,1)S(1)}, bf16[64,1024]{1,0:T(8,128)(2,1)S(1)}, u32[]{:S(2)}, u32[]{:S(2)}) collective-permute-start(bf16[64,1024]{1,0:T(8,128)(2,1)S(1)} %get-tuple-element.95), channel_id=1, source_target_pairs={{0,24},{4,28},{8,16},{12,20},{16,8},{20,12},{24,0},{28,4},{1,25},{... | collective-permute-start | bytes 393224 | tf_op jit(solution)/shard_map/ppermute | solution.py:15
  84.3 3.3 %collective-permute-start.29 = (bf16[64,1024]{1,0:T(8,128)(2,1)S(1)}, bf16[64,1024]{1,0:T(8,128)(2,1)S(1)}, u32[]{:S(2)}, u32[]{:S(2)}) collective-permute-start(bf16[64,1024]{1,0:T(8,128)(2,1)S(1)} %get-tuple-element.96), channel_id=1, source_target_pairs={{0,28},{4,24},{8,20},{12,16},{16,12},{20,8},{24,4},{28,0},{1,29},{... | collective-permute-start | bytes 393224 | tf_op jit(solution)/shard_map/ppermute | solution.py:15
  87.6 2.2 %copy-done.1 = bf16[1,4096,512]{2,1,0:T(8,128)(2,1)S(1)} copy-done((bf16[1,4096,512]{2,1,0:T(8,128)(2,1)S(1)}, bf16[1,4096,512]{2,1,0:T(8,128)(2,1)}, u32[]{:S(2)}) %copy-start.1) | copy-done | bytes 4194328
  89.8 2.2 %copy-done.2 = bf16[1,512,4096]{2,1,0:T(8,128)(2,1)S(1)} copy-done((bf16[1,512,4096]{2,1,0:T(8,128)(2,1)S(1)}, bf16[1,512,4096]{2,1,0:T(8,128)(2,1)}, u32[]{:S(2)}) %copy-start.2) | copy-done | bytes 4194328
  92.0 1.0 load.1
  94.4 4.3 %expert_ffn.3 = (bf16[256,1024]{1,0:T(8,128)(2,1)S(1)}, bf16[256,1024]{1,0:T(8,128)(2,1)S(1)}, bf16[256,1024]{1,0:T(8,128)(2,1)S(1)}, bf16[256,1024]{1,0:T(8,128)(2,1)S(1)}) custom-call(s32[2]{0:T(128)S(1)} %pad_add_fusion.refs_0_, bf16[256,1024]{1,0:T(8,128)(2,1)S(1)} %pack.3.refs_1_, bf16[256,1024]{1,0:T(8,128)(2,1)S(1)} %collective-permute-done.9.refs_2_, ...), custom_call_target="tpu_custom_call" | custom-call | flops 3221225472 | bytes 16777216 | tf_op jit(solution)/shard_map/expert_ffn/pallas_call | solution.py:492
  99.8 2.2 %collective-permute-done.31.refs_3_ = bf16[128,1024]{1,0:T(8,128)(2,1)S(1)} collective-permute-done((bf16[128,1024]{1,0:T(8,128)(2,1)S(1)}, bf16[128,1024]{1,0:T(8,128)(2,1)S(1)}, u32[]{:S(2)}, u32[]{:S(2)}) %collective-permute-start.31) | collective-permute-done | bytes 262176 | tf_op jit(solution)/shard_map/ppermute | solution.py:15
  101.9 2.6 %expert_ffn.4 = (bf16[128,1024]{1,0:T(8,128)(2,1)S(1)}, bf16[128,1024]{1,0:T(8,128)(2,1)S(1)}, bf16[128,1024]{1,0:T(8,128)(2,1)S(1)}, bf16[128,1024]{1,0:T(8,128)(2,1)S(1)}) custom-call(s32[2]{0:T(128)S(1)} %pad_add_fusion.refs_0_, bf16[128,1024]{1,0:T(8,128)(2,1)S(1)} %pack.4.refs_1_, bf16[128,1024]{1,0:T(8,128)(2,1)S(1)} %collective-permute-done.20.refs_2_, ...), custom_call_target="tpu_custom_call" | custom-call | flops 1610612736 | bytes 14680064 | tf_op jit(solution)/shard_map/expert_ffn/pallas_call | solution.py:492
  105.2 2.6 %expert_ffn.5 = (bf16[128,1024]{1,0:T(8,128)(2,1)S(1)}, bf16[128,1024]{1,0:T(8,128)(2,1)S(1)}, bf16[128,1024]{1,0:T(8,128)(2,1)S(1)}, bf16[128,1024]{1,0:T(8,128)(2,1)S(1)}) custom-call(s32[2]{0:T(128)S(1)} %pad_add_fusion.refs_0_, bf16[128,1024]{1,0:T(8,128)(2,1)S(1)} %pack.5.refs_1_, bf16[128,1024]{1,0:T(8,128)(2,1)S(1)} %collective-permute-done.30.refs_2_, ...), custom_call_target="tpu_custom_call" | custom-call | flops 1610612736 | bytes 14680064 | tf_op jit(solution)/shard_map/expert_ffn/pallas_call | solution.py:492
  109.5 1.5 collective-permute-start.25
  111.8 17.4 %collective-permute-done.25.refs_1_ = bf16[128,1024]{1,0:T(8,128)(2,1)S(1)} collective-permute-done((bf16[128,1024]{1,0:T(8,128)(2,1)S(1)}, bf16[128,1024]{1,0:T(8,128)(2,1)S(1)}, u32[]{:S(2)}, u32[]{:S(2)}) %collective-permute-start.25) | collective-permute-done | bytes 262176 | tf_op jit(solution)/shard_map/ppermute | solution.py:15
  129.2 1.4 collective-permute-start.26
  130.6 1.4 collective-permute-start.27
  132.0 2.2 %collective-permute-done.35.refs_1_ = bf16[128,1024]{1,0:T(8,128)(2,1)S(1)} collective-permute-done((bf16[128,1024]{1,0:T(8,128)(2,1)S(1)}, bf16[128,1024]{1,0:T(8,128)(2,1)S(1)}, u32[]{:S(2)}, u32[]{:S(2)}) %collective-permute-start.35) | collective-permute-done | bytes 262176 | tf_op jit(solution)/shard_map/ppermute | solution.py:15
  135.0 3.1 %collective-permute-start.37 = (bf16[64,1024]{1,0:T(8,128)(2,1)S(1)}, bf16[64,1024]{1,0:T(8,128)(2,1)S(1)}, u32[]{:S(2)}, u32[]{:S(2)}) collective-permute-start(bf16[64,1024]{1,0:T(8,128)(2,1)S(1)} %get-tuple-element.104), channel_id=1, source_target_pairs={{0,28},{4,24},{8,20},{12,16},{16,12},{20,8},{24,4},{28,0},{1,29},{... | collective-permute-start | bytes 393224 | tf_op jit(solution)/shard_map/ppermute | solution.py:15
  138.1 1.7 %collective-permute-start.15 = (bf16[64,1024]{1,0:T(8,128)(2,1)S(1)}, bf16[64,1024]{1,0:T(8,128)(2,1)S(1)}, u32[]{:S(2)}, u32[]{:S(2)}) collective-permute-start(bf16[64,1024]{1,0:T(8,128)(2,1)S(1)} %get-tuple-element.82), channel_id=1, source_target_pairs={{0,4},{4,0},{8,12},{12,8},{16,20},{20,16},{24,28},{28,24},{1,5},{5... | collective-permute-start | bytes 393224 | tf_op jit(solution)/shard_map/ppermute | solution.py:15
  139.9 6.3 %collective-permute-done.26.refs_4_ = bf16[64,1024]{1,0:T(8,128)(2,1)S(1)} collective-permute-done((bf16[64,1024]{1,0:T(8,128)(2,1)S(1)}, bf16[64,1024]{1,0:T(8,128)(2,1)S(1)}, u32[]{:S(2)}, u32[]{:S(2)}) %collective-permute-start.26) | collective-permute-done | bytes 131104 | tf_op jit(solution)/shard_map/ppermute | solution.py:15
  146.2 3.3 %collective-permute-done.27.refs_5_ = bf16[64,1024]{1,0:T(8,128)(2,1)S(1)} collective-permute-done((bf16[64,1024]{1,0:T(8,128)(2,1)S(1)}, bf16[64,1024]{1,0:T(8,128)(2,1)S(1)}, u32[]{:S(2)}, u32[]{:S(2)}) %collective-permute-start.27) | collective-permute-done | bytes 131104 | tf_op jit(solution)/shard_map/ppermute | solution.py:15
  149.5 2.0 %collective-permute-done.16.refs_2_ = bf16[64,1024]{1,0:T(8,128)(2,1)S(1)} collective-permute-done((bf16[64,1024]{1,0:T(8,128)(2,1)S(1)}, bf16[64,1024]{1,0:T(8,128)(2,1)S(1)}, u32[]{:S(2)}, u32[]{:S(2)}) %collective-permute-start.16) | collective-permute-done | bytes 131104 | tf_op jit(solution)/shard_map/ppermute | solution.py:15
  151.5 3.9 %collective-permute-done.17.refs_3_ = bf16[64,1024]{1,0:T(8,128)(2,1)S(1)} collective-permute-done((bf16[64,1024]{1,0:T(8,128)(2,1)S(1)}, bf16[64,1024]{1,0:T(8,128)(2,1)S(1)}, u32[]{:S(2)}, u32[]{:S(2)}) %collective-permute-start.17) | collective-permute-done | bytes 131104 | tf_op jit(solution)/shard_map/ppermute | solution.py:15
  155.4 1.2 combine.1
  (91 shorter events, 15.0 us)
Async XLA Ops:
  0.0 39.6 %copy-start.18 = (s32[128,2]{0,1:T(2,128)S(1)}, s32[128,2]{0,1:T(2,128)}, u32[]{:S(2)}) copy-start(s32[128,2]{0,1:T(2,128)} %param.31) | copy-start | bytes 3076
  0.0 39.7 %copy-start.19 = (f32[128,2]{0,1:T(2,128)S(1)}, f32[128,2]{0,1:T(2,128)}, u32[]{:S(2)}) copy-start(f32[128,2]{0,1:T(2,128)} %param.32) | copy-start | bytes 3076
  0.1 1.6 %copy-start.3 = (bf16[256,4096]{1,0:T(8,128)(2,1)S(1)}, bf16[256,4096]{1,0:T(8,128)(2,1)}, u32[]{:S(2)}) copy-start(bf16[256,4096]{1,0:T(8,128)(2,1)} %refs_1_.4) | copy-start | bytes 6291460
  1.7 1.2 copy-start.4
  4.6 38.1 %collective-permute-start.3 = (bf16[256,1024]{1,0:T(8,128)(2,1)}, bf16[256,1024]{1,0:T(8,128)(2,1)S(1)}, u32[]{:S(2)}, u32[]{:S(2)}) collective-permute-start(bf16[256,1024]{1,0:T(8,128)(2,1)} %get-tuple-element.60), channel_id=1, source_target_pairs={{0,1},{1,0},{2,3},{3,2},{4,5},{5,4},{6,7},{7,6},{8,9},{9,8},{10,11... | collective-permute-start | bytes 1572872 | tf_op jit(solution)/shard_map/ppermute | solution.py:15
  5.1 37.6 %collective-permute-start.4 = (bf16[256,1024]{1,0:T(8,128)(2,1)}, bf16[256,1024]{1,0:T(8,128)(2,1)S(1)}, u32[]{:S(2)}, u32[]{:S(2)}) collective-permute-start(bf16[256,1024]{1,0:T(8,128)(2,1)} %get-tuple-element.61), channel_id=1, source_target_pairs={{0,2},{1,3},{2,0},{3,1},{4,6},{5,7},{6,4},{7,5},{8,10},{9,11},{10,... | collective-permute-start | bytes 1572872 | tf_op jit(solution)/shard_map/ppermute | solution.py:15
  7.7 35.0 %collective-permute-start.5 = (bf16[256,1024]{1,0:T(8,128)(2,1)S(1)}, bf16[256,1024]{1,0:T(8,128)(2,1)S(1)}, u32[]{:S(2)}, u32[]{:S(2)}) collective-permute-start(bf16[256,1024]{1,0:T(8,128)(2,1)S(1)} %get-tuple-element.62), channel_id=1, source_target_pairs={{0,3},{1,2},{2,1},{3,0},{4,7},{5,6},{6,5},{7,4},{8,11},{9,10},{10,... | collective-permute-start | bytes 1572872 | tf_op jit(solution)/shard_map/ppermute | solution.py:15
  10.5 0.9 copy-start.11
  33.4 0.9 copy-start.6
  37.0 1.7 %collective-permute-start = (bf16[128,256]{1,0:T(8,128)(2,1)S(1)}, bf16[128,256]{1,0:T(8,128)(2,1)S(1)}, u32[]{:S(2)}, u32[]{:S(2)}) collective-permute-start(bf16[128,256]{1,0:T(8,128)(2,1)S(1)} %mixer_readout.1.refs_0_), channel_id=1, source_target_pairs={{0,1},{1,0},{2,3},{3,2},{4,5},{5,4},{6,7},{7,6},{8,9},{9,8},{10,11... | collective-permute-start | bytes 196616 | tf_op jit(solution)/shard_map/ppermute | solution.py:15
  37.1 4.5 %collective-permute-start.1 = (bf16[128,256]{1,0:T(8,128)(2,1)S(1)}, bf16[128,256]{1,0:T(8,128)(2,1)S(1)}, u32[]{:S(2)}, u32[]{:S(2)}) collective-permute-start(bf16[128,256]{1,0:T(8,128)(2,1)S(1)} %mixer_readout.1.refs_0_), channel_id=1, source_target_pairs={{0,2},{1,3},{2,0},{3,1},{4,6},{5,7},{6,4},{7,5},{8,10},{9,11},{10,... | collective-permute-start | bytes 196616 | tf_op jit(solution)/shard_map/ppermute | solution.py:15
  38.6 4.1 %collective-permute-start.2 = (bf16[128,256]{1,0:T(8,128)(2,1)S(1)}, bf16[128,256]{1,0:T(8,128)(2,1)S(1)}, u32[]{:S(2)}, u32[]{:S(2)}) collective-permute-start(bf16[128,256]{1,0:T(8,128)(2,1)S(1)} %mixer_readout.1.refs_0_), channel_id=1, source_target_pairs={{0,3},{1,2},{2,1},{3,0},{4,7},{5,6},{6,5},{7,4},{8,11},{9,10},{10,... | collective-permute-start | bytes 196616 | tf_op jit(solution)/shard_map/ppermute | solution.py:15
  39.8 47.8 %copy-start = (bf16[1,4096,512]{2,1,0:T(8,128)(2,1)S(1)}, bf16[1,4096,512]{2,1,0:T(8,128)(2,1)}, u32[]{:S(2)}) copy-start(bf16[1,4096,512]{2,1,0:T(8,128)(2,1)} %param.33) | copy-start | bytes 12582916
  43.6 5.6 %collective-permute-start.6 = (bf16[64,1024]{1,0:T(8,128)(2,1)S(1)}, bf16[64,1024]{1,0:T(8,128)(2,1)S(1)}, u32[]{:S(2)}, u32[]{:S(2)}) collective-permute-start(bf16[64,1024]{1,0:T(8,128)(2,1)S(1)} %get-tuple-element.69), channel_id=1, source_target_pairs={{0,4},{4,0},{8,12},{12,8},{16,20},{20,16},{24,28},{28,24},{1,5},{5... | collective-permute-start | bytes 393224 | tf_op jit(solution)/shard_map/ppermute | solution.py:15
  44.0 6.4 %collective-permute-start.7 = (bf16[64,1024]{1,0:T(8,128)(2,1)S(1)}, bf16[64,1024]{1,0:T(8,128)(2,1)S(1)}, u32[]{:S(2)}, u32[]{:S(2)}) collective-permute-start(bf16[64,1024]{1,0:T(8,128)(2,1)S(1)} %get-tuple-element.70), channel_id=1, source_target_pairs={{0,8},{4,12},{8,0},{12,4},{16,24},{20,28},{24,16},{28,20},{1,9},{5... | collective-permute-start | bytes 393224 | tf_op jit(solution)/shard_map/ppermute | solution.py:15
  44.9 8.3 %collective-permute-start.8 = (bf16[64,1024]{1,0:T(8,128)(2,1)S(1)}, bf16[64,1024]{1,0:T(8,128)(2,1)S(1)}, u32[]{:S(2)}, u32[]{:S(2)}) collective-permute-start(bf16[64,1024]{1,0:T(8,128)(2,1)S(1)} %get-tuple-element.71), channel_id=1, source_target_pairs={{0,12},{4,8},{8,4},{12,0},{16,28},{20,24},{24,20},{28,16},{1,13},{... | collective-permute-start | bytes 393224 | tf_op jit(solution)/shard_map/ppermute | solution.py:15
  53.2 12.9 %collective-permute-start.10 = (bf16[256,1024]{1,0:T(8,128)(2,1)S(1)}, bf16[256,1024]{1,0:T(8,128)(2,1)S(1)}, u32[]{:S(2)}, u32[]{:S(2)}) collective-permute-start(bf16[256,1024]{1,0:T(8,128)(2,1)S(1)} %pack.3.refs_1_), channel_id=1, source_target_pairs={{0,2},{1,3},{2,0},{3,1},{4,6},{5,7},{6,4},{7,5},{8,10},{9,11},{10,... | collective-permute-start | bytes 1572872 | tf_op jit(solution)/shard_map/ppermute | solution.py:15
  54.8 39.6 %collective-permute-start.9 = (bf16[256,1024]{1,0:T(8,128)(2,1)S(1)}, bf16[256,1024]{1,0:T(8,128)(2,1)S(1)}, u32[]{:S(2)}, u32[]{:S(2)}) collective-permute-start(bf16[256,1024]{1,0:T(8,128)(2,1)S(1)} %pack.3.refs_1_), channel_id=1, source_target_pairs={{0,1},{1,0},{2,3},{3,2},{4,5},{5,4},{6,7},{7,6},{8,9},{9,8},{10,11... | collective-permute-start | bytes 1572872 | tf_op jit(solution)/shard_map/ppermute | solution.py:15
  66.2 28.2 %collective-permute-start.11 = (bf16[256,1024]{1,0:T(8,128)(2,1)S(1)}, bf16[256,1024]{1,0:T(8,128)(2,1)S(1)}, u32[]{:S(2)}, u32[]{:S(2)}) collective-permute-start(bf16[256,1024]{1,0:T(8,128)(2,1)S(1)} %collective-permute-done.10.refs_3_), channel_id=1, source_target_pairs={{0,1},{1,0},{2,3},{3,2},{4,5},{5,4},{6,7},{7,6},{8,9},{9,8},{10,11... | collective-permute-start | bytes 1572872 | tf_op jit(solution)/shard_map/ppermute | solution.py:15
  66.2 12.4 %collective-permute-start.18 = (bf16[64,1024]{1,0:T(8,128)(2,1)S(1)}, bf16[64,1024]{1,0:T(8,128)(2,1)S(1)}, u32[]{:S(2)}, u32[]{:S(2)}) collective-permute-start(bf16[64,1024]{1,0:T(8,128)(2,1)S(1)} %get-tuple-element.85), channel_id=1, source_target_pairs={{0,16},{4,20},{8,24},{12,28},{16,0},{20,4},{24,8},{28,12},{1,17},{... | collective-permute-start | bytes 393224 | tf_op jit(solution)/shard_map/ppermute | solution.py:15
  66.7 14.5 %collective-permute-start.19 = (bf16[64,1024]{1,0:T(8,128)(2,1)S(1)}, bf16[64,1024]{1,0:T(8,128)(2,1)S(1)}, u32[]{:S(2)}, u32[]{:S(2)}) collective-permute-start(bf16[64,1024]{1,0:T(8,128)(2,1)S(1)} %get-tuple-element.86), channel_id=1, source_target_pairs={{0,20},{4,16},{8,28},{12,24},{16,4},{20,0},{24,12},{28,8},{1,21},{... | collective-permute-start | bytes 393224 | tf_op jit(solution)/shard_map/ppermute | solution.py:15
  81.2 13.2 %collective-permute-start.21 = (bf16[128,1024]{1,0:T(8,128)(2,1)S(1)}, bf16[128,1024]{1,0:T(8,128)(2,1)S(1)}, u32[]{:S(2)}, u32[]{:S(2)}) collective-permute-start(bf16[128,1024]{1,0:T(8,128)(2,1)S(1)} %pack.4.refs_1_), channel_id=1, source_target_pairs={{0,2},{1,3},{2,0},{3,1},{4,6},{5,7},{6,4},{7,5},{8,10},{9,11},{10,... | collective-permute-start | bytes 786440 | tf_op jit(solution)/shard_map/ppermute | solution.py:15
  82.7 10.3 %collective-permute-start.28 = (bf16[64,1024]{1,0:T(8,128)(2,1)S(1)}, bf16[64,1024]{1,0:T(8,128)(2,1)S(1)}, u32[]{:S(2)}, u32[]{:S(2)}) collective-permute-start(bf16[64,1024]{1,0:T(8,128)(2,1)S(1)} %get-tuple-element.95), channel_id=1, source_target_pairs={{0,24},{4,28},{8,16},{12,20},{16,8},{20,12},{24,0},{28,4},{1,25},{... | collective-permute-start | bytes 393224 | tf_op jit(solution)/shard_map/ppermute | solution.py:15
  84.3 9.4 %collective-permute-start.29 = (bf16[64,1024]{1,0:T(8,128)(2,1)S(1)}, bf16[64,1024]{1,0:T(8,128)(2,1)S(1)}, u32[]{:S(2)}, u32[]{:S(2)}) collective-permute-start(bf16[64,1024]{1,0:T(8,128)(2,1)S(1)} %get-tuple-element.96), channel_id=1, source_target_pairs={{0,28},{4,24},{8,20},{12,16},{16,12},{20,8},{24,4},{28,0},{1,29},{... | collective-permute-start | bytes 393224 | tf_op jit(solution)/shard_map/ppermute | solution.py:15
  87.6 2.2 %copy-start.1 = (bf16[1,4096,512]{2,1,0:T(8,128)(2,1)S(1)}, bf16[1,4096,512]{2,1,0:T(8,128)(2,1)}, u32[]{:S(2)}) copy-start(bf16[1,4096,512]{2,1,0:T(8,128)(2,1)} %param.34) | copy-start | bytes 12582916
  89.8 2.2 %copy-start.2 = (bf16[1,512,4096]{2,1,0:T(8,128)(2,1)S(1)}, bf16[1,512,4096]{2,1,0:T(8,128)(2,1)}, u32[]{:S(2)}) copy-start(bf16[1,512,4096]{2,1,0:T(8,128)(2,1)} %param.35) | copy-start | bytes 12582916
  92.0 2.4 %copy-start.9 = (f32[4096]{0:T(1024)S(1)}, f32[4096]{0:T(1024)}, u32[]{:S(2)}) copy-start(f32[4096]{0:T(1024)} %param.30) | copy-start | bytes 49156
  93.0 6.3 %collective-permute-start.20 = (bf16[128,1024]{1,0:T(8,128)(2,1)S(1)}, bf16[128,1024]{1,0:T(8,128)(2,1)S(1)}, u32[]{:S(2)}, u32[]{:S(2)}) collective-permute-start(bf16[128,1024]{1,0:T(8,128)(2,1)S(1)} %pack.4.refs_1_), channel_id=1, source_target_pairs={{0,1},{1,0},{2,3},{3,2},{4,5},{5,4},{6,7},{7,6},{8,9},{9,8},{10,11... | collective-permute-start | bytes 786440 | tf_op jit(solution)/shard_map/ppermute | solution.py:15
  93.7 8.2 %collective-permute-start.31 = (bf16[128,1024]{1,0:T(8,128)(2,1)S(1)}, bf16[128,1024]{1,0:T(8,128)(2,1)S(1)}, u32[]{:S(2)}, u32[]{:S(2)}) collective-permute-start(bf16[128,1024]{1,0:T(8,128)(2,1)S(1)} %pack.5.refs_1_), channel_id=1, source_target_pairs={{0,2},{1,3},{2,0},{3,1},{4,6},{5,7},{6,4},{7,5},{8,10},{9,11},{10,... | collective-permute-start | bytes 786440 | tf_op jit(solution)/shard_map/ppermute | solution.py:15
  94.4 7.5 %collective-permute-start.22 = (bf16[128,1024]{1,0:T(8,128)(2,1)S(1)}, bf16[128,1024]{1,0:T(8,128)(2,1)S(1)}, u32[]{:S(2)}, u32[]{:S(2)}) collective-permute-start(bf16[128,1024]{1,0:T(8,128)(2,1)S(1)} %collective-permute-done.21.refs_3_), channel_id=1, source_target_pairs={{0,1},{1,0},{2,3},{3,2},{4,5},{5,4},{6,7},{7,6},{8,9},{9,8},{10,11... | collective-permute-start | bytes 786440 | tf_op jit(solution)/shard_map/ppermute | solution.py:15
  98.7 9.7 %collective-permute-start.12 = (bf16[256,1024]{1,0:T(8,128)(2,1)S(1)}, bf16[256,1024]{1,0:T(8,128)(2,1)S(1)}, u32[]{:S(2)}, u32[]{:S(2)}) collective-permute-start(bf16[256,1024]{1,0:T(8,128)(2,1)S(1)} %get-tuple-element.77), channel_id=1, source_target_pairs={{0,1},{1,0},{2,3},{3,2},{4,5},{5,4},{6,7},{7,6},{8,9},{9,8},{10,11... | collective-permute-start | bytes 1572872 | tf_op jit(solution)/shard_map/ppermute | solution.py:15
  99.2 9.2 %collective-permute-start.13 = (bf16[256,1024]{1,0:T(8,128)(2,1)S(1)}, bf16[256,1024]{1,0:T(8,128)(2,1)S(1)}, u32[]{:S(2)}, u32[]{:S(2)}) collective-permute-start(bf16[256,1024]{1,0:T(8,128)(2,1)S(1)} %get-tuple-element.78), channel_id=1, source_target_pairs={{0,1},{1,0},{2,3},{3,2},{4,5},{5,4},{6,7},{7,6},{8,9},{9,8},{10,11... | collective-permute-start | bytes 1572872 | tf_op jit(solution)/shard_map/ppermute | solution.py:15
  99.3 5.8 %collective-permute-start.30 = (bf16[128,1024]{1,0:T(8,128)(2,1)S(1)}, bf16[128,1024]{1,0:T(8,128)(2,1)S(1)}, u32[]{:S(2)}, u32[]{:S(2)}) collective-permute-start(bf16[128,1024]{1,0:T(8,128)(2,1)S(1)} %pack.5.refs_1_), channel_id=1, source_target_pairs={{0,1},{1,0},{2,3},{3,2},{4,5},{5,4},{6,7},{7,6},{8,9},{9,8},{10,11... | collective-permute-start | bytes 786440 | tf_op jit(solution)/shard_map/ppermute | solution.py:15
  101.9 3.3 %collective-permute-start.32 = (bf16[128,1024]{1,0:T(8,128)(2,1)S(1)}, bf16[128,1024]{1,0:T(8,128)(2,1)S(1)}, u32[]{:S(2)}, u32[]{:S(2)}) collective-permute-start(bf16[128,1024]{1,0:T(8,128)(2,1)S(1)} %collective-permute-done.31.refs_3_), channel_id=1, source_target_pairs={{0,1},{1,0},{2,3},{3,2},{4,5},{5,4},{6,7},{7,6},{8,9},{9,8},{10,11... | collective-permute-start | bytes 786440 | tf_op jit(solution)/shard_map/ppermute | solution.py:15
  104.5 4.8 %collective-permute-start.23 = (bf16[128,1024]{1,0:T(8,128)(2,1)S(1)}, bf16[128,1024]{1,0:T(8,128)(2,1)S(1)}, u32[]{:S(2)}, u32[]{:S(2)}) collective-permute-start(bf16[128,1024]{1,0:T(8,128)(2,1)S(1)} %get-tuple-element.89), channel_id=1, source_target_pairs={{0,1},{1,0},{2,3},{3,2},{4,5},{5,4},{6,7},{7,6},{8,9},{9,8},{10,11... | collective-permute-start | bytes 786440 | tf_op jit(solution)/shard_map/ppermute | solution.py:15
  105.1 4.2 %collective-permute-start.24 = (bf16[128,1024]{1,0:T(8,128)(2,1)S(1)}, bf16[128,1024]{1,0:T(8,128)(2,1)S(1)}, u32[]{:S(2)}, u32[]{:S(2)}) collective-permute-start(bf16[128,1024]{1,0:T(8,128)(2,1)S(1)} %get-tuple-element.90), channel_id=1, source_target_pairs={{0,1},{1,0},{2,3},{3,2},{4,5},{5,4},{6,7},{7,6},{8,9},{9,8},{10,11... | collective-permute-start | bytes 786440 | tf_op jit(solution)/shard_map/ppermute | solution.py:15
  107.9 3.1 %collective-permute-start.33 = (bf16[128,1024]{1,0:T(8,128)(2,1)S(1)}, bf16[128,1024]{1,0:T(8,128)(2,1)S(1)}, u32[]{:S(2)}, u32[]{:S(2)}) collective-permute-start(bf16[128,1024]{1,0:T(8,128)(2,1)S(1)} %get-tuple-element.99), channel_id=1, source_target_pairs={{0,1},{1,0},{2,3},{3,2},{4,5},{5,4},{6,7},{7,6},{8,9},{9,8},{10,11... | collective-permute-start | bytes 786440 | tf_op jit(solution)/shard_map/ppermute | solution.py:15
  108.4 2.6 %collective-permute-start.34 = (bf16[128,1024]{1,0:T(8,128)(2,1)S(1)}, bf16[128,1024]{1,0:T(8,128)(2,1)S(1)}, u32[]{:S(2)}, u32[]{:S(2)}) collective-permute-start(bf16[128,1024]{1,0:T(8,128)(2,1)S(1)} %get-tuple-element.100), channel_id=1, source_target_pairs={{0,1},{1,0},{2,3},{3,2},{4,5},{5,4},{6,7},{7,6},{8,9},{9,8},{10,11... | collective-permute-start | bytes 786440 | tf_op jit(solution)/shard_map/ppermute | solution.py:15
  108.7 29.3 %collective-permute-start.14 = (bf16[256,1024]{1,0:T(8,128)(2,1)S(1)}, bf16[256,1024]{1,0:T(8,128)(2,1)S(1)}, u32[]{:S(2)}, u32[]{:S(2)}) collective-permute-start(bf16[256,1024]{1,0:T(8,128)(2,1)S(1)} %get-tuple-element.80), channel_id=1, source_target_pairs={{0,2},{1,3},{2,0},{3,1},{4,6},{5,7},{6,4},{7,5},{8,10},{9,11},{10,... | collective-permute-start | bytes 1572872 | tf_op jit(solution)/shard_map/ppermute | solution.py:15
  109.5 19.7 %collective-permute-start.25 = (bf16[128,1024]{1,0:T(8,128)(2,1)S(1)}, bf16[128,1024]{1,0:T(8,128)(2,1)S(1)}, u32[]{:S(2)}, u32[]{:S(2)}) collective-permute-start(bf16[128,1024]{1,0:T(8,128)(2,1)S(1)} %get-tuple-element.92), channel_id=1, source_target_pairs={{0,2},{1,3},{2,0},{3,1},{4,6},{5,7},{6,4},{7,5},{8,10},{9,11},{10,... | collective-permute-start | bytes 786440 | tf_op jit(solution)/shard_map/ppermute | solution.py:15
  111.1 23.1 %collective-permute-start.35 = (bf16[128,1024]{1,0:T(8,128)(2,1)S(1)}, bf16[128,1024]{1,0:T(8,128)(2,1)S(1)}, u32[]{:S(2)}, u32[]{:S(2)}) collective-permute-start(bf16[128,1024]{1,0:T(8,128)(2,1)S(1)} %get-tuple-element.102), channel_id=1, source_target_pairs={{0,2},{1,3},{2,0},{3,1},{4,6},{5,7},{6,4},{7,5},{8,10},{9,11},{10,... | collective-permute-start | bytes 786440 | tf_op jit(solution)/shard_map/ppermute | solution.py:15
  129.2 17.0 %collective-permute-start.26 = (bf16[64,1024]{1,0:T(8,128)(2,1)S(1)}, bf16[64,1024]{1,0:T(8,128)(2,1)S(1)}, u32[]{:S(2)}, u32[]{:S(2)}) collective-permute-start(bf16[64,1024]{1,0:T(8,128)(2,1)S(1)} %get-tuple-element.93), channel_id=1, source_target_pairs={{0,16},{4,20},{8,24},{12,28},{16,0},{20,4},{24,8},{28,12},{1,17},{... | collective-permute-start | bytes 393224 | tf_op jit(solution)/shard_map/ppermute | solution.py:15
  130.6 18.9 %collective-permute-start.27 = (bf16[64,1024]{1,0:T(8,128)(2,1)S(1)}, bf16[64,1024]{1,0:T(8,128)(2,1)S(1)}, u32[]{:S(2)}, u32[]{:S(2)}) collective-permute-start(bf16[64,1024]{1,0:T(8,128)(2,1)S(1)} %get-tuple-element.94), channel_id=1, source_target_pairs={{0,20},{4,16},{8,28},{12,24},{16,4},{20,0},{24,12},{28,8},{1,21},{... | collective-permute-start | bytes 393224 | tf_op jit(solution)/shard_map/ppermute | solution.py:15
  134.3 15.2 %collective-permute-start.36 = (bf16[64,1024]{1,0:T(8,128)(2,1)S(1)}, bf16[64,1024]{1,0:T(8,128)(2,1)S(1)}, u32[]{:S(2)}, u32[]{:S(2)}) collective-permute-start(bf16[64,1024]{1,0:T(8,128)(2,1)S(1)} %get-tuple-element.103), channel_id=1, source_target_pairs={{0,24},{4,28},{8,16},{12,20},{16,8},{20,12},{24,0},{28,4},{1,25},{... | collective-permute-start | bytes 393224 | tf_op jit(solution)/shard_map/ppermute | solution.py:15
  135.0 14.6 %collective-permute-start.37 = (bf16[64,1024]{1,0:T(8,128)(2,1)S(1)}, bf16[64,1024]{1,0:T(8,128)(2,1)S(1)}, u32[]{:S(2)}, u32[]{:S(2)}) collective-permute-start(bf16[64,1024]{1,0:T(8,128)(2,1)S(1)} %get-tuple-element.104), channel_id=1, source_target_pairs={{0,28},{4,24},{8,20},{12,16},{16,12},{20,8},{24,4},{28,0},{1,29},{... | collective-permute-start | bytes 393224 | tf_op jit(solution)/shard_map/ppermute | solution.py:15
  138.1 11.4 %collective-permute-start.15 = (bf16[64,1024]{1,0:T(8,128)(2,1)S(1)}, bf16[64,1024]{1,0:T(8,128)(2,1)S(1)}, u32[]{:S(2)}, u32[]{:S(2)}) collective-permute-start(bf16[64,1024]{1,0:T(8,128)(2,1)S(1)} %get-tuple-element.82), channel_id=1, source_target_pairs={{0,4},{4,0},{8,12},{12,8},{16,20},{20,16},{24,28},{28,24},{1,5},{5... | collective-permute-start | bytes 393224 | tf_op jit(solution)/shard_map/ppermute | solution.py:15
  146.2 5.3 %collective-permute-start.16 = (bf16[64,1024]{1,0:T(8,128)(2,1)S(1)}, bf16[64,1024]{1,0:T(8,128)(2,1)S(1)}, u32[]{:S(2)}, u32[]{:S(2)}) collective-permute-start(bf16[64,1024]{1,0:T(8,128)(2,1)S(1)} %get-tuple-element.83), channel_id=1, source_target_pairs={{0,8},{4,12},{8,0},{12,4},{16,24},{20,28},{24,16},{28,20},{1,9},{5... | collective-permute-start | bytes 393224 | tf_op jit(solution)/shard_map/ppermute | solution.py:15
  149.5 5.9 %collective-permute-start.17 = (bf16[64,1024]{1,0:T(8,128)(2,1)S(1)}, bf16[64,1024]{1,0:T(8,128)(2,1)S(1)}, u32[]{:S(2)}, u32[]{:S(2)}) collective-permute-start(bf16[64,1024]{1,0:T(8,128)(2,1)S(1)} %get-tuple-element.84), channel_id=1, source_target_pairs={{0,12},{4,8},{8,4},{12,0},{16,28},{20,24},{24,20},{28,16},{1,13},{... | collective-permute-start | bytes 393224 | tf_op jit(solution)/shard_map/ppermute | solution.py:15
  (10 other events, 7.9 us)

commit v2 on v1

--- a/solution.py
+++ b/solution.py
@@ -215,6 +215,10 @@
     return [pl.BlockSpec(memory_space=pltpu.HBM)] * count
 
 
+def in_hbm(args):
+    return [pltpu.with_memory_space_constraint(arg, pltpu.HBM) for arg in args]
+
+
 def staged(kernel, first, count):
     def run(*refs):
         sources, buffers, sems = refs[first : first + count], refs[-count - 1 : -1], refs[-1]
@@ -237,81 +241,142 @@
     ]
 
 
-def mixer(place, signal, damp, turn, pace, ent_re, ent_im, emit_re, emit_im, bypass, shrink):
+def mixer_args(signal, damp, turn, pace, ent_re, ent_im, emit_re, emit_im, bypass, shrink):
+    return (
+        signal, damp, turn, pace.reshape(1, -1), ent_re.transpose(0, 2, 1),
+        ent_im.transpose(0, 2, 1), shrink, bypass.reshape(1, -1), emit_re, emit_im,
+    )
+
+
+def first_kernel(*refs):
+    sources, outs, buffers, sems = refs[:10], refs[10:16], refs[16:24], refs[24]
+    for copy in run_copies([*zip(sources[:8], buffers), *zip(sources[8:], outs[4:])], sems):
+        copy.wait()
+    scan_kernel(*buffers[:7], *outs[4:6], buffers[7], *outs[:4])
+
+
+def mixer(place, args):
+    signal, damp, emit = args[0], args[1], args[8]
     groups, states = damp.shape
     channels, length = signal.shape
     total = groups * states
     count = lax.axis_size("sp")
     bits = (length - 1).bit_length()
-    args = (
-        signal, damp, turn, pace.reshape(1, groups), ent_re.transpose(0, 2, 1),
-        ent_im.transpose(0, 2, 1), shrink, emit_re, emit_im, bypass.reshape(1, channels),
-    )
-    summary, local, powers, gone = pl.pallas_call(
-        staged(scan_kernel, 0, len(args)),
-        in_specs=hbm(len(args)),
-        out_specs=vmem(4),
+    summary, local, powers, gone, emit_re, emit_im = pl.pallas_call(
+        first_kernel,
+        in_specs=hbm(10),
+        out_specs=vmem(6),
         out_shape=[
             jax.ShapeDtypeStruct((count, 8, total // 2), F32),
             jax.ShapeDtypeStruct((length, channels), F32),
             jax.ShapeDtypeStruct((2 * bits, total), F32),
             jax.ShapeDtypeStruct((length, groups), F32),
+            jax.ShapeDtypeStruct(emit.shape, F32),
+            jax.ShapeDtypeStruct(emit.shape, F32),
         ],
-        scratch_shapes=stage(args),
+        scratch_shapes=[pltpu.VMEM(arg.shape, arg.dtype) for arg in args[:8]]
+        + [pltpu.SemaphoreType.DMA((10,))],
         compiler_params=pltpu.CompilerParams(vmem_limit_bytes=16 * 2**20),
         name="mixer_scan",
-    )(*args)
+    )(*in_hbm(args))
     pieces = lax.all_to_all(summary, "sp", 0, 0, tiled=True)
-    args = (emit_re, emit_im)
     return pl.pallas_call(
-        staged(readout_kernel, 5, len(args)),
-        in_specs=[pl.BlockSpec(memory_space=pltpu.SMEM)] + vmem(4) + hbm(len(args)),
+        readout_kernel,
+        in_specs=[pl.BlockSpec(memory_space=pltpu.SMEM)] + vmem(6),
         out_specs=vmem(1)[0],
         out_shape=jax.ShapeDtypeStruct((length, channels), BF16),
-        scratch_shapes=stage(args),
         compiler_params=pltpu.CompilerParams(vmem_limit_bytes=16 * 2**20),
         name="mixer_readout",
-    )(place, pieces, local, powers, gone, *args)
-
-
-def cut_kernel(n_tp, place_ref, exit_ref, skip_ref, *refs):
-    outs, sems = refs[: n_tp + 1], refs[n_tp + 1]
-    me = place_ref[1]
-    wide = outs[0].shape[1]
-    copies = []
-    for k in range(n_tp):
-        source = exit_ref.at[:, pl.ds(pl.multiple_of((me ^ k) * wide, wide), wide)]
-        copies.append(pltpu.make_async_copy(source, outs[k], sems.at[k]))
-    source = skip_ref.at[:, pl.ds(pl.multiple_of(me * wide, wide), wide)]
-    copies.append(pltpu.make_async_copy(source, outs[n_tp], sems.at[n_tp]))
+    )(place, pieces, local, powers, gone, emit_re, emit_im)
+
+
+def block_of(ref, place_ref, k, wide):
+    return ref.at[:, pl.ds(pl.multiple_of((place_ref[1] ^ k) * wide, wide), wide)]
+
+
+def run_copies(pairs, sems):
+    copies = [
+        pltpu.make_async_copy(source, target, sems.at[i])
+        for i, (source, target) in enumerate(pairs)
+    ]
     for copy in copies:
         copy.start()
-    for copy in copies:
+    return copies
+
+
+def cut_kernel(n_tp, place_ref, exit_ref, skip_ref, *refs):
+    evens, odd_ref, skip_out, sems = refs[: n_tp // 2], refs[-3], refs[-2], refs[-1]
+    wide = skip_out.shape[1]
+    pairs = []
+    for i, ref in enumerate(evens):
+        target = odd_ref.at[:, i * wide : (i + 1) * wide]
+        pairs.append((block_of(exit_ref, place_ref, 2 * i + 1, wide), target))
+        pairs.append((block_of(exit_ref, place_ref, 2 * i, wide), ref))
+    pairs.append((block_of(skip_ref, place_ref, 0, wide), skip_out))
+    for copy in run_copies(pairs, sems):
         copy.wait()
 
 
 def cut_blocks(place, exit_matrix, skip, n_tp):
-    wide = skip.shape[1] // n_tp
-    block = jax.ShapeDtypeStruct((exit_matrix.shape[0], wide), BF16)
-    anywhere = pl.BlockSpec(memory_space=pl.ANY)
-    *exits, own_skip = pl.pallas_call(
+    channels, wide = exit_matrix.shape[0], exit_matrix.shape[1] // n_tp
+    *evens, odd, own_skip = pl.pallas_call(
         lambda *refs: cut_kernel(n_tp, *refs),
         in_specs=[pl.BlockSpec(memory_space=pltpu.SMEM)] + hbm(2),
-        out_specs=[anywhere] * (n_tp + 1),
-        out_shape=[block] * n_tp + [jax.ShapeDtypeStruct((skip.shape[0], wide), BF16)],
+        out_specs=vmem(n_tp // 2 + 2),
+        out_shape=[jax.ShapeDtypeStruct((channels, wide), BF16)] * (n_tp // 2)
+        + [
+            jax.ShapeDtypeStruct((channels, wide * n_tp // 2), BF16),
+            jax.ShapeDtypeStruct((skip.shape[0], wide), BF16),
+        ],
         scratch_shapes=[pltpu.SemaphoreType.DMA((n_tp + 1,))],
-        compiler_params=pltpu.CompilerParams(vmem_limit_bytes=2**20),
+        compiler_params=pltpu.CompilerParams(vmem_limit_bytes=4 * 2**20),
         name="cut_blocks",
-    )(place, exit_matrix, skip)
-    return exits, own_skip
+    )(place, *in_hbm((exit_matrix, skip)))
+    return evens, odd, own_skip
+
+
+def partial_kernel(mixed_ref, other_ref, odd_ref, *refs):
+    evens, outs = refs[: len(refs) // 2], refs[len(refs) // 2 :]
+    wide = evens[0].shape[1]
+    for i, (even, out) in enumerate(zip(evens, outs)):
+        total = jnp.dot(mixed_ref[...], even[...], preferred_element_type=F32)
+        total = total + jnp.dot(
+            other_ref[...], odd_ref[:, i * wide : (i + 1) * wide], preferred_element_type=F32
+        )
+        out[...] = total.astype(out.dtype)
+
+
+def partial_sums(mixed, other, odd, evens):
+    length, wide = mixed.shape[0], evens[0].shape[1]
+    kinds = [F32] + [BF16] * (len(evens) - 1)
+    return pl.pallas_call(
+        partial_kernel,
+        in_specs=vmem(3 + len(evens)),
+        out_specs=vmem(len(evens)),
+        out_shape=[jax.ShapeDtypeStruct((length, wide), kind) for kind in kinds],
+        compiler_params=pltpu.CompilerParams(vmem_limit_bytes=8 * 2**20),
+        name="partial_sums",
+    )(mixed, other, odd, *evens)
 
 
 def route_kernel(experts, capacity, place_ref, chosen_ref, score_ref, pick_ref, high_ref, low_ref):
-    chosen, score = chosen_ref[...], score_ref[...]
-    length, top = chosen.shape
-    share = score / jnp.sum(score, axis=1, keepdims=True)
+    top, length = chosen_ref.shape
+    square = (length, length)
+    diagonal = (
+        lax.broadcasted_iota(jnp.int32, square, 0) == lax.broadcasted_iota(jnp.int32, square, 1)
+    )
+
+    def column(row):
+        spread = jnp.where(diagonal, jnp.broadcast_to(row, square), 0.0)
+        return jnp.sum(spread, axis=1, keepdims=True)
+
+    score = [column(score_ref[k : k + 1, :]) for k in range(top)]
+    chosen = [
+        column(chosen_ref[k : k + 1, :].astype(F32)).astype(jnp.int32) for k in range(top)
+    ]
+    whole = sum(score)
     lane = lax.broadcasted_iota(jnp.int32, (length, experts), 1)
-    named = [chosen[:, k : k + 1] == lane for k in range(top)]
+    named = [chosen[k] == lane for k in range(top)]
     counted = sum(jnp.where(one, 1.0, 0.0) for one in named)
     before = (
         lax.broadcasted_iota(jnp.int32, (length, length), 0)
@@ -325,9 +390,9 @@
     pick = weight = 0.0
     for k, one in enumerate(named):
         rank = jnp.sum(jnp.where(one, ranks, 0.0), axis=1, keepdims=True).astype(jnp.int32)
-        hit = grid == (chosen[:, k : k + 1] ^ place_ref[0]) * capacity + rank
+        hit = grid == (chosen[k] ^ place_ref[0]) * capacity + rank
         pick = pick + jnp.where(hit, 1.0, 0.0)
-        weight = weight + jnp.where(hit, share[:, k : k + 1], 0.0)
+        weight = weight + jnp.where(hit, score[k] / whole, 0.0)
     pick_ref[...] = jnp.transpose(pick).astype(BF16)
     high = weight.astype(BF16)
     high_ref[...] = high
@@ -337,14 +402,16 @@
 def route(place, chosen, score, experts, capacity):
     length = chosen.shape[0]
     weight = jax.ShapeDtypeStruct((length, experts * capacity), BF16)
+    args = (chosen.T, score.T)
     return pl.pallas_call(
-        lambda *refs: route_kernel(experts, capacity, *refs),
-        in_specs=[pl.BlockSpec(memory_space=pltpu.SMEM)] + vmem(2),
+        staged(lambda *refs: route_kernel(experts, capacity, *refs), 1, len(args)),
+        in_specs=[pl.BlockSpec(memory_space=pltpu.SMEM)] + hbm(2),
         out_specs=vmem(3),
+        scratch_shapes=stage(args),
         out_shape=[jax.ShapeDtypeStruct((experts * capacity, length), BF16), weight, weight],
         compiler_params=pltpu.CompilerParams(vmem_limit_bytes=8 * 2**20),
         name="route",
-    )(place, chosen, score)
+    )(place, *in_hbm(args))
 
 
 def pack_kernel(*refs):
@@ -365,12 +432,11 @@
     )(*parts)
 
 
-def project_kernel(n_tp, *refs):
-    mixed, exits = refs[:n_tp], refs[n_tp : 2 * n_tp]
-    skip_ref, pick_ref, stream_ref, *rows = refs[2 * n_tp :]
-    total = 0.0
-    for k in range(n_tp):
-        total = total + jnp.dot(mixed[k][...], exits[k][...], preferred_element_type=F32)
+def project_kernel(count, *refs):
+    skip_ref, pick_ref, stream_ref, *rows = refs[count:]
+    total = refs[0][...]
+    for ref in refs[1:count]:
+        total = total + ref[...].astype(F32)
     stream = (skip_ref[...].astype(F32) + total.astype(BF16).astype(F32)).astype(BF16)
     stream_ref[...] = stream
     picked = jnp.dot(pick_ref[...], stream, preferred_element_type=F32).astype(BF16)
@@ -379,18 +445,17 @@
         ref[...] = picked[k * height : (k + 1) * height]
 
 
-def project(mixed, exits, skip, pick, experts):
+def project(sums, skip, pick, experts):
     length, d_local = skip.shape
-    n_tp = len(mixed)
     return pl.pallas_call(
-        lambda *refs: project_kernel(n_tp, *refs),
-        in_specs=vmem(2 * n_tp + 2),
+        lambda *refs: project_kernel(len(sums), *refs),
+        in_specs=vmem(len(sums) + 2),
         out_specs=vmem(1 + experts),
         out_shape=[jax.ShapeDtypeStruct((length, d_local), BF16)]
         + [jax.ShapeDtypeStruct((pick.shape[0] // experts, d_local), BF16)] * experts,
-        compiler_params=pltpu.CompilerParams(vmem_limit_bytes=12 * 2**20),
+        compiler_params=pltpu.CompilerParams(vmem_limit_bytes=8 * 2**20),
         name="project",
-    )(*mixed, *exits, skip, pick)
+    )(*sums, skip, pick)
 
 
 def fold_kernel(pairs, *refs):
@@ -435,15 +500,16 @@
     )(stream, high, low, *back)
 
 
-def ffn_kernel(n_tp, width, place_ref, *refs):
-    pieces = refs[:n_tp]
-    scale_ref, gate_ref, up_ref, down_ref = refs[n_tp : n_tp + 4]
-    outs = refs[n_tp + 4 :]
+def ffn_kernel(n_tp, groups, width, place_ref, *refs):
+    pieces = refs[: n_tp * groups]
+    scale_ref, gate_ref, up_ref, down_ref = refs[n_tp * groups : n_tp * groups + 4]
+    outs = refs[n_tp * groups + 4 :]
     me = place_ref[1]
     d_local = pieces[0].shape[1]
     square = gate = up = 0.0
     for k in range(n_tp):
-        rows = pieces[k][...].astype(F32)
+        parts = [pieces[g * n_tp + k][...] for g in range(groups)]
+        rows = jnp.concatenate(parts, axis=0).astype(F32)
         square = square + jnp.sum(rows * rows, axis=1, keepdims=True)
         place = pl.multiple_of((me ^ k) * d_local, d_local)
         scaled = (rows * scale_ref[me ^ k]).astype(BF16)
@@ -456,9 +522,14 @@
     hidden = (gate * jax.nn.sigmoid(gate) * (up * inv_rms)).astype(BF16)
     for k in range(n_tp):
         place = pl.multiple_of((me ^ k) * d_local, d_local)
-        outs[k][...] = jnp.dot(
+        done = jnp.dot(
             hidden, down_ref[:, pl.ds(place, d_local)], preferred_element_type=F32
         ).astype(BF16)
+        start = 0
+        for g in range(groups):
+            out = outs[g * n_tp + k]
+            out[...] = done[start : start + out.shape[0]]
+            start += out.shape[0]
 
 
 def load_kernel(*refs):
@@ -482,18 +553,19 @@
         scratch_shapes=[pltpu.SemaphoreType.DMA((len(weights),))],
         compiler_params=pltpu.CompilerParams(vmem_limit_bytes=16 * 2**20),
         name="load",
-    )(*weights)
-
-
-def ffn(place, pieces, scale, gate_w, up_w, down_w):
-    n_tp = len(pieces)
-    rows, d_local = pieces[0].shape
+    )(*in_hbm(weights))
+
+
+def ffn(place, grouped, scale, gate_w, up_w, down_w):
+    n_tp, groups = len(grouped[0]), len(grouped)
+    pieces = [piece for group in grouped for piece in group]
+    rows = sum(group[0].shape[0] for group in grouped)
     width, units = gate_w.shape
-    return pl.pallas_call(
-        lambda *refs: ffn_kernel(n_tp, width, *refs),
-        in_specs=[pl.BlockSpec(memory_space=pltpu.SMEM)] + vmem(n_tp + 4),
-        out_specs=vmem(n_tp),
-        out_shape=[jax.ShapeDtypeStruct((rows, d_local), BF16)] * n_tp,
+    outs = pl.pallas_call(
+        lambda *refs: ffn_kernel(n_tp, groups, width, *refs),
+        in_specs=[pl.BlockSpec(memory_space=pltpu.SMEM)] + vmem(len(pieces) + 4),
+        out_specs=vmem(len(pieces)),
+        out_shape=[jax.ShapeDtypeStruct(piece.shape, BF16) for piece in pieces],
         compiler_params=pltpu.CompilerParams(vmem_limit_bytes=24 * 2**20),
         cost_estimate=pl.CostEstimate(
             flops=6 * rows * width * units,
@@ -502,6 +574,7 @@
         ),
         name="expert_ffn",
     )(place, *pieces, scale, gate_w, up_w, down_w)
+    return [outs[g * n_tp : (g + 1) * n_tp] for g in range(groups)]
 
 
 def gather_pieces(own, n_tp):
@@ -556,12 +629,7 @@
     tok_local, top = selected_specialists.shape
     capacity = 2 * tok_local * top // experts
     place = jnp.stack([lax.axis_index("sp"), lax.axis_index("tp")]).astype(jnp.int32)
-    exits, own_skip = cut_blocks(place, lane_exit_matrix, skipline_stream, n_tp)
-    for k in range(1, n_tp):
-        exits[k] = swap(exits[k], "tp", k)
-
-    mixed = mixer(
-        place,
+    args = mixer_args(
         lane_source_signal,
         spectral_damping_part,
         spectral_angular_part,
@@ -573,33 +641,54 @@
         lane_bypass_factor,
         spike_shrink_offset,
     )
-    others = [mixed]
-    for k in range(1, n_tp):
-        others.append(swap(mixed, "tp", k))
+    evens, odd, own_skip = cut_blocks(place, lane_exit_matrix, skipline_stream, n_tp)
+    odd = swap(odd, "tp", 1)
+    mixed = mixer(place, args)
+    other = swap(mixed, "tp", 1)
+    held = dict(zip(range(0, n_tp, 2), partial_sums(mixed, other, odd, evens)))
+    sums = [held[0]]
+    bit = 2
+    while bit < n_tp:
+        for k in [k for k in held if k & bit]:
+            moved = swap(held.pop(k), "tp", bit)
+            if k == bit:
+                sums.append(moved)
+            else:
+                held[k ^ bit] = (held[k ^ bit].astype(F32) + moved.astype(F32)).astype(BF16)
+        bit *= 2
     pick, high, low = route(place, selected_specialists, dispatcher_scores, experts, capacity)
-    gate_w, up_w, down_w = load(
-        specialist_valve_matrix[0], specialist_widen_matrix[0], specialist_shrink_matrix[0]
-    )
+    gate_w, up_w = load(specialist_valve_matrix[0], specialist_widen_matrix[0])
+    (down_w,) = load(specialist_shrink_matrix[0])
     scale = specialist_scaling_vector.reshape(n_tp, 1, d_local)
 
-    stream, *rows = project(others, exits, own_skip, pick, experts)
+    stream, *rows = project(sums, own_skip, pick, experts)
     arrived = {}
     for k in range(experts):
         arrived[k] = swap(rows[k], "sp", k) if k else rows[k]
+    chunks = chunks_of(experts)
+    pieces = []
+    for chunk in chunks:
+        own = [arrived[k] for k in chunk]
+        pieces.append(gather_pieces(pack(own) if len(own) > 1 else own[0], n_tp))
+    parts = []
+    for members in calls_of(len(chunks)):
+        parts += ffn(place, [pieces[i] for i in members], scale, gate_w, up_w, down_w)
     back = {}
-    for chunk in chunks_of(experts):
-        pieces = gather_pieces(pack([arrived[k] for k in chunk]), n_tp)
-        parts = ffn(place, pieces, scale, gate_w, up_w, down_w)
-        sums = scatter_sum(parts, n_tp, len(chunk))
+    for c, chunk in enumerate(chunks):
+        sums = scatter_sum(parts[c], n_tp, len(chunk))
         for k, total in zip(chunk, sums):
             back[k] = swap(total, "sp", k) if k else total
     return combine(stream, high, low, [back[k] for k in range(experts)])
 
 
 def chunks_of(experts):
-    near = list(range(experts // 2))
-    far = list(range(experts // 2, experts))
-    return near, far[: experts // 4], far[experts // 4 :]
+    half, part = experts // 2, experts // 4
+    cuts = [0, max(1, experts // 8), half, half + part, experts]
+    return [list(range(a, b)) for a, b in zip(cuts, cuts[1:])]
+
+
+def calls_of(chunks):
+    return [(0, 1)] + [(c,) for c in range(2, chunks)]
 
 
 def solution(mesh):

time: 157 us -> 138 us (0.88)
  local copies, waits for them, and re-layouts: 17.1 us -> 0.01 us
  waiting for transfers between devices: 69.4 us -> 61.2 us
  Pallas kernels: 22.4 us -> 28.1 us
    unnamed x42 -> x2, local copies, waits for them, and re-layouts: 17.1 us -> 0.01 us
    ppermute x38 -> x41, waiting for transfers between devices: 69.4 us -> 61.2 us  [swap(): return lax.ppermute(value, axis, [(i, i ^ bits) for i in range(count)])]
    pallas_call x1 -> x2, Pallas kernels: 1.04 us -> 5.69 us  [load(): pl.pallas_call(load_kernel, in_specs=hbm(len(weights)), out_specs=vmem(le...]
    pallas_call x7 -> x8, Pallas kernels: 17.7 us -> 18.3 us  [the longest x3 9.35 us: ffn(): pl.pallas_call(lambda *refs: ffn_kernel(n_tp, groups, width, *refs), in_s...]
    ppermute x38 -> x41, starting transfers between devices: 34 us -> 34.2 us  [swap(): return lax.ppermute(value, axis, [(i, i ^ bits) for i in range(count)])]
  transfers between devices with their start and end apart: 38 -> 41, of which waited for: 16 -> 17; matrix products, arithmetic and copies ran while one was open for 0% -> 0% of each run, Pallas kernels for 12% -> 17%
where the time goes in v2:
time: 138 us
  waiting for transfers between devices  61.2 us (44%)
  starting transfers between devices  34.2 us (25%)
  Pallas kernels  28.1 us (20%)
  blocking collectives  14.2 us (10%)
    ppermute x41, waiting for transfers between devices, swap(): return lax.ppermute(value, axis, [(i, i ^ bits) for i in range(count)])  61.2 us
    ppermute x41, starting transfers between devices, swap(): return lax.ppermute(value, axis, [(i, i ^ bits) for i in range(count)])  34.2 us
    all_to_all x1, blocking collectives, mixer(): pieces = lax.all_to_all(summary, 'sp', 0, 0, tiled=True)  14.2 us
    pallas_call x3, Pallas kernels, ffn(): pl.pallas_call(lambda *refs: ffn_kernel(n_tp, groups, width, *refs), in_s...  9.35 us
    pallas_call x2, Pallas kernels, load(): pl.pallas_call(load_kernel, in_specs=hbm(len(weights)), out_specs=vmem(le...  5.69 us
    pallas_call x1, Pallas kernels, mixer(): pl.pallas_call(first_kernel, in_specs=hbm(10), out_specs=vmem(6), out_sha...  4.86 us
  transfers between devices with their start and end apart: 41, of which 17 were waited for; matrix products, arithmetic and copies ran while one was open for 0% of the time, Pallas kernels for 17%

profile of v2, /device:TPU:0, one launch (start us, length us, event | category | flops | bytes accessed | tf_op | source)
XLA Modules:
  0.0 138.0 jit_solution(9463924733061943573)
XLA Ops:
  0.1 2.2 %cut_blocks.1 = (bf16[256,1024]{1,0:T(8,128)(2,1)S(1)}, bf16[256,1024]{1,0:T(8,128)(2,1)S(1)}, bf16[256,2048]{1,0:T(8,128)(2,1)S(1)}, bf16[128,1024]{1,0:T(8,128)(2,1)S(1)}) custom-call(s32[2]{0:T(128)S(1)} %pad_add_fusion.mine_ref.refs_0_, bf16[256,4096]{1,0:T(8,128)(2,1)} %refs_1_.3, bf16[128,4096]{1,0:T(8,128)(2,1)} %refs_2_.3), custom_call_target="tpu_custom_call" | custom-call | tf_op jit(solution)/shard_map/cut_blocks/pallas_call | solution.py:322
  2.3 0.6 collective-permute-start.1
  2.8 4.9 %mixer_scan.1 = (f32[8,8,512]{2,1,0:T(8,128)S(1)}, f32[128,256]{1,0:T(8,128)S(1)}, f32[14,1024]{1,0:T(8,128)S(1)}, f32[128,16]{1,0:T(8,128)S(1)}, f32[16,16,64]{2,1,0:T(8,128)S(1)}, /*index=5*/f32[16,16,64]{2,1,0:T(8,128)S(1)}) custom-call(bf16[256,128]{1,0:T(8,128)(2,1)} %refs_0_.1, f32[16,64]{1,0:T(8,128)} %refs_1_.2, f32[16,64]{1,0:T(8,128)} %refs_2_.2, ...), custom_call_target="tpu_custom_call" | custom-call | tf_op jit(solution)/shard_map/mixer_scan/pallas_call | solution.py:265
  7.7 14.2 %all_to_all.5.pieces_ref = f32[8,8,512]{2,1,0:T(8,128)S(1)} all-to-all(f32[8,8,512]{2,1,0:T(8,128)S(1)} %get-tuple-element.62), channel_id=1, replica_groups=mesh['sp'=8,'tp'=4] {'sp'}, dimensions={0} | all-to-all | bytes 262144 | tf_op jit(solution)/shard_map/all_to_all | solution.py:282
  21.9 1.4 %mixer_readout.1.mixed_ref = bf16[128,256]{1,0:T(8,128)(2,1)S(1)} custom-call(s32[2]{0:T(128)S(1)} %pad_add_fusion.mine_ref.refs_0_, f32[8,8,512]{2,1,0:T(8,128)S(1)} %all_to_all.5.pieces_ref, f32[128,256]{1,0:T(8,128)S(1)} %get-tuple-element.63.local_ref, f32[14,1024]{1,0:T(8,128)S(1)} %get-tuple-element.64.powers_ref, ...), custom_call_target="tpu_custom_call" | custom-call | tf_op jit(solution)/shard_map/mixer_readout/pallas_call | solution.py:283
  23.4 1.2 collective-permute-done.other_ref
  25.1 1.6 %collective-permute-start.2 = (bf16[128,1024]{1,0:T(8,128)(2,1)S(1)}, bf16[128,1024]{1,0:T(8,128)(2,1)S(1)}, u32[]{:S(2)}, u32[]{:S(2)}) collective-permute-start(bf16[128,1024]{1,0:T(8,128)(2,1)S(1)} %get-tuple-element.72), channel_id=1, source_target_pairs={{0,2},{1,3},{2,0},{3,1},{4,6},{5,7},{6,4},{7,5},{8,10},{9,11},{10,... | collective-permute-start | bytes 786440 | tf_op jit(solution)/shard_map/ppermute | solution.py:15
  26.7 1.8 %route.1 = (bf16[512,128]{1,0:T(8,128)(2,1)S(1)}, bf16[128,512]{1,0:T(8,128)(2,1)S(1)}, bf16[128,512]{1,0:T(8,128)(2,1)S(1)}) custom-call(s32[2]{0:T(128)S(1)} %pad_add_fusion.mine_ref.refs_0_, s32[2,128]{1,0:T(2,128)} %bitcast.21, f32[2,128]{1,0:T(2,128)} %bitcast.22), custom_call_target="tpu_custom_call" | custom-call | tf_op jit(solution)/shard_map/route/pallas_call | solution.py:406
  28.5 5.1 %collective-permute-done.2.refs_1_ = bf16[128,1024]{1,0:T(8,128)(2,1)S(1)} collective-permute-done((bf16[128,1024]{1,0:T(8,128)(2,1)S(1)}, bf16[128,1024]{1,0:T(8,128)(2,1)S(1)}, u32[]{:S(2)}, u32[]{:S(2)}) %collective-permute-start.2) | collective-permute-done | bytes 262176 | tf_op jit(solution)/shard_map/ppermute | solution.py:15
  34.4 1.0 collective-permute-start.7
  35.4 2.2 %collective-permute-start.8 = (bf16[64,1024]{1,0:T(8,128)(2,1)S(1)}, bf16[64,1024]{1,0:T(8,128)(2,1)S(1)}, u32[]{:S(2)}, u32[]{:S(2)}) collective-permute-start(bf16[64,1024]{1,0:T(8,128)(2,1)S(1)} %get-tuple-element.81), channel_id=1, source_target_pairs={{0,12},{4,8},{8,4},{12,0},{16,28},{20,24},{24,20},{28,16},{1,13},{... | collective-permute-start | bytes 393224 | tf_op jit(solution)/shard_map/ppermute | solution.py:15
  37.6 2.5 %collective-permute-done.6.refs_0_ = bf16[64,1024]{1,0:T(8,128)(2,1)S(1)} collective-permute-done((bf16[64,1024]{1,0:T(8,128)(2,1)S(1)}, bf16[64,1024]{1,0:T(8,128)(2,1)S(1)}, u32[]{:S(2)}, u32[]{:S(2)}) %collective-permute-start.6) | collective-permute-done | bytes 131104 | tf_op jit(solution)/shard_map/ppermute | solution.py:15
  40.3 2.5 %collective-permute-done.8.refs_2_ = bf16[64,1024]{1,0:T(8,128)(2,1)S(1)} collective-permute-done((bf16[64,1024]{1,0:T(8,128)(2,1)S(1)}, bf16[64,1024]{1,0:T(8,128)(2,1)S(1)}, u32[]{:S(2)}, u32[]{:S(2)}) %collective-permute-start.8) | collective-permute-done | bytes 131104 | tf_op jit(solution)/shard_map/ppermute | solution.py:15
  42.8 1.6 %collective-permute-start.10 = (bf16[192,1024]{1,0:T(8,128)(2,1)S(1)}, bf16[192,1024]{1,0:T(8,128)(2,1)S(1)}, u32[]{:S(2)}, u32[]{:S(2)}) collective-permute-start(bf16[192,1024]{1,0:T(8,128)(2,1)S(1)} %pack.3.refs_5_), channel_id=1, source_target_pairs={{0,2},{1,3},{2,0},{3,1},{4,6},{5,7},{6,4},{7,5},{8,10},{9,11},{10,... | collective-permute-start | bytes 1179656 | tf_op jit(solution)/shard_map/ppermute | solution.py:15
  44.9 2.2 %collective-permute-start.22 = (bf16[64,1024]{1,0:T(8,128)(2,1)S(1)}, bf16[64,1024]{1,0:T(8,128)(2,1)S(1)}, u32[]{:S(2)}, u32[]{:S(2)}) collective-permute-start(bf16[64,1024]{1,0:T(8,128)(2,1)S(1)} %get-tuple-element.100), channel_id=1, source_target_pairs={{0,20},{4,16},{8,28},{12,24},{16,4},{20,0},{24,12},{28,8},{1,21},{... | collective-permute-start | bytes 393224 | tf_op jit(solution)/shard_map/ppermute | solution.py:15
  47.1 1.6 %collective-permute-start.31 = (bf16[64,1024]{1,0:T(8,128)(2,1)S(1)}, bf16[64,1024]{1,0:T(8,128)(2,1)S(1)}, u32[]{:S(2)}, u32[]{:S(2)}) collective-permute-start(bf16[64,1024]{1,0:T(8,128)(2,1)S(1)} %get-tuple-element.109), channel_id=1, source_target_pairs={{0,24},{4,28},{8,16},{12,20},{16,8},{20,12},{24,0},{28,4},{1,25},{... | collective-permute-start | bytes 393224 | tf_op jit(solution)/shard_map/ppermute | solution.py:15
  48.8 3.3 %collective-permute-start.32 = (bf16[64,1024]{1,0:T(8,128)(2,1)S(1)}, bf16[64,1024]{1,0:T(8,128)(2,1)S(1)}, u32[]{:S(2)}, u32[]{:S(2)}) collective-permute-start(bf16[64,1024]{1,0:T(8,128)(2,1)S(1)} %get-tuple-element.110), channel_id=1, source_target_pairs={{0,28},{4,24},{8,20},{12,16},{16,12},{20,8},{24,4},{28,0},{1,29},{... | collective-permute-start | bytes 393224 | tf_op jit(solution)/shard_map/ppermute | solution.py:15
  52.1 7.8 %collective-permute-done.21.refs_0_ = bf16[64,1024]{1,0:T(8,128)(2,1)S(1)} collective-permute-done((bf16[64,1024]{1,0:T(8,128)(2,1)S(1)}, bf16[64,1024]{1,0:T(8,128)(2,1)S(1)}, u32[]{:S(2)}, u32[]{:S(2)}) %collective-permute-start.21) | collective-permute-done | bytes 131104 | tf_op jit(solution)/shard_map/ppermute | solution.py:15
  59.8 3.8 %collective-permute-done.22.refs_1_ = bf16[64,1024]{1,0:T(8,128)(2,1)S(1)} collective-permute-done((bf16[64,1024]{1,0:T(8,128)(2,1)S(1)}, bf16[64,1024]{1,0:T(8,128)(2,1)S(1)}, u32[]{:S(2)}, u32[]{:S(2)}) %collective-permute-start.22) | collective-permute-done | bytes 131104 | tf_op jit(solution)/shard_map/ppermute | solution.py:15
  63.6 0.5 collective-permute-start.11
  64.2 0.6 collective-permute-start.4
  64.7 1.5 %collective-permute-start.24 = (bf16[128,1024]{1,0:T(8,128)(2,1)S(1)}, bf16[128,1024]{1,0:T(8,128)(2,1)S(1)}, u32[]{:S(2)}, u32[]{:S(2)}) collective-permute-start(bf16[128,1024]{1,0:T(8,128)(2,1)S(1)} %pack.4.refs_1_), channel_id=1, source_target_pairs={{0,2},{1,3},{2,0},{3,1},{4,6},{5,7},{6,4},{7,5},{8,10},{9,11},{10,... | collective-permute-start | bytes 786440 | tf_op jit(solution)/shard_map/ppermute | solution.py:15
  66.3 0.6 collective-permute-start.34
  66.9 3.7 %collective-permute-done.4.refs_3_ = bf16[64,1024]{1,0:T(8,128)(2,1)S(1)} collective-permute-done((bf16[64,1024]{1,0:T(8,128)(2,1)S(1)}, bf16[64,1024]{1,0:T(8,128)(2,1)S(1)}, u32[]{:S(2)}, u32[]{:S(2)}) %collective-permute-start.4) | collective-permute-done | bytes 131104 | tf_op jit(solution)/shard_map/ppermute | solution.py:15
  70.6 2.2 %load.3.refs_12_.refs_8_ = bf16[512,4096]{1,0:T(8,128)(2,1)S(1)} custom-call(bf16[512,4096]{1,0:T(8,128)(2,1)} %bitcast.15), custom_call_target="tpu_custom_call" | custom-call | tf_op jit(solution)/shard_map/load/pallas_call | solution.py:548
  72.8 3.5 %load.2 = (bf16[4096,512]{1,0:T(8,128)(2,1)S(1)}, bf16[4096,512]{1,0:T(8,128)(2,1)S(1)}) custom-call(bf16[4096,512]{1,0:T(8,128)(2,1)} %bitcast.16, bf16[4096,512]{1,0:T(8,128)(2,1)} %bitcast.17), custom_call_target="tpu_custom_call" | custom-call | tf_op jit(solution)/shard_map/load/pallas_call | solution.py:548
  76.3 0.6 collective-permute-start.23
  77.0 3.9 %collective-permute-done.34.refs_3_ = bf16[128,1024]{1,0:T(8,128)(2,1)S(1)} collective-permute-done((bf16[128,1024]{1,0:T(8,128)(2,1)S(1)}, bf16[128,1024]{1,0:T(8,128)(2,1)S(1)}, u32[]{:S(2)}, u32[]{:S(2)}) %collective-permute-start.34) | collective-permute-done | bytes 262176 | tf_op jit(solution)/shard_map/ppermute | solution.py:15
  81.4 4.2 %expert_ffn.3 = (bf16[64,1024]{1,0:T(8,128)(2,1)S(1)}, bf16[64,1024]{1,0:T(8,128)(2,1)S(1)}, bf16[64,1024]{1,0:T(8,128)(2,1)S(1)}, bf16[64,1024]{1,0:T(8,128)(2,...) custom-call(s32[2]{0:T(128)S(1)} %pad_add_fusion.mine_ref.refs_0_, ...), custom_call_target="tpu_custom_call" | custom-call | flops 3221225472 | bytes 16777216 | tf_op jit(solution)/shard_map/expert_ffn/pallas_call | solution.py:564
  86.2 2.6 %expert_ffn.4 = (bf16[128,1024]{1,0:T(8,128)(2,1)S(1)}, bf16[128,1024]{1,0:T(8,128)(2,1)S(1)}, bf16[128,1024]{1,0:T(8,128)(2,1)S(1)}, bf16[128,1024]{1,0:T(8,128)(2,1)S(1)}) custom-call(s32[2]{0:T(128)S(1)} %pad_add_fusion.mine_ref.refs_0_, bf16[128,1024]{1,0:T(8,128)(2,1)S(1)} %pack.4.refs_1_, bf16[128,1024]{1,0:T(8,128)(2,1)S(1)} %collective-permute-done.23.refs_2_, ...), custom_call_target="tpu_custom_call" | custom-call | flops 1610612736 | bytes 14680064 | tf_op jit(solution)/shard_map/expert_ffn/pallas_call | solution.py:564
  89.3 2.6 %expert_ffn.5 = (bf16[128,1024]{1,0:T(8,128)(2,1)S(1)}, bf16[128,1024]{1,0:T(8,128)(2,1)S(1)}, bf16[128,1024]{1,0:T(8,128)(2,1)S(1)}, bf16[128,1024]{1,0:T(8,128)(2,1)S(1)}) custom-call(s32[2]{0:T(128)S(1)} %pad_add_fusion.mine_ref.refs_0_, bf16[128,1024]{1,0:T(8,128)(2,1)S(1)} %pack.5.refs_1_, bf16[128,1024]{1,0:T(8,128)(2,1)S(1)} %collective-permute-done.33.refs_2_, ...), custom_call_target="tpu_custom_call" | custom-call | flops 1610612736 | bytes 14680064 | tf_op jit(solution)/shard_map/expert_ffn/pallas_call | solution.py:564
  92.7 0.6 collective-permute-start.17
  93.4 1.6 %collective-permute-start.28 = (bf16[128,1024]{1,0:T(8,128)(2,1)S(1)}, bf16[128,1024]{1,0:T(8,128)(2,1)S(1)}, u32[]{:S(2)}, u32[]{:S(2)}) collective-permute-start(bf16[128,1024]{1,0:T(8,128)(2,1)S(1)} %get-tuple-element.106), channel_id=1, source_target_pairs={{0,2},{1,3},{2,0},{3,1},{4,6},{5,7},{6,4},{7,5},{8,10},{9,11},{10,... | collective-permute-start | bytes 786440 | tf_op jit(solution)/shard_map/ppermute | solution.py:15
  95.1 0.6 collective-permute-start.38
  96.2 0.8 collective-permute-done.12.refs_2_
  97.3 1.6 %collective-permute-start.14 = (bf16[64,1024]{1,0:T(8,128)(2,1)S(1)}, bf16[64,1024]{1,0:T(8,128)(2,1)S(1)}, u32[]{:S(2)}, u32[]{:S(2)}) collective-permute-start(bf16[64,1024]{1,0:T(8,128)(2,1)S(1)} %get-tuple-element.89), channel_id=1, source_target_pairs={{0,2},{1,3},{2,0},{3,1},{4,6},{5,7},{6,4},{7,5},{8,10},{9,11},{10,... | collective-permute-start | bytes 393224 | tf_op jit(solution)/shard_map/ppermute | solution.py:15
  98.9 11.5 %collective-permute-done.28.refs_1_ = bf16[128,1024]{1,0:T(8,128)(2,1)S(1)} collective-permute-done((bf16[128,1024]{1,0:T(8,128)(2,1)S(1)}, bf16[128,1024]{1,0:T(8,128)(2,1)S(1)}, u32[]{:S(2)}, u32[]{:S(2)}) %collective-permute-start.28) | collective-permute-done | bytes 262176 | tf_op jit(solution)/shard_map/ppermute | solution.py:15
  110.4 1.7 %collective-permute-start.29 = (bf16[64,1024]{1,0:T(8,128)(2,1)S(1)}, bf16[64,1024]{1,0:T(8,128)(2,1)S(1)}, u32[]{:S(2)}, u32[]{:S(2)}) collective-permute-start(bf16[64,1024]{1,0:T(8,128)(2,1)S(1)} %get-tuple-element.107), channel_id=1, source_target_pairs={{0,16},{4,20},{8,24},{12,28},{16,0},{20,4},{24,8},{28,12},{1,17},{... | collective-permute-start | bytes 393224 | tf_op jit(solution)/shard_map/ppermute | solution.py:15
  112.1 1.2 collective-permute-start.30
  113.3 2.7 %collective-permute-done.38.refs_1_ = bf16[128,1024]{1,0:T(8,128)(2,1)S(1)} collective-permute-done((bf16[128,1024]{1,0:T(8,128)(2,1)S(1)}, bf16[128,1024]{1,0:T(8,128)(2,1)S(1)}, u32[]{:S(2)}, u32[]{:S(2)}) %collective-permute-start.38) | collective-permute-done | bytes 262176 | tf_op jit(solution)/shard_map/ppermute | solution.py:15
  116.1 1.9 %collective-permute-start.39 = (bf16[64,1024]{1,0:T(8,128)(2,1)S(1)}, bf16[64,1024]{1,0:T(8,128)(2,1)S(1)}, u32[]{:S(2)}, u32[]{:S(2)}) collective-permute-start(bf16[64,1024]{1,0:T(8,128)(2,1)S(1)} %get-tuple-element.117), channel_id=1, source_target_pairs={{0,24},{4,28},{8,16},{12,20},{16,8},{20,12},{24,0},{28,4},{1,25},{... | collective-permute-start | bytes 393224 | tf_op jit(solution)/shard_map/ppermute | solution.py:15
  118.0 1.9 %collective-permute-start.40 = (bf16[64,1024]{1,0:T(8,128)(2,1)S(1)}, bf16[64,1024]{1,0:T(8,128)(2,1)S(1)}, u32[]{:S(2)}, u32[]{:S(2)}) collective-permute-start(bf16[64,1024]{1,0:T(8,128)(2,1)S(1)} %get-tuple-element.118), channel_id=1, source_target_pairs={{0,28},{4,24},{8,20},{12,16},{16,12},{20,8},{24,4},{28,0},{1,29},{... | collective-permute-start | bytes 393224 | tf_op jit(solution)/shard_map/ppermute | solution.py:15
  119.9 1.6 %collective-permute-start.18 = (bf16[64,1024]{1,0:T(8,128)(2,1)S(1)}, bf16[64,1024]{1,0:T(8,128)(2,1)S(1)}, u32[]{:S(2)}, u32[]{:S(2)}) collective-permute-start(bf16[64,1024]{1,0:T(8,128)(2,1)S(1)} %get-tuple-element.96), channel_id=1, source_target_pairs={{0,4},{4,0},{8,12},{12,8},{16,20},{20,16},{24,28},{28,24},{1,5},{5... | collective-permute-start | bytes 393224 | tf_op jit(solution)/shard_map/ppermute | solution.py:15
  121.6 5.7 %collective-permute-done.29.refs_4_ = bf16[64,1024]{1,0:T(8,128)(2,1)S(1)} collective-permute-done((bf16[64,1024]{1,0:T(8,128)(2,1)S(1)}, bf16[64,1024]{1,0:T(8,128)(2,1)S(1)}, u32[]{:S(2)}, u32[]{:S(2)}) %collective-permute-start.29) | collective-permute-done | bytes 131104 | tf_op jit(solution)/shard_map/ppermute | solution.py:15
  127.3 3.8 %collective-permute-done.30.refs_5_ = bf16[64,1024]{1,0:T(8,128)(2,1)S(1)} collective-permute-done((bf16[64,1024]{1,0:T(8,128)(2,1)S(1)}, bf16[64,1024]{1,0:T(8,128)(2,1)S(1)}, u32[]{:S(2)}, u32[]{:S(2)}) %collective-permute-start.30) | collective-permute-done | bytes 131104 | tf_op jit(solution)/shard_map/ppermute | solution.py:15
  131.1 1.4 %collective-permute-done.19.refs_2_ = bf16[64,1024]{1,0:T(8,128)(2,1)S(1)} collective-permute-done((bf16[64,1024]{1,0:T(8,128)(2,1)S(1)}, bf16[64,1024]{1,0:T(8,128)(2,1)S(1)}, u32[]{:S(2)}, u32[]{:S(2)}) %collective-permute-start.19) | collective-permute-done | bytes 131104 | tf_op jit(solution)/shard_map/ppermute | solution.py:15
  132.5 4.4 %collective-permute-done.20.refs_3_ = bf16[64,1024]{1,0:T(8,128)(2,1)S(1)} collective-permute-done((bf16[64,1024]{1,0:T(8,128)(2,1)S(1)}, bf16[64,1024]{1,0:T(8,128)(2,1)S(1)}, u32[]{:S(2)}, u32[]{:S(2)}) %collective-permute-start.20) | collective-permute-done | bytes 131104 | tf_op jit(solution)/shard_map/ppermute | solution.py:15
  136.9 1.2 combine.1
  (61 shorter events, 6.0 us)
Async XLA Ops:
  2.3 22.4 %collective-permute-start.1 = (bf16[256,2048]{1,0:T(8,128)(2,1)S(1)}, bf16[256,2048]{1,0:T(8,128)(2,1)S(1)}, u32[]{:S(2)}, u32[]{:S(2)}) collective-permute-start(bf16[256,2048]{1,0:T(8,128)(2,1)S(1)} %get-tuple-element.68), channel_id=1, source_target_pairs={{0,1},{1,0},{2,3},{3,2},{4,5},{5,4},{6,7},{7,6},{8,9},{9,8},{10,11... | collective-permute-start | bytes 3145736 | tf_op jit(solution)/shard_map/ppermute | solution.py:15
  23.3 1.3 collective-permute-start
  25.1 8.4 %collective-permute-start.2 = (bf16[128,1024]{1,0:T(8,128)(2,1)S(1)}, bf16[128,1024]{1,0:T(8,128)(2,1)S(1)}, u32[]{:S(2)}, u32[]{:S(2)}) collective-permute-start(bf16[128,1024]{1,0:T(8,128)(2,1)S(1)} %get-tuple-element.72), channel_id=1, source_target_pairs={{0,2},{1,3},{2,0},{3,1},{4,6},{5,7},{6,4},{7,5},{8,10},{9,11},{10,... | collective-permute-start | bytes 786440 | tf_op jit(solution)/shard_map/ppermute | solution.py:15
  34.0 6.1 %collective-permute-start.6 = (bf16[64,1024]{1,0:T(8,128)(2,1)S(1)}, bf16[64,1024]{1,0:T(8,128)(2,1)S(1)}, u32[]{:S(2)}, u32[]{:S(2)}) collective-permute-start(bf16[64,1024]{1,0:T(8,128)(2,1)S(1)} %get-tuple-element.79), channel_id=1, source_target_pairs={{0,4},{4,0},{8,12},{12,8},{16,20},{20,16},{24,28},{28,24},{1,5},{5... | collective-permute-start | bytes 393224 | tf_op jit(solution)/shard_map/ppermute | solution.py:15
  34.4 5.9 %collective-permute-start.7 = (bf16[64,1024]{1,0:T(8,128)(2,1)S(1)}, bf16[64,1024]{1,0:T(8,128)(2,1)S(1)}, u32[]{:S(2)}, u32[]{:S(2)}) collective-permute-start(bf16[64,1024]{1,0:T(8,128)(2,1)S(1)} %get-tuple-element.80), channel_id=1, source_target_pairs={{0,8},{4,12},{8,0},{12,4},{16,24},{20,28},{24,16},{28,20},{1,9},{5... | collective-permute-start | bytes 393224 | tf_op jit(solution)/shard_map/ppermute | solution.py:15
  35.4 7.4 %collective-permute-start.8 = (bf16[64,1024]{1,0:T(8,128)(2,1)S(1)}, bf16[64,1024]{1,0:T(8,128)(2,1)S(1)}, u32[]{:S(2)}, u32[]{:S(2)}) collective-permute-start(bf16[64,1024]{1,0:T(8,128)(2,1)S(1)} %get-tuple-element.81), channel_id=1, source_target_pairs={{0,12},{4,8},{8,4},{12,0},{16,28},{20,24},{24,20},{28,16},{1,13},{... | collective-permute-start | bytes 393224 | tf_op jit(solution)/shard_map/ppermute | solution.py:15
  42.8 20.8 %collective-permute-start.10 = (bf16[192,1024]{1,0:T(8,128)(2,1)S(1)}, bf16[192,1024]{1,0:T(8,128)(2,1)S(1)}, u32[]{:S(2)}, u32[]{:S(2)}) collective-permute-start(bf16[192,1024]{1,0:T(8,128)(2,1)S(1)} %pack.3.refs_5_), channel_id=1, source_target_pairs={{0,2},{1,3},{2,0},{3,1},{4,6},{5,7},{6,4},{7,5},{8,10},{9,11},{10,... | collective-permute-start | bytes 1179656 | tf_op jit(solution)/shard_map/ppermute | solution.py:15
  44.4 15.4 %collective-permute-start.21 = (bf16[64,1024]{1,0:T(8,128)(2,1)S(1)}, bf16[64,1024]{1,0:T(8,128)(2,1)S(1)}, u32[]{:S(2)}, u32[]{:S(2)}) collective-permute-start(bf16[64,1024]{1,0:T(8,128)(2,1)S(1)} %get-tuple-element.99), channel_id=1, source_target_pairs={{0,16},{4,20},{8,24},{12,28},{16,0},{20,4},{24,8},{28,12},{1,17},{... | collective-permute-start | bytes 393224 | tf_op jit(solution)/shard_map/ppermute | solution.py:15
  44.9 18.7 %collective-permute-start.22 = (bf16[64,1024]{1,0:T(8,128)(2,1)S(1)}, bf16[64,1024]{1,0:T(8,128)(2,1)S(1)}, u32[]{:S(2)}, u32[]{:S(2)}) collective-permute-start(bf16[64,1024]{1,0:T(8,128)(2,1)S(1)} %get-tuple-element.100), channel_id=1, source_target_pairs={{0,20},{4,16},{8,28},{12,24},{16,4},{20,0},{24,12},{28,8},{1,21},{... | collective-permute-start | bytes 393224 | tf_op jit(solution)/shard_map/ppermute | solution.py:15
  47.1 17.0 %collective-permute-start.31 = (bf16[64,1024]{1,0:T(8,128)(2,1)S(1)}, bf16[64,1024]{1,0:T(8,128)(2,1)S(1)}, u32[]{:S(2)}, u32[]{:S(2)}) collective-permute-start(bf16[64,1024]{1,0:T(8,128)(2,1)S(1)} %get-tuple-element.109), channel_id=1, source_target_pairs={{0,24},{4,28},{8,16},{12,20},{16,8},{20,12},{24,0},{28,4},{1,25},{... | collective-permute-start | bytes 393224 | tf_op jit(solution)/shard_map/ppermute | solution.py:15
  48.8 16.0 %collective-permute-start.32 = (bf16[64,1024]{1,0:T(8,128)(2,1)S(1)}, bf16[64,1024]{1,0:T(8,128)(2,1)S(1)}, u32[]{:S(2)}, u32[]{:S(2)}) collective-permute-start(bf16[64,1024]{1,0:T(8,128)(2,1)S(1)} %get-tuple-element.110), channel_id=1, source_target_pairs={{0,28},{4,24},{8,20},{12,16},{16,12},{20,8},{24,4},{28,0},{1,29},{... | collective-permute-start | bytes 393224 | tf_op jit(solution)/shard_map/ppermute | solution.py:15
  59.8 6.5 %collective-permute-start.3 = (bf16[64,1024]{1,0:T(8,128)(2,1)S(1)}, bf16[64,1024]{1,0:T(8,128)(2,1)S(1)}, u32[]{:S(2)}, u32[]{:S(2)}) collective-permute-start(bf16[64,1024]{1,0:T(8,128)(2,1)S(1)} %get-tuple-element.78.refs_1_), channel_id=1, source_target_pairs={{0,1},{1,0},{2,3},{3,2},{4,5},{5,4},{6,7},{7,6},{8,9},{9,8},{10,11... | collective-permute-start | bytes 393224 | tf_op jit(solution)/shard_map/ppermute | solution.py:15
  63.6 17.3 %collective-permute-start.9 = (bf16[192,1024]{1,0:T(8,128)(2,1)S(1)}, bf16[192,1024]{1,0:T(8,128)(2,1)S(1)}, u32[]{:S(2)}, u32[]{:S(2)}) collective-permute-start(bf16[192,1024]{1,0:T(8,128)(2,1)S(1)} %pack.3.refs_5_), channel_id=1, source_target_pairs={{0,1},{1,0},{2,3},{3,2},{4,5},{5,4},{6,7},{7,6},{8,9},{9,8},{10,11... | collective-permute-start | bytes 1179656 | tf_op jit(solution)/shard_map/ppermute | solution.py:15
  63.6 17.8 %collective-permute-start.11 = (bf16[192,1024]{1,0:T(8,128)(2,1)S(1)}, bf16[192,1024]{1,0:T(8,128)(2,1)S(1)}, u32[]{:S(2)}, u32[]{:S(2)}) collective-permute-start(bf16[192,1024]{1,0:T(8,128)(2,1)S(1)} %collective-permute-done.10.refs_7_), channel_id=1, source_target_pairs={{0,1},{1,0},{2,3},{3,2},{4,5},{5,4},{6,7},{7,6},{8,9},{9,8},{10,11... | collective-permute-start | bytes 1179656 | tf_op jit(solution)/shard_map/ppermute | solution.py:15
  64.2 6.4 %collective-permute-start.4 = (bf16[64,1024]{1,0:T(8,128)(2,1)S(1)}, bf16[64,1024]{1,0:T(8,128)(2,1)S(1)}, u32[]{:S(2)}, u32[]{:S(2)}) collective-permute-start(bf16[64,1024]{1,0:T(8,128)(2,1)S(1)} %get-tuple-element.78.refs_1_), channel_id=1, source_target_pairs={{0,2},{1,3},{2,0},{3,1},{4,6},{5,7},{6,4},{7,5},{8,10},{9,11},{10,... | collective-permute-start | bytes 393224 | tf_op jit(solution)/shard_map/ppermute | solution.py:15
  64.7 12.2 %collective-permute-start.24 = (bf16[128,1024]{1,0:T(8,128)(2,1)S(1)}, bf16[128,1024]{1,0:T(8,128)(2,1)S(1)}, u32[]{:S(2)}, u32[]{:S(2)}) collective-permute-start(bf16[128,1024]{1,0:T(8,128)(2,1)S(1)} %pack.4.refs_1_), channel_id=1, source_target_pairs={{0,2},{1,3},{2,0},{3,1},{4,6},{5,7},{6,4},{7,5},{8,10},{9,11},{10,... | collective-permute-start | bytes 786440 | tf_op jit(solution)/shard_map/ppermute | solution.py:15
  66.3 14.6 %collective-permute-start.34 = (bf16[128,1024]{1,0:T(8,128)(2,1)S(1)}, bf16[128,1024]{1,0:T(8,128)(2,1)S(1)}, u32[]{:S(2)}, u32[]{:S(2)}) collective-permute-start(bf16[128,1024]{1,0:T(8,128)(2,1)S(1)} %pack.5.refs_1_), channel_id=1, source_target_pairs={{0,2},{1,3},{2,0},{3,1},{4,6},{5,7},{6,4},{7,5},{8,10},{9,11},{10,... | collective-permute-start | bytes 786440 | tf_op jit(solution)/shard_map/ppermute | solution.py:15
  70.6 5.7 %collective-permute-start.5 = (bf16[64,1024]{1,0:T(8,128)(2,1)S(1)}, bf16[64,1024]{1,0:T(8,128)(2,1)S(1)}, u32[]{:S(2)}, u32[]{:S(2)}) collective-permute-start(bf16[64,1024]{1,0:T(8,128)(2,1)S(1)} %collective-permute-done.4.refs_3_), channel_id=1, source_target_pairs={{0,1},{1,0},{2,3},{3,2},{4,5},{5,4},{6,7},{7,6},{8,9},{9,8},{10,11... | collective-permute-start | bytes 393224 | tf_op jit(solution)/shard_map/ppermute | solution.py:15
  72.8 8.6 %copy-start = (f32[4096]{0:T(1024)S(1)}, f32[4096]{0:T(1024)}, u32[]{:S(2)}) copy-start(f32[4096]{0:T(1024)} %param.30) | copy-start | bytes 49156
  76.3 9.3 %collective-permute-start.23 = (bf16[128,1024]{1,0:T(8,128)(2,1)S(1)}, bf16[128,1024]{1,0:T(8,128)(2,1)S(1)}, u32[]{:S(2)}, u32[]{:S(2)}) collective-permute-start(bf16[128,1024]{1,0:T(8,128)(2,1)S(1)} %pack.4.refs_1_), channel_id=1, source_target_pairs={{0,1},{1,0},{2,3},{3,2},{4,5},{5,4},{6,7},{7,6},{8,9},{9,8},{10,11... | collective-permute-start | bytes 786440 | tf_op jit(solution)/shard_map/ppermute | solution.py:15
  76.9 12.0 %collective-permute-start.33 = (bf16[128,1024]{1,0:T(8,128)(2,1)S(1)}, bf16[128,1024]{1,0:T(8,128)(2,1)S(1)}, u32[]{:S(2)}, u32[]{:S(2)}) collective-permute-start(bf16[128,1024]{1,0:T(8,128)(2,1)S(1)} %pack.5.refs_1_), channel_id=1, source_target_pairs={{0,1},{1,0},{2,3},{3,2},{4,5},{5,4},{6,7},{7,6},{8,9},{9,8},{10,11... | collective-permute-start | bytes 786440 | tf_op jit(solution)/shard_map/ppermute | solution.py:15
  80.9 5.3 %collective-permute-start.25 = (bf16[128,1024]{1,0:T(8,128)(2,1)S(1)}, bf16[128,1024]{1,0:T(8,128)(2,1)S(1)}, u32[]{:S(2)}, u32[]{:S(2)}) collective-permute-start(bf16[128,1024]{1,0:T(8,128)(2,1)S(1)} %collective-permute-done.24.refs_3_), channel_id=1, source_target_pairs={{0,1},{1,0},{2,3},{3,2},{4,5},{5,4},{6,7},{7,6},{8,9},{9,8},{10,11... | collective-permute-start | bytes 786440 | tf_op jit(solution)/shard_map/ppermute | solution.py:15
  80.9 8.5 %collective-permute-start.35 = (bf16[128,1024]{1,0:T(8,128)(2,1)S(1)}, bf16[128,1024]{1,0:T(8,128)(2,1)S(1)}, u32[]{:S(2)}, u32[]{:S(2)}) collective-permute-start(bf16[128,1024]{1,0:T(8,128)(2,1)S(1)} %collective-permute-done.34.refs_3_), channel_id=1, source_target_pairs={{0,1},{1,0},{2,3},{3,2},{4,5},{5,4},{6,7},{7,6},{8,9},{9,8},{10,11... | collective-permute-start | bytes 786440 | tf_op jit(solution)/shard_map/ppermute | solution.py:15
  85.6 6.5 %collective-permute-start.15 = (bf16[192,1024]{1,0:T(8,128)(2,1)S(1)}, bf16[192,1024]{1,0:T(8,128)(2,1)S(1)}, u32[]{:S(2)}, u32[]{:S(2)}) collective-permute-start(bf16[192,1024]{1,0:T(8,128)(2,1)S(1)} %get-tuple-element.92), channel_id=1, source_target_pairs={{0,1},{1,0},{2,3},{3,2},{4,5},{5,4},{6,7},{7,6},{8,9},{9,8},{10,11... | collective-permute-start | bytes 1179656 | tf_op jit(solution)/shard_map/ppermute | solution.py:15
  85.7 6.9 %collective-permute-start.16 = (bf16[192,1024]{1,0:T(8,128)(2,1)S(1)}, bf16[192,1024]{1,0:T(8,128)(2,1)S(1)}, u32[]{:S(2)}, u32[]{:S(2)}) collective-permute-start(bf16[192,1024]{1,0:T(8,128)(2,1)S(1)} %get-tuple-element.93), channel_id=1, source_target_pairs={{0,1},{1,0},{2,3},{3,2},{4,5},{5,4},{6,7},{7,6},{8,9},{9,8},{10,11... | collective-permute-start | bytes 1179656 | tf_op jit(solution)/shard_map/ppermute | solution.py:15
  88.8 4.5 %collective-permute-start.26 = (bf16[128,1024]{1,0:T(8,128)(2,1)S(1)}, bf16[128,1024]{1,0:T(8,128)(2,1)S(1)}, u32[]{:S(2)}, u32[]{:S(2)}) collective-permute-start(bf16[128,1024]{1,0:T(8,128)(2,1)S(1)} %get-tuple-element.103), channel_id=1, source_target_pairs={{0,1},{1,0},{2,3},{3,2},{4,5},{5,4},{6,7},{7,6},{8,9},{9,8},{10,11... | collective-permute-start | bytes 786440 | tf_op jit(solution)/shard_map/ppermute | solution.py:15
  88.9 4.4 %collective-permute-start.27 = (bf16[128,1024]{1,0:T(8,128)(2,1)S(1)}, bf16[128,1024]{1,0:T(8,128)(2,1)S(1)}, u32[]{:S(2)}, u32[]{:S(2)}) collective-permute-start(bf16[128,1024]{1,0:T(8,128)(2,1)S(1)} %get-tuple-element.104), channel_id=1, source_target_pairs={{0,1},{1,0},{2,3},{3,2},{4,5},{5,4},{6,7},{7,6},{8,9},{9,8},{10,11... | collective-permute-start | bytes 786440 | tf_op jit(solution)/shard_map/ppermute | solution.py:15
  91.9 3.1 %collective-permute-start.36 = (bf16[128,1024]{1,0:T(8,128)(2,1)S(1)}, bf16[128,1024]{1,0:T(8,128)(2,1)S(1)}, u32[]{:S(2)}, u32[]{:S(2)}) collective-permute-start(bf16[128,1024]{1,0:T(8,128)(2,1)S(1)} %get-tuple-element.113), channel_id=1, source_target_pairs={{0,1},{1,0},{2,3},{3,2},{4,5},{5,4},{6,7},{7,6},{8,9},{9,8},{10,11... | collective-permute-start | bytes 786440 | tf_op jit(solution)/shard_map/ppermute | solution.py:15
  92.1 2.9 %collective-permute-start.37 = (bf16[128,1024]{1,0:T(8,128)(2,1)S(1)}, bf16[128,1024]{1,0:T(8,128)(2,1)S(1)}, u32[]{:S(2)}, u32[]{:S(2)}) collective-permute-start(bf16[128,1024]{1,0:T(8,128)(2,1)S(1)} %get-tuple-element.114), channel_id=1, source_target_pairs={{0,1},{1,0},{2,3},{3,2},{4,5},{5,4},{6,7},{7,6},{8,9},{9,8},{10,11... | collective-permute-start | bytes 786440 | tf_op jit(solution)/shard_map/ppermute | solution.py:15
  92.7 25.3 %collective-permute-start.17 = (bf16[192,1024]{1,0:T(8,128)(2,1)S(1)}, bf16[192,1024]{1,0:T(8,128)(2,1)S(1)}, u32[]{:S(2)}, u32[]{:S(2)}) collective-permute-start(bf16[192,1024]{1,0:T(8,128)(2,1)S(1)} %get-tuple-element.95), channel_id=1, source_target_pairs={{0,2},{1,3},{2,0},{3,1},{4,6},{5,7},{6,4},{7,5},{8,10},{9,11},{10,... | collective-permute-start | bytes 1179656 | tf_op jit(solution)/shard_map/ppermute | solution.py:15
  93.4 17.0 %collective-permute-start.28 = (bf16[128,1024]{1,0:T(8,128)(2,1)S(1)}, bf16[128,1024]{1,0:T(8,128)(2,1)S(1)}, u32[]{:S(2)}, u32[]{:S(2)}) collective-permute-start(bf16[128,1024]{1,0:T(8,128)(2,1)S(1)} %get-tuple-element.106), channel_id=1, source_target_pairs={{0,2},{1,3},{2,0},{3,1},{4,6},{5,7},{6,4},{7,5},{8,10},{9,11},{10,... | collective-permute-start | bytes 786440 | tf_op jit(solution)/shard_map/ppermute | solution.py:15
  95.1 20.9 %collective-permute-start.38 = (bf16[128,1024]{1,0:T(8,128)(2,1)S(1)}, bf16[128,1024]{1,0:T(8,128)(2,1)S(1)}, u32[]{:S(2)}, u32[]{:S(2)}) collective-permute-start(bf16[128,1024]{1,0:T(8,128)(2,1)S(1)} %get-tuple-element.116), channel_id=1, source_target_pairs={{0,2},{1,3},{2,0},{3,1},{4,6},{5,7},{6,4},{7,5},{8,10},{9,11},{10,... | collective-permute-start | bytes 786440 | tf_op jit(solution)/shard_map/ppermute | solution.py:15
  95.7 1.3 collective-permute-start.12
  95.7 1.5 %collective-permute-start.13 = (bf16[64,1024]{1,0:T(8,128)(2,1)S(1)}, bf16[64,1024]{1,0:T(8,128)(2,1)S(1)}, u32[]{:S(2)}, u32[]{:S(2)}) collective-permute-start(bf16[64,1024]{1,0:T(8,128)(2,1)S(1)} %get-tuple-element.87), channel_id=1, source_target_pairs={{0,1},{1,0},{2,3},{3,2},{4,5},{5,4},{6,7},{7,6},{8,9},{9,8},{10,11... | collective-permute-start | bytes 393224 | tf_op jit(solution)/shard_map/ppermute | solution.py:15
  97.3 22.6 %collective-permute-start.14 = (bf16[64,1024]{1,0:T(8,128)(2,1)S(1)}, bf16[64,1024]{1,0:T(8,128)(2,1)S(1)}, u32[]{:S(2)}, u32[]{:S(2)}) collective-permute-start(bf16[64,1024]{1,0:T(8,128)(2,1)S(1)} %get-tuple-element.89), channel_id=1, source_target_pairs={{0,2},{1,3},{2,0},{3,1},{4,6},{5,7},{6,4},{7,5},{8,10},{9,11},{10,... | collective-permute-start | bytes 393224 | tf_op jit(solution)/shard_map/ppermute | solution.py:15
  110.4 16.8 %collective-permute-start.29 = (bf16[64,1024]{1,0:T(8,128)(2,1)S(1)}, bf16[64,1024]{1,0:T(8,128)(2,1)S(1)}, u32[]{:S(2)}, u32[]{:S(2)}) collective-permute-start(bf16[64,1024]{1,0:T(8,128)(2,1)S(1)} %get-tuple-element.107), channel_id=1, source_target_pairs={{0,16},{4,20},{8,24},{12,28},{16,0},{20,4},{24,8},{28,12},{1,17},{... | collective-permute-start | bytes 393224 | tf_op jit(solution)/shard_map/ppermute | solution.py:15
  112.1 18.9 %collective-permute-start.30 = (bf16[64,1024]{1,0:T(8,128)(2,1)S(1)}, bf16[64,1024]{1,0:T(8,128)(2,1)S(1)}, u32[]{:S(2)}, u32[]{:S(2)}) collective-permute-start(bf16[64,1024]{1,0:T(8,128)(2,1)S(1)} %get-tuple-element.108), channel_id=1, source_target_pairs={{0,20},{4,16},{8,28},{12,24},{16,4},{20,0},{24,12},{28,8},{1,21},{... | collective-permute-start | bytes 393224 | tf_op jit(solution)/shard_map/ppermute | solution.py:15
  116.1 15.0 %collective-permute-start.39 = (bf16[64,1024]{1,0:T(8,128)(2,1)S(1)}, bf16[64,1024]{1,0:T(8,128)(2,1)S(1)}, u32[]{:S(2)}, u32[]{:S(2)}) collective-permute-start(bf16[64,1024]{1,0:T(8,128)(2,1)S(1)} %get-tuple-element.117), channel_id=1, source_target_pairs={{0,24},{4,28},{8,16},{12,20},{16,8},{20,12},{24,0},{28,4},{1,25},{... | collective-permute-start | bytes 393224 | tf_op jit(solution)/shard_map/ppermute | solution.py:15
  118.0 13.1 %collective-permute-start.40 = (bf16[64,1024]{1,0:T(8,128)(2,1)S(1)}, bf16[64,1024]{1,0:T(8,128)(2,1)S(1)}, u32[]{:S(2)}, u32[]{:S(2)}) collective-permute-start(bf16[64,1024]{1,0:T(8,128)(2,1)S(1)} %get-tuple-element.118), channel_id=1, source_target_pairs={{0,28},{4,24},{8,20},{12,16},{16,12},{20,8},{24,4},{28,0},{1,29},{... | collective-permute-start | bytes 393224 | tf_op jit(solution)/shard_map/ppermute | solution.py:15
  119.9 11.1 %collective-permute-start.18 = (bf16[64,1024]{1,0:T(8,128)(2,1)S(1)}, bf16[64,1024]{1,0:T(8,128)(2,1)S(1)}, u32[]{:S(2)}, u32[]{:S(2)}) collective-permute-start(bf16[64,1024]{1,0:T(8,128)(2,1)S(1)} %get-tuple-element.96), channel_id=1, source_target_pairs={{0,4},{4,0},{8,12},{12,8},{16,20},{20,16},{24,28},{28,24},{1,5},{5... | collective-permute-start | bytes 393224 | tf_op jit(solution)/shard_map/ppermute | solution.py:15
  127.3 5.3 %collective-permute-start.19 = (bf16[64,1024]{1,0:T(8,128)(2,1)S(1)}, bf16[64,1024]{1,0:T(8,128)(2,1)S(1)}, u32[]{:S(2)}, u32[]{:S(2)}) collective-permute-start(bf16[64,1024]{1,0:T(8,128)(2,1)S(1)} %get-tuple-element.97), channel_id=1, source_target_pairs={{0,8},{4,12},{8,0},{12,4},{16,24},{20,28},{24,16},{28,20},{1,9},{5... | collective-permute-start | bytes 393224 | tf_op jit(solution)/shard_map/ppermute | solution.py:15
  131.0 5.9 %collective-permute-start.20 = (bf16[64,1024]{1,0:T(8,128)(2,1)S(1)}, bf16[64,1024]{1,0:T(8,128)(2,1)S(1)}, u32[]{:S(2)}, u32[]{:S(2)}) collective-permute-start(bf16[64,1024]{1,0:T(8,128)(2,1)S(1)} %get-tuple-element.98), channel_id=1, source_target_pairs={{0,12},{4,8},{8,4},{12,0},{16,28},{20,24},{24,20},{28,16},{1,13},{... | collective-permute-start | bytes 393224 | tf_op jit(solution)/shard_map/ppermute | solution.py:15

commit v3 on v2

--- a/solution.py
+++ b/solution.py
@@ -92,9 +92,6 @@
         pow_im.append(2.0 * re * im)
     for i, value in enumerate(pow_re + pow_im):
         powers_ref[i : i + 1, :] = value
-    last = pow_re[-1], pow_im[-1]
-    full_re = last[0] * last[0] - last[1] * last[1]
-    full_im = 2.0 * last[0] * last[1]
 
     shrink = shrink_ref[...]
     summed = shrink
@@ -107,7 +104,7 @@
         offset *= 2
     columns = jnp.transpose(jnp.exp(jnp.concatenate([shrink, summed], axis=0)))
     gone_ref[...] = columns[:, groups:]
-    all_gone = expanded(columns[length - 8 :, groups:], states)[7:8]
+    all_gone = columns[length - 8 :, groups:][7:8]
     flipped = jnp.transpose(signal_ref[...].astype(F32))
     local = bypass_ref[...] * flipped
     flipped = flipped.astype(BF16)
@@ -143,15 +140,16 @@
         xs_re.append(x_re[length - 8 :])
         xs_im.append(x_im[length - 8 :])
     local_ref[...] = local
-    ends = []
-    for value in (
-        full_re * all_gone,
-        full_im * all_gone,
-        jnp.concatenate(xs_re, axis=1)[7:8],
-        jnp.concatenate(xs_im, axis=1)[7:8],
-    ):
-        ends += [value[:, : total // 2], value[:, total // 2 :]]
-    ends = jnp.concatenate(ends, axis=0)
+    spare = summary_ref.shape[2] - 2 * total - groups
+    ends = jnp.concatenate(
+        [
+            jnp.concatenate(xs_re, axis=1)[7:8],
+            jnp.concatenate(xs_im, axis=1)[7:8],
+            all_gone,
+            jnp.zeros((1, spare), F32),
+        ],
+        axis=1,
+    )
     for s in range(summary_ref.shape[0]):
         summary_ref[s] = ends
 
@@ -162,21 +160,23 @@
     groups, lanes, states = emit_re_ref.shape
     length, total = local_ref.shape[0], powers_ref.shape[1]
     mine = mine_ref[0]
-    re = jnp.zeros((2, pieces_ref.shape[2]), F32)
+    bits = powers_ref.shape[0] // 2
+    half_re, half_im = powers_ref[bits - 1 : bits, :], powers_ref[2 * bits - 1 : 2 * bits, :]
+    full_re = half_re * half_re - half_im * half_im
+    full_im = 2.0 * half_re * half_im
+    re = jnp.zeros((1, total), F32)
     im = re
     for s in range(pieces_ref.shape[0] - 1):
         piece = pieces_ref[s]
-        m_re, m_im, a_re, a_im = piece[0:2], piece[2:4], piece[4:6], piece[6:8]
-        new_re = m_re * re - m_im * im + a_re
-        new_im = m_re * im + m_im * re + a_im
+        fade = expanded(piece[:, 2 * total : 2 * total + groups], states)
+        m_re, m_im = full_re * fade, full_im * fade
+        new_re = m_re * re - m_im * im + piece[:, :total]
+        new_im = m_re * im + m_im * re + piece[:, total : 2 * total]
         re = jnp.where(s < mine, new_re, re)
         im = jnp.where(s < mine, new_im, im)
-    re = jnp.concatenate([re[0:1], re[1:2]], axis=1)
-    im = jnp.concatenate([im[0:1], im[1:2]], axis=1)
     emit_re = block_rows(emit_re_ref[...].reshape(groups * lanes, states), groups, lanes)
     emit_im = block_rows(emit_im_ref[...].reshape(groups * lanes, states), groups, lanes)
     value = local_ref[...]
-    bits = powers_ref.shape[0] // 2
     wide = min(128, total)
     each = wide // states
     near = lax.broadcasted_iota(jnp.int32, (8, wide), 0) + 1
@@ -267,7 +267,7 @@
         in_specs=hbm(10),
         out_specs=vmem(6),
         out_shape=[
-            jax.ShapeDtypeStruct((count, 8, total // 2), F32),
+            jax.ShapeDtypeStruct((count, 1, 2 * total + 128), F32),
             jax.ShapeDtypeStruct((length, channels), F32),
             jax.ShapeDtypeStruct((2 * bits, total), F32),
             jax.ShapeDtypeStruct((length, groups), F32),

time: 138 us -> 138 us (level)
  no operation moved by 1% of the time
where the time goes in v3:
time: 138 us; the launch traced here: 137 us
  waiting for transfers between devices  61.5 us (45%)
  starting transfers between devices  33.9 us (25%)
  Pallas kernels  28.1 us (20%)
  blocking collectives  13.5 us (10%)
    ppermute x41, waiting for transfers between devices, swap(): return lax.ppermute(value, axis, [(i, i ^ bits) for i in range(count)])  61.5 us
    ppermute x41, starting transfers between devices, swap(): return lax.ppermute(value, axis, [(i, i ^ bits) for i in range(count)])  33.9 us
    all_to_all x1, blocking collectives, mixer(): pieces = lax.all_to_all(summary, 'sp', 0, 0, tiled=True)  13.5 us
    pallas_call x3, Pallas kernels, ffn(): pl.pallas_call(lambda *refs: ffn_kernel(n_tp, groups, width, *refs), in_s...  9.35 us
    pallas_call x2, Pallas kernels, load(): pl.pallas_call(load_kernel, in_specs=hbm(len(weights)), out_specs=vmem(le...  5.69 us
    pallas_call x1, Pallas kernels, mixer(): pl.pallas_call(first_kernel, in_specs=hbm(10), out_specs=vmem(6), out_sha...  4.87 us
  transfers between devices with their start and end apart: 41, of which 17 were waited for; matrix products, arithmetic and copies ran while one was open for 0% of the time, Pallas kernels for 17%

profile of v3, /device:TPU:0, one launch (start us, length us, event | category | flops | bytes accessed | tf_op | source)
XLA Modules:
  0.0 137.3 jit_solution(11304345583046086031)
XLA Ops:
  0.1 2.2 %cut_blocks.1 = (bf16[256,1024]{1,0:T(8,128)(2,1)S(1)}, bf16[256,1024]{1,0:T(8,128)(2,1)S(1)}, bf16[256,2048]{1,0:T(8,128)(2,1)S(1)}, bf16[128,1024]{1,0:T(8,128)(2,1)S(1)}) custom-call(s32[2]{0:T(128)S(1)} %pad_add_fusion.mine_ref.refs_0_, bf16[256,4096]{1,0:T(8,128)(2,1)} %refs_1_.3, bf16[128,4096]{1,0:T(8,128)(2,1)} %refs_2_.3), custom_call_target="tpu_custom_call" | custom-call | tf_op jit(solution)/shard_map/cut_blocks/pallas_call | solution.py:322
  2.3 0.6 collective-permute-start.1
  2.8 4.9 %mixer_scan.1 = (f32[8,1,2176]{2,1,0:T(1,128)S(1)}, f32[128,256]{1,0:T(8,128)S(1)}, f32[14,1024]{1,0:T(8,128)S(1)}, f32[128,16]{1,0:T(8,128)S(1)}, f32[16,16,64]{2,1,0:T(8,128)S(1)}, /*index=5*/f32[16,16,64]{2,1,0:T(8,128)S(1)}) custom-call(bf16[256,128]{1,0:T(8,128)(2,1)} %refs_0_.1, f32[16,64]{1,0:T(8,128)} %refs_1_.2, f32[16,64]{1,0:T(8,128)} %refs_2_.2, ...), custom_call_target="tpu_custom_call" | custom-call | tf_op jit(solution)/shard_map/mixer_scan/pallas_call | solution.py:265
  7.7 13.5 %all_to_all.5.pieces_ref = f32[8,1,2176]{2,1,0:T(1,128)S(1)} all-to-all(f32[8,1,2176]{2,1,0:T(1,128)S(1)} %get-tuple-element.62), channel_id=1, replica_groups=mesh['sp'=8,'tp'=4] {'sp'}, dimensions={0} | all-to-all | bytes 139264 | tf_op jit(solution)/shard_map/all_to_all | solution.py:282
  21.2 1.4 %mixer_readout.1.mixed_ref = bf16[128,256]{1,0:T(8,128)(2,1)S(1)} custom-call(s32[2]{0:T(128)S(1)} %pad_add_fusion.mine_ref.refs_0_, f32[8,1,2176]{2,1,0:T(1,128)S(1)} %all_to_all.5.pieces_ref, f32[128,256]{1,0:T(8,128)S(1)} %get-tuple-element.63.local_ref, f32[14,1024]{1,0:T(8,128)S(1)} %get-tuple-element.64.powers_ref, ...), custom_call_target="tpu_custom_call" | custom-call | tf_op jit(solution)/shard_map/mixer_readout/pallas_call | solution.py:283
  22.7 1.2 collective-permute-done.other_ref
  24.4 1.6 %collective-permute-start.2 = (bf16[128,1024]{1,0:T(8,128)(2,1)S(1)}, bf16[128,1024]{1,0:T(8,128)(2,1)S(1)}, u32[]{:S(2)}, u32[]{:S(2)}) collective-permute-start(bf16[128,1024]{1,0:T(8,128)(2,1)S(1)} %get-tuple-element.72), channel_id=1, source_target_pairs={{0,2},{1,3},{2,0},{3,1},{4,6},{5,7},{6,4},{7,5},{8,10},{9,11},{10,... | collective-permute-start | bytes 786440 | tf_op jit(solution)/shard_map/ppermute | solution.py:15
  26.0 1.8 %route.1 = (bf16[512,128]{1,0:T(8,128)(2,1)S(1)}, bf16[128,512]{1,0:T(8,128)(2,1)S(1)}, bf16[128,512]{1,0:T(8,128)(2,1)S(1)}) custom-call(s32[2]{0:T(128)S(1)} %pad_add_fusion.mine_ref.refs_0_, s32[2,128]{1,0:T(2,128)} %bitcast.21, f32[2,128]{1,0:T(2,128)} %bitcast.22), custom_call_target="tpu_custom_call" | custom-call | tf_op jit(solution)/shard_map/route/pallas_call | solution.py:406
  27.8 5.1 %collective-permute-done.2.refs_1_ = bf16[128,1024]{1,0:T(8,128)(2,1)S(1)} collective-permute-done((bf16[128,1024]{1,0:T(8,128)(2,1)S(1)}, bf16[128,1024]{1,0:T(8,128)(2,1)S(1)}, u32[]{:S(2)}, u32[]{:S(2)}) %collective-permute-start.2) | collective-permute-done | bytes 262176 | tf_op jit(solution)/shard_map/ppermute | solution.py:15
  33.8 0.8 collective-permute-start.7
  34.6 2.3 %collective-permute-start.8 = (bf16[64,1024]{1,0:T(8,128)(2,1)S(1)}, bf16[64,1024]{1,0:T(8,128)(2,1)S(1)}, u32[]{:S(2)}, u32[]{:S(2)}) collective-permute-start(bf16[64,1024]{1,0:T(8,128)(2,1)S(1)} %get-tuple-element.81), channel_id=1, source_target_pairs={{0,12},{4,8},{8,4},{12,0},{16,28},{20,24},{24,20},{28,16},{1,13},{... | collective-permute-start | bytes 393224 | tf_op jit(solution)/shard_map/ppermute | solution.py:15
  36.9 2.5 %collective-permute-done.6.refs_0_ = bf16[64,1024]{1,0:T(8,128)(2,1)S(1)} collective-permute-done((bf16[64,1024]{1,0:T(8,128)(2,1)S(1)}, bf16[64,1024]{1,0:T(8,128)(2,1)S(1)}, u32[]{:S(2)}, u32[]{:S(2)}) %collective-permute-start.6) | collective-permute-done | bytes 131104 | tf_op jit(solution)/shard_map/ppermute | solution.py:15
  39.6 2.5 %collective-permute-done.8.refs_2_ = bf16[64,1024]{1,0:T(8,128)(2,1)S(1)} collective-permute-done((bf16[64,1024]{1,0:T(8,128)(2,1)S(1)}, bf16[64,1024]{1,0:T(8,128)(2,1)S(1)}, u32[]{:S(2)}, u32[]{:S(2)}) %collective-permute-start.8) | collective-permute-done | bytes 131104 | tf_op jit(solution)/shard_map/ppermute | solution.py:15
  42.1 1.6 %collective-permute-start.10 = (bf16[192,1024]{1,0:T(8,128)(2,1)S(1)}, bf16[192,1024]{1,0:T(8,128)(2,1)S(1)}, u32[]{:S(2)}, u32[]{:S(2)}) collective-permute-start(bf16[192,1024]{1,0:T(8,128)(2,1)S(1)} %pack.3.refs_5_), channel_id=1, source_target_pairs={{0,2},{1,3},{2,0},{3,1},{4,6},{5,7},{6,4},{7,5},{8,10},{9,11},{10,... | collective-permute-start | bytes 1179656 | tf_op jit(solution)/shard_map/ppermute | solution.py:15
  44.2 2.3 %collective-permute-start.22 = (bf16[64,1024]{1,0:T(8,128)(2,1)S(1)}, bf16[64,1024]{1,0:T(8,128)(2,1)S(1)}, u32[]{:S(2)}, u32[]{:S(2)}) collective-permute-start(bf16[64,1024]{1,0:T(8,128)(2,1)S(1)} %get-tuple-element.100), channel_id=1, source_target_pairs={{0,20},{4,16},{8,28},{12,24},{16,4},{20,0},{24,12},{28,8},{1,21},{... | collective-permute-start | bytes 393224 | tf_op jit(solution)/shard_map/ppermute | solution.py:15
  46.5 1.3 collective-permute-start.31
  47.8 3.6 %collective-permute-start.32 = (bf16[64,1024]{1,0:T(8,128)(2,1)S(1)}, bf16[64,1024]{1,0:T(8,128)(2,1)S(1)}, u32[]{:S(2)}, u32[]{:S(2)}) collective-permute-start(bf16[64,1024]{1,0:T(8,128)(2,1)S(1)} %get-tuple-element.110), channel_id=1, source_target_pairs={{0,28},{4,24},{8,20},{12,16},{16,12},{20,8},{24,4},{28,0},{1,29},{... | collective-permute-start | bytes 393224 | tf_op jit(solution)/shard_map/ppermute | solution.py:15
  51.4 7.7 %collective-permute-done.21.refs_0_ = bf16[64,1024]{1,0:T(8,128)(2,1)S(1)} collective-permute-done((bf16[64,1024]{1,0:T(8,128)(2,1)S(1)}, bf16[64,1024]{1,0:T(8,128)(2,1)S(1)}, u32[]{:S(2)}, u32[]{:S(2)}) %collective-permute-start.21) | collective-permute-done | bytes 131104 | tf_op jit(solution)/shard_map/ppermute | solution.py:15
  59.1 4.2 %collective-permute-done.22.refs_1_ = bf16[64,1024]{1,0:T(8,128)(2,1)S(1)} collective-permute-done((bf16[64,1024]{1,0:T(8,128)(2,1)S(1)}, bf16[64,1024]{1,0:T(8,128)(2,1)S(1)}, u32[]{:S(2)}, u32[]{:S(2)}) %collective-permute-start.22) | collective-permute-done | bytes 131104 | tf_op jit(solution)/shard_map/ppermute | solution.py:15
  63.3 0.5 collective-permute-start.11
  63.8 0.6 collective-permute-start.4
  64.4 1.5 %collective-permute-start.24 = (bf16[128,1024]{1,0:T(8,128)(2,1)S(1)}, bf16[128,1024]{1,0:T(8,128)(2,1)S(1)}, u32[]{:S(2)}, u32[]{:S(2)}) collective-permute-start(bf16[128,1024]{1,0:T(8,128)(2,1)S(1)} %pack.4.refs_1_), channel_id=1, source_target_pairs={{0,2},{1,3},{2,0},{3,1},{4,6},{5,7},{6,4},{7,5},{8,10},{9,11},{10,... | collective-permute-start | bytes 786440 | tf_op jit(solution)/shard_map/ppermute | solution.py:15
  65.9 0.6 collective-permute-start.34
  66.5 3.7 %collective-permute-done.4.refs_3_ = bf16[64,1024]{1,0:T(8,128)(2,1)S(1)} collective-permute-done((bf16[64,1024]{1,0:T(8,128)(2,1)S(1)}, bf16[64,1024]{1,0:T(8,128)(2,1)S(1)}, u32[]{:S(2)}, u32[]{:S(2)}) %collective-permute-start.4) | collective-permute-done | bytes 131104 | tf_op jit(solution)/shard_map/ppermute | solution.py:15
  70.3 2.2 %load.3.refs_12_.refs_8_ = bf16[512,4096]{1,0:T(8,128)(2,1)S(1)} custom-call(bf16[512,4096]{1,0:T(8,128)(2,1)} %bitcast.15), custom_call_target="tpu_custom_call" | custom-call | tf_op jit(solution)/shard_map/load/pallas_call | solution.py:548
  72.5 3.5 %load.2 = (bf16[4096,512]{1,0:T(8,128)(2,1)S(1)}, bf16[4096,512]{1,0:T(8,128)(2,1)S(1)}) custom-call(bf16[4096,512]{1,0:T(8,128)(2,1)} %bitcast.16, bf16[4096,512]{1,0:T(8,128)(2,1)} %bitcast.17), custom_call_target="tpu_custom_call" | custom-call | tf_op jit(solution)/shard_map/load/pallas_call | solution.py:548
  76.0 0.6 collective-permute-start.23
  76.6 3.9 %collective-permute-done.34.refs_3_ = bf16[128,1024]{1,0:T(8,128)(2,1)S(1)} collective-permute-done((bf16[128,1024]{1,0:T(8,128)(2,1)S(1)}, bf16[128,1024]{1,0:T(8,128)(2,1)S(1)}, u32[]{:S(2)}, u32[]{:S(2)}) %collective-permute-start.34) | collective-permute-done | bytes 262176 | tf_op jit(solution)/shard_map/ppermute | solution.py:15
  81.0 4.2 %expert_ffn.3 = (bf16[64,1024]{1,0:T(8,128)(2,1)S(1)}, bf16[64,1024]{1,0:T(8,128)(2,1)S(1)}, bf16[64,1024]{1,0:T(8,128)(2,1)S(1)}, bf16[64,1024]{1,0:T(8,128)(2,...) custom-call(s32[2]{0:T(128)S(1)} %pad_add_fusion.mine_ref.refs_0_, ...), custom_call_target="tpu_custom_call" | custom-call | flops 3221225472 | bytes 16777216 | tf_op jit(solution)/shard_map/expert_ffn/pallas_call | solution.py:564
  85.8 2.6 %expert_ffn.4 = (bf16[128,1024]{1,0:T(8,128)(2,1)S(1)}, bf16[128,1024]{1,0:T(8,128)(2,1)S(1)}, bf16[128,1024]{1,0:T(8,128)(2,1)S(1)}, bf16[128,1024]{1,0:T(8,128)(2,1)S(1)}) custom-call(s32[2]{0:T(128)S(1)} %pad_add_fusion.mine_ref.refs_0_, bf16[128,1024]{1,0:T(8,128)(2,1)S(1)} %pack.4.refs_1_, bf16[128,1024]{1,0:T(8,128)(2,1)S(1)} %collective-permute-done.23.refs_2_, ...), custom_call_target="tpu_custom_call" | custom-call | flops 1610612736 | bytes 14680064 | tf_op jit(solution)/shard_map/expert_ffn/pallas_call | solution.py:564
  89.0 2.6 %expert_ffn.5 = (bf16[128,1024]{1,0:T(8,128)(2,1)S(1)}, bf16[128,1024]{1,0:T(8,128)(2,1)S(1)}, bf16[128,1024]{1,0:T(8,128)(2,1)S(1)}, bf16[128,1024]{1,0:T(8,128)(2,1)S(1)}) custom-call(s32[2]{0:T(128)S(1)} %pad_add_fusion.mine_ref.refs_0_, bf16[128,1024]{1,0:T(8,128)(2,1)S(1)} %pack.5.refs_1_, bf16[128,1024]{1,0:T(8,128)(2,1)S(1)} %collective-permute-done.33.refs_2_, ...), custom_call_target="tpu_custom_call" | custom-call | flops 1610612736 | bytes 14680064 | tf_op jit(solution)/shard_map/expert_ffn/pallas_call | solution.py:564
  92.4 0.6 collective-permute-start.17
  93.1 1.6 %collective-permute-start.28 = (bf16[128,1024]{1,0:T(8,128)(2,1)S(1)}, bf16[128,1024]{1,0:T(8,128)(2,1)S(1)}, u32[]{:S(2)}, u32[]{:S(2)}) collective-permute-start(bf16[128,1024]{1,0:T(8,128)(2,1)S(1)} %get-tuple-element.106), channel_id=1, source_target_pairs={{0,2},{1,3},{2,0},{3,1},{4,6},{5,7},{6,4},{7,5},{8,10},{9,11},{10,... | collective-permute-start | bytes 786440 | tf_op jit(solution)/shard_map/ppermute | solution.py:15
  94.8 0.6 collective-permute-start.38
  95.9 0.8 collective-permute-done.12.refs_2_
  97.0 1.6 %collective-permute-start.14 = (bf16[64,1024]{1,0:T(8,128)(2,1)S(1)}, bf16[64,1024]{1,0:T(8,128)(2,1)S(1)}, u32[]{:S(2)}, u32[]{:S(2)}) collective-permute-start(bf16[64,1024]{1,0:T(8,128)(2,1)S(1)} %get-tuple-element.89), channel_id=1, source_target_pairs={{0,2},{1,3},{2,0},{3,1},{4,6},{5,7},{6,4},{7,5},{8,10},{9,11},{10,... | collective-permute-start | bytes 393224 | tf_op jit(solution)/shard_map/ppermute | solution.py:15
  98.5 11.5 %collective-permute-done.28.refs_1_ = bf16[128,1024]{1,0:T(8,128)(2,1)S(1)} collective-permute-done((bf16[128,1024]{1,0:T(8,128)(2,1)S(1)}, bf16[128,1024]{1,0:T(8,128)(2,1)S(1)}, u32[]{:S(2)}, u32[]{:S(2)}) %collective-permute-start.28) | collective-permute-done | bytes 262176 | tf_op jit(solution)/shard_map/ppermute | solution.py:15
  110.1 1.0 collective-permute-start.29
  111.1 1.5 %collective-permute-start.30 = (bf16[64,1024]{1,0:T(8,128)(2,1)S(1)}, bf16[64,1024]{1,0:T(8,128)(2,1)S(1)}, u32[]{:S(2)}, u32[]{:S(2)}) collective-permute-start(bf16[64,1024]{1,0:T(8,128)(2,1)S(1)} %get-tuple-element.108), channel_id=1, source_target_pairs={{0,20},{4,16},{8,28},{12,24},{16,4},{20,0},{24,12},{28,8},{1,21},{... | collective-permute-start | bytes 393224 | tf_op jit(solution)/shard_map/ppermute | solution.py:15
  112.6 3.0 %collective-permute-done.38.refs_1_ = bf16[128,1024]{1,0:T(8,128)(2,1)S(1)} collective-permute-done((bf16[128,1024]{1,0:T(8,128)(2,1)S(1)}, bf16[128,1024]{1,0:T(8,128)(2,1)S(1)}, u32[]{:S(2)}, u32[]{:S(2)}) %collective-permute-start.38) | collective-permute-done | bytes 262176 | tf_op jit(solution)/shard_map/ppermute | solution.py:15
  115.7 1.6 %collective-permute-start.39 = (bf16[64,1024]{1,0:T(8,128)(2,1)S(1)}, bf16[64,1024]{1,0:T(8,128)(2,1)S(1)}, u32[]{:S(2)}, u32[]{:S(2)}) collective-permute-start(bf16[64,1024]{1,0:T(8,128)(2,1)S(1)} %get-tuple-element.117), channel_id=1, source_target_pairs={{0,24},{4,28},{8,16},{12,20},{16,8},{20,12},{24,0},{28,4},{1,25},{... | collective-permute-start | bytes 393224 | tf_op jit(solution)/shard_map/ppermute | solution.py:15
  117.3 1.9 %collective-permute-start.40 = (bf16[64,1024]{1,0:T(8,128)(2,1)S(1)}, bf16[64,1024]{1,0:T(8,128)(2,1)S(1)}, u32[]{:S(2)}, u32[]{:S(2)}) collective-permute-start(bf16[64,1024]{1,0:T(8,128)(2,1)S(1)} %get-tuple-element.118), channel_id=1, source_target_pairs={{0,28},{4,24},{8,20},{12,16},{16,12},{20,8},{24,4},{28,0},{1,29},{... | collective-permute-start | bytes 393224 | tf_op jit(solution)/shard_map/ppermute | solution.py:15
  119.2 2.0 %collective-permute-start.18 = (bf16[64,1024]{1,0:T(8,128)(2,1)S(1)}, bf16[64,1024]{1,0:T(8,128)(2,1)S(1)}, u32[]{:S(2)}, u32[]{:S(2)}) collective-permute-start(bf16[64,1024]{1,0:T(8,128)(2,1)S(1)} %get-tuple-element.96), channel_id=1, source_target_pairs={{0,4},{4,0},{8,12},{12,8},{16,20},{20,16},{24,28},{28,24},{1,5},{5... | collective-permute-start | bytes 393224 | tf_op jit(solution)/shard_map/ppermute | solution.py:15
  121.2 4.9 %collective-permute-done.29.refs_4_ = bf16[64,1024]{1,0:T(8,128)(2,1)S(1)} collective-permute-done((bf16[64,1024]{1,0:T(8,128)(2,1)S(1)}, bf16[64,1024]{1,0:T(8,128)(2,1)S(1)}, u32[]{:S(2)}, u32[]{:S(2)}) %collective-permute-start.29) | collective-permute-done | bytes 131104 | tf_op jit(solution)/shard_map/ppermute | solution.py:15
  126.2 4.1 %collective-permute-done.30.refs_5_ = bf16[64,1024]{1,0:T(8,128)(2,1)S(1)} collective-permute-done((bf16[64,1024]{1,0:T(8,128)(2,1)S(1)}, bf16[64,1024]{1,0:T(8,128)(2,1)S(1)}, u32[]{:S(2)}, u32[]{:S(2)}) %collective-permute-start.30) | collective-permute-done | bytes 131104 | tf_op jit(solution)/shard_map/ppermute | solution.py:15
  130.4 1.3 collective-permute-done.19.refs_2_
  131.7 4.5 %collective-permute-done.20.refs_3_ = bf16[64,1024]{1,0:T(8,128)(2,1)S(1)} collective-permute-done((bf16[64,1024]{1,0:T(8,128)(2,1)S(1)}, bf16[64,1024]{1,0:T(8,128)(2,1)S(1)}, u32[]{:S(2)}, u32[]{:S(2)}) %collective-permute-start.20) | collective-permute-done | bytes 131104 | tf_op jit(solution)/shard_map/ppermute | solution.py:15
  136.2 1.2 combine.1
  (61 shorter events, 6.1 us)
Async XLA Ops:
  2.3 21.7 %collective-permute-start.1 = (bf16[256,2048]{1,0:T(8,128)(2,1)S(1)}, bf16[256,2048]{1,0:T(8,128)(2,1)S(1)}, u32[]{:S(2)}, u32[]{:S(2)}) collective-permute-start(bf16[256,2048]{1,0:T(8,128)(2,1)S(1)} %get-tuple-element.68), channel_id=1, source_target_pairs={{0,1},{1,0},{2,3},{3,2},{4,5},{5,4},{6,7},{7,6},{8,9},{9,8},{10,11... | collective-permute-start | bytes 3145736 | tf_op jit(solution)/shard_map/ppermute | solution.py:15
  22.7 1.3 collective-permute-start
  24.4 8.4 %collective-permute-start.2 = (bf16[128,1024]{1,0:T(8,128)(2,1)S(1)}, bf16[128,1024]{1,0:T(8,128)(2,1)S(1)}, u32[]{:S(2)}, u32[]{:S(2)}) collective-permute-start(bf16[128,1024]{1,0:T(8,128)(2,1)S(1)} %get-tuple-element.72), channel_id=1, source_target_pairs={{0,2},{1,3},{2,0},{3,1},{4,6},{5,7},{6,4},{7,5},{8,10},{9,11},{10,... | collective-permute-start | bytes 786440 | tf_op jit(solution)/shard_map/ppermute | solution.py:15
  33.3 6.1 %collective-permute-start.6 = (bf16[64,1024]{1,0:T(8,128)(2,1)S(1)}, bf16[64,1024]{1,0:T(8,128)(2,1)S(1)}, u32[]{:S(2)}, u32[]{:S(2)}) collective-permute-start(bf16[64,1024]{1,0:T(8,128)(2,1)S(1)} %get-tuple-element.79), channel_id=1, source_target_pairs={{0,4},{4,0},{8,12},{12,8},{16,20},{20,16},{24,28},{28,24},{1,5},{5... | collective-permute-start | bytes 393224 | tf_op jit(solution)/shard_map/ppermute | solution.py:15
  33.8 5.8 %collective-permute-start.7 = (bf16[64,1024]{1,0:T(8,128)(2,1)S(1)}, bf16[64,1024]{1,0:T(8,128)(2,1)S(1)}, u32[]{:S(2)}, u32[]{:S(2)}) collective-permute-start(bf16[64,1024]{1,0:T(8,128)(2,1)S(1)} %get-tuple-element.80), channel_id=1, source_target_pairs={{0,8},{4,12},{8,0},{12,4},{16,24},{20,28},{24,16},{28,20},{1,9},{5... | collective-permute-start | bytes 393224 | tf_op jit(solution)/shard_map/ppermute | solution.py:15
  34.6 7.5 %collective-permute-start.8 = (bf16[64,1024]{1,0:T(8,128)(2,1)S(1)}, bf16[64,1024]{1,0:T(8,128)(2,1)S(1)}, u32[]{:S(2)}, u32[]{:S(2)}) collective-permute-start(bf16[64,1024]{1,0:T(8,128)(2,1)S(1)} %get-tuple-element.81), channel_id=1, source_target_pairs={{0,12},{4,8},{8,4},{12,0},{16,28},{20,24},{24,20},{28,16},{1,13},{... | collective-permute-start | bytes 393224 | tf_op jit(solution)/shard_map/ppermute | solution.py:15
  42.1 21.1 %collective-permute-start.10 = (bf16[192,1024]{1,0:T(8,128)(2,1)S(1)}, bf16[192,1024]{1,0:T(8,128)(2,1)S(1)}, u32[]{:S(2)}, u32[]{:S(2)}) collective-permute-start(bf16[192,1024]{1,0:T(8,128)(2,1)S(1)} %pack.3.refs_5_), channel_id=1, source_target_pairs={{0,2},{1,3},{2,0},{3,1},{4,6},{5,7},{6,4},{7,5},{8,10},{9,11},{10,... | collective-permute-start | bytes 1179656 | tf_op jit(solution)/shard_map/ppermute | solution.py:15
  43.7 15.4 %collective-permute-start.21 = (bf16[64,1024]{1,0:T(8,128)(2,1)S(1)}, bf16[64,1024]{1,0:T(8,128)(2,1)S(1)}, u32[]{:S(2)}, u32[]{:S(2)}) collective-permute-start(bf16[64,1024]{1,0:T(8,128)(2,1)S(1)} %get-tuple-element.99), channel_id=1, source_target_pairs={{0,16},{4,20},{8,24},{12,28},{16,0},{20,4},{24,8},{28,12},{1,17},{... | collective-permute-start | bytes 393224 | tf_op jit(solution)/shard_map/ppermute | solution.py:15
  44.2 19.1 %collective-permute-start.22 = (bf16[64,1024]{1,0:T(8,128)(2,1)S(1)}, bf16[64,1024]{1,0:T(8,128)(2,1)S(1)}, u32[]{:S(2)}, u32[]{:S(2)}) collective-permute-start(bf16[64,1024]{1,0:T(8,128)(2,1)S(1)} %get-tuple-element.100), channel_id=1, source_target_pairs={{0,20},{4,16},{8,28},{12,24},{16,4},{20,0},{24,12},{28,8},{1,21},{... | collective-permute-start | bytes 393224 | tf_op jit(solution)/shard_map/ppermute | solution.py:15
  46.5 17.3 %collective-permute-start.31 = (bf16[64,1024]{1,0:T(8,128)(2,1)S(1)}, bf16[64,1024]{1,0:T(8,128)(2,1)S(1)}, u32[]{:S(2)}, u32[]{:S(2)}) collective-permute-start(bf16[64,1024]{1,0:T(8,128)(2,1)S(1)} %get-tuple-element.109), channel_id=1, source_target_pairs={{0,24},{4,28},{8,16},{12,20},{16,8},{20,12},{24,0},{28,4},{1,25},{... | collective-permute-start | bytes 393224 | tf_op jit(solution)/shard_map/ppermute | solution.py:15
  47.8 16.6 %collective-permute-start.32 = (bf16[64,1024]{1,0:T(8,128)(2,1)S(1)}, bf16[64,1024]{1,0:T(8,128)(2,1)S(1)}, u32[]{:S(2)}, u32[]{:S(2)}) collective-permute-start(bf16[64,1024]{1,0:T(8,128)(2,1)S(1)} %get-tuple-element.110), channel_id=1, source_target_pairs={{0,28},{4,24},{8,20},{12,16},{16,12},{20,8},{24,4},{28,0},{1,29},{... | collective-permute-start | bytes 393224 | tf_op jit(solution)/shard_map/ppermute | solution.py:15
  59.1 6.8 %collective-permute-start.3 = (bf16[64,1024]{1,0:T(8,128)(2,1)S(1)}, bf16[64,1024]{1,0:T(8,128)(2,1)S(1)}, u32[]{:S(2)}, u32[]{:S(2)}) collective-permute-start(bf16[64,1024]{1,0:T(8,128)(2,1)S(1)} %get-tuple-element.78.refs_1_), channel_id=1, source_target_pairs={{0,1},{1,0},{2,3},{3,2},{4,5},{5,4},{6,7},{7,6},{8,9},{9,8},{10,11... | collective-permute-start | bytes 393224 | tf_op jit(solution)/shard_map/ppermute | solution.py:15
  63.3 17.3 %collective-permute-start.9 = (bf16[192,1024]{1,0:T(8,128)(2,1)S(1)}, bf16[192,1024]{1,0:T(8,128)(2,1)S(1)}, u32[]{:S(2)}, u32[]{:S(2)}) collective-permute-start(bf16[192,1024]{1,0:T(8,128)(2,1)S(1)} %pack.3.refs_5_), channel_id=1, source_target_pairs={{0,1},{1,0},{2,3},{3,2},{4,5},{5,4},{6,7},{7,6},{8,9},{9,8},{10,11... | collective-permute-start | bytes 1179656 | tf_op jit(solution)/shard_map/ppermute | solution.py:15
  63.3 17.8 %collective-permute-start.11 = (bf16[192,1024]{1,0:T(8,128)(2,1)S(1)}, bf16[192,1024]{1,0:T(8,128)(2,1)S(1)}, u32[]{:S(2)}, u32[]{:S(2)}) collective-permute-start(bf16[192,1024]{1,0:T(8,128)(2,1)S(1)} %collective-permute-done.10.refs_7_), channel_id=1, source_target_pairs={{0,1},{1,0},{2,3},{3,2},{4,5},{5,4},{6,7},{7,6},{8,9},{9,8},{10,11... | collective-permute-start | bytes 1179656 | tf_op jit(solution)/shard_map/ppermute | solution.py:15
  63.8 6.4 %collective-permute-start.4 = (bf16[64,1024]{1,0:T(8,128)(2,1)S(1)}, bf16[64,1024]{1,0:T(8,128)(2,1)S(1)}, u32[]{:S(2)}, u32[]{:S(2)}) collective-permute-start(bf16[64,1024]{1,0:T(8,128)(2,1)S(1)} %get-tuple-element.78.refs_1_), channel_id=1, source_target_pairs={{0,2},{1,3},{2,0},{3,1},{4,6},{5,7},{6,4},{7,5},{8,10},{9,11},{10,... | collective-permute-start | bytes 393224 | tf_op jit(solution)/shard_map/ppermute | solution.py:15
  64.4 12.2 %collective-permute-start.24 = (bf16[128,1024]{1,0:T(8,128)(2,1)S(1)}, bf16[128,1024]{1,0:T(8,128)(2,1)S(1)}, u32[]{:S(2)}, u32[]{:S(2)}) collective-permute-start(bf16[128,1024]{1,0:T(8,128)(2,1)S(1)} %pack.4.refs_1_), channel_id=1, source_target_pairs={{0,2},{1,3},{2,0},{3,1},{4,6},{5,7},{6,4},{7,5},{8,10},{9,11},{10,... | collective-permute-start | bytes 786440 | tf_op jit(solution)/shard_map/ppermute | solution.py:15
  65.9 14.6 %collective-permute-start.34 = (bf16[128,1024]{1,0:T(8,128)(2,1)S(1)}, bf16[128,1024]{1,0:T(8,128)(2,1)S(1)}, u32[]{:S(2)}, u32[]{:S(2)}) collective-permute-start(bf16[128,1024]{1,0:T(8,128)(2,1)S(1)} %pack.5.refs_1_), channel_id=1, source_target_pairs={{0,2},{1,3},{2,0},{3,1},{4,6},{5,7},{6,4},{7,5},{8,10},{9,11},{10,... | collective-permute-start | bytes 786440 | tf_op jit(solution)/shard_map/ppermute | solution.py:15
  70.3 5.7 %collective-permute-start.5 = (bf16[64,1024]{1,0:T(8,128)(2,1)S(1)}, bf16[64,1024]{1,0:T(8,128)(2,1)S(1)}, u32[]{:S(2)}, u32[]{:S(2)}) collective-permute-start(bf16[64,1024]{1,0:T(8,128)(2,1)S(1)} %collective-permute-done.4.refs_3_), channel_id=1, source_target_pairs={{0,1},{1,0},{2,3},{3,2},{4,5},{5,4},{6,7},{7,6},{8,9},{9,8},{10,11... | collective-permute-start | bytes 393224 | tf_op jit(solution)/shard_map/ppermute | solution.py:15
  72.5 8.6 %copy-start = (f32[4096]{0:T(1024)S(1)}, f32[4096]{0:T(1024)}, u32[]{:S(2)}) copy-start(f32[4096]{0:T(1024)} %param.30) | copy-start | bytes 49156
  76.0 9.3 %collective-permute-start.23 = (bf16[128,1024]{1,0:T(8,128)(2,1)S(1)}, bf16[128,1024]{1,0:T(8,128)(2,1)S(1)}, u32[]{:S(2)}, u32[]{:S(2)}) collective-permute-start(bf16[128,1024]{1,0:T(8,128)(2,1)S(1)} %pack.4.refs_1_), channel_id=1, source_target_pairs={{0,1},{1,0},{2,3},{3,2},{4,5},{5,4},{6,7},{7,6},{8,9},{9,8},{10,11... | collective-permute-start | bytes 786440 | tf_op jit(solution)/shard_map/ppermute | solution.py:15
  76.6 12.0 %collective-permute-start.33 = (bf16[128,1024]{1,0:T(8,128)(2,1)S(1)}, bf16[128,1024]{1,0:T(8,128)(2,1)S(1)}, u32[]{:S(2)}, u32[]{:S(2)}) collective-permute-start(bf16[128,1024]{1,0:T(8,128)(2,1)S(1)} %pack.5.refs_1_), channel_id=1, source_target_pairs={{0,1},{1,0},{2,3},{3,2},{4,5},{5,4},{6,7},{7,6},{8,9},{9,8},{10,11... | collective-permute-start | bytes 786440 | tf_op jit(solution)/shard_map/ppermute | solution.py:15
  80.5 5.3 %collective-permute-start.25 = (bf16[128,1024]{1,0:T(8,128)(2,1)S(1)}, bf16[128,1024]{1,0:T(8,128)(2,1)S(1)}, u32[]{:S(2)}, u32[]{:S(2)}) collective-permute-start(bf16[128,1024]{1,0:T(8,128)(2,1)S(1)} %collective-permute-done.24.refs_3_), channel_id=1, source_target_pairs={{0,1},{1,0},{2,3},{3,2},{4,5},{5,4},{6,7},{7,6},{8,9},{9,8},{10,11... | collective-permute-start | bytes 786440 | tf_op jit(solution)/shard_map/ppermute | solution.py:15
  80.5 8.4 %collective-permute-start.35 = (bf16[128,1024]{1,0:T(8,128)(2,1)S(1)}, bf16[128,1024]{1,0:T(8,128)(2,1)S(1)}, u32[]{:S(2)}, u32[]{:S(2)}) collective-permute-start(bf16[128,1024]{1,0:T(8,128)(2,1)S(1)} %collective-permute-done.34.refs_3_), channel_id=1, source_target_pairs={{0,1},{1,0},{2,3},{3,2},{4,5},{5,4},{6,7},{7,6},{8,9},{9,8},{10,11... | collective-permute-start | bytes 786440 | tf_op jit(solution)/shard_map/ppermute | solution.py:15
  85.2 6.5 %collective-permute-start.15 = (bf16[192,1024]{1,0:T(8,128)(2,1)S(1)}, bf16[192,1024]{1,0:T(8,128)(2,1)S(1)}, u32[]{:S(2)}, u32[]{:S(2)}) collective-permute-start(bf16[192,1024]{1,0:T(8,128)(2,1)S(1)} %get-tuple-element.92), channel_id=1, source_target_pairs={{0,1},{1,0},{2,3},{3,2},{4,5},{5,4},{6,7},{7,6},{8,9},{9,8},{10,11... | collective-permute-start | bytes 1179656 | tf_op jit(solution)/shard_map/ppermute | solution.py:15
  85.3 6.9 %collective-permute-start.16 = (bf16[192,1024]{1,0:T(8,128)(2,1)S(1)}, bf16[192,1024]{1,0:T(8,128)(2,1)S(1)}, u32[]{:S(2)}, u32[]{:S(2)}) collective-permute-start(bf16[192,1024]{1,0:T(8,128)(2,1)S(1)} %get-tuple-element.93), channel_id=1, source_target_pairs={{0,1},{1,0},{2,3},{3,2},{4,5},{5,4},{6,7},{7,6},{8,9},{9,8},{10,11... | collective-permute-start | bytes 1179656 | tf_op jit(solution)/shard_map/ppermute | solution.py:15
  88.4 4.5 %collective-permute-start.26 = (bf16[128,1024]{1,0:T(8,128)(2,1)S(1)}, bf16[128,1024]{1,0:T(8,128)(2,1)S(1)}, u32[]{:S(2)}, u32[]{:S(2)}) collective-permute-start(bf16[128,1024]{1,0:T(8,128)(2,1)S(1)} %get-tuple-element.103), channel_id=1, source_target_pairs={{0,1},{1,0},{2,3},{3,2},{4,5},{5,4},{6,7},{7,6},{8,9},{9,8},{10,11... | collective-permute-start | bytes 786440 | tf_op jit(solution)/shard_map/ppermute | solution.py:15
  88.6 4.4 %collective-permute-start.27 = (bf16[128,1024]{1,0:T(8,128)(2,1)S(1)}, bf16[128,1024]{1,0:T(8,128)(2,1)S(1)}, u32[]{:S(2)}, u32[]{:S(2)}) collective-permute-start(bf16[128,1024]{1,0:T(8,128)(2,1)S(1)} %get-tuple-element.104), channel_id=1, source_target_pairs={{0,1},{1,0},{2,3},{3,2},{4,5},{5,4},{6,7},{7,6},{8,9},{9,8},{10,11... | collective-permute-start | bytes 786440 | tf_op jit(solution)/shard_map/ppermute | solution.py:15
  91.6 3.1 %collective-permute-start.36 = (bf16[128,1024]{1,0:T(8,128)(2,1)S(1)}, bf16[128,1024]{1,0:T(8,128)(2,1)S(1)}, u32[]{:S(2)}, u32[]{:S(2)}) collective-permute-start(bf16[128,1024]{1,0:T(8,128)(2,1)S(1)} %get-tuple-element.113), channel_id=1, source_target_pairs={{0,1},{1,0},{2,3},{3,2},{4,5},{5,4},{6,7},{7,6},{8,9},{9,8},{10,11... | collective-permute-start | bytes 786440 | tf_op jit(solution)/shard_map/ppermute | solution.py:15
  91.7 2.9 %collective-permute-start.37 = (bf16[128,1024]{1,0:T(8,128)(2,1)S(1)}, bf16[128,1024]{1,0:T(8,128)(2,1)S(1)}, u32[]{:S(2)}, u32[]{:S(2)}) collective-permute-start(bf16[128,1024]{1,0:T(8,128)(2,1)S(1)} %get-tuple-element.114), channel_id=1, source_target_pairs={{0,1},{1,0},{2,3},{3,2},{4,5},{5,4},{6,7},{7,6},{8,9},{9,8},{10,11... | collective-permute-start | bytes 786440 | tf_op jit(solution)/shard_map/ppermute | solution.py:15
  92.4 24.9 %collective-permute-start.17 = (bf16[192,1024]{1,0:T(8,128)(2,1)S(1)}, bf16[192,1024]{1,0:T(8,128)(2,1)S(1)}, u32[]{:S(2)}, u32[]{:S(2)}) collective-permute-start(bf16[192,1024]{1,0:T(8,128)(2,1)S(1)} %get-tuple-element.95), channel_id=1, source_target_pairs={{0,2},{1,3},{2,0},{3,1},{4,6},{5,7},{6,4},{7,5},{8,10},{9,11},{10,... | collective-permute-start | bytes 1179656 | tf_op jit(solution)/shard_map/ppermute | solution.py:15
  93.1 16.9 %collective-permute-start.28 = (bf16[128,1024]{1,0:T(8,128)(2,1)S(1)}, bf16[128,1024]{1,0:T(8,128)(2,1)S(1)}, u32[]{:S(2)}, u32[]{:S(2)}) collective-permute-start(bf16[128,1024]{1,0:T(8,128)(2,1)S(1)} %get-tuple-element.106), channel_id=1, source_target_pairs={{0,2},{1,3},{2,0},{3,1},{4,6},{5,7},{6,4},{7,5},{8,10},{9,11},{10,... | collective-permute-start | bytes 786440 | tf_op jit(solution)/shard_map/ppermute | solution.py:15
  94.8 20.9 %collective-permute-start.38 = (bf16[128,1024]{1,0:T(8,128)(2,1)S(1)}, bf16[128,1024]{1,0:T(8,128)(2,1)S(1)}, u32[]{:S(2)}, u32[]{:S(2)}) collective-permute-start(bf16[128,1024]{1,0:T(8,128)(2,1)S(1)} %get-tuple-element.116), channel_id=1, source_target_pairs={{0,2},{1,3},{2,0},{3,1},{4,6},{5,7},{6,4},{7,5},{8,10},{9,11},{10,... | collective-permute-start | bytes 786440 | tf_op jit(solution)/shard_map/ppermute | solution.py:15
  95.4 1.3 collective-permute-start.12
  95.4 1.5 %collective-permute-start.13 = (bf16[64,1024]{1,0:T(8,128)(2,1)S(1)}, bf16[64,1024]{1,0:T(8,128)(2,1)S(1)}, u32[]{:S(2)}, u32[]{:S(2)}) collective-permute-start(bf16[64,1024]{1,0:T(8,128)(2,1)S(1)} %get-tuple-element.87), channel_id=1, source_target_pairs={{0,1},{1,0},{2,3},{3,2},{4,5},{5,4},{6,7},{7,6},{8,9},{9,8},{10,11... | collective-permute-start | bytes 393224 | tf_op jit(solution)/shard_map/ppermute | solution.py:15
  97.0 22.3 %collective-permute-start.14 = (bf16[64,1024]{1,0:T(8,128)(2,1)S(1)}, bf16[64,1024]{1,0:T(8,128)(2,1)S(1)}, u32[]{:S(2)}, u32[]{:S(2)}) collective-permute-start(bf16[64,1024]{1,0:T(8,128)(2,1)S(1)} %get-tuple-element.89), channel_id=1, source_target_pairs={{0,2},{1,3},{2,0},{3,1},{4,6},{5,7},{6,4},{7,5},{8,10},{9,11},{10,... | collective-permute-start | bytes 393224 | tf_op jit(solution)/shard_map/ppermute | solution.py:15
  110.1 16.1 %collective-permute-start.29 = (bf16[64,1024]{1,0:T(8,128)(2,1)S(1)}, bf16[64,1024]{1,0:T(8,128)(2,1)S(1)}, u32[]{:S(2)}, u32[]{:S(2)}) collective-permute-start(bf16[64,1024]{1,0:T(8,128)(2,1)S(1)} %get-tuple-element.107), channel_id=1, source_target_pairs={{0,16},{4,20},{8,24},{12,28},{16,0},{20,4},{24,8},{28,12},{1,17},{... | collective-permute-start | bytes 393224 | tf_op jit(solution)/shard_map/ppermute | solution.py:15
  111.1 19.2 %collective-permute-start.30 = (bf16[64,1024]{1,0:T(8,128)(2,1)S(1)}, bf16[64,1024]{1,0:T(8,128)(2,1)S(1)}, u32[]{:S(2)}, u32[]{:S(2)}) collective-permute-start(bf16[64,1024]{1,0:T(8,128)(2,1)S(1)} %get-tuple-element.108), channel_id=1, source_target_pairs={{0,20},{4,16},{8,28},{12,24},{16,4},{20,0},{24,12},{28,8},{1,21},{... | collective-permute-start | bytes 393224 | tf_op jit(solution)/shard_map/ppermute | solution.py:15
  115.7 14.6 %collective-permute-start.39 = (bf16[64,1024]{1,0:T(8,128)(2,1)S(1)}, bf16[64,1024]{1,0:T(8,128)(2,1)S(1)}, u32[]{:S(2)}, u32[]{:S(2)}) collective-permute-start(bf16[64,1024]{1,0:T(8,128)(2,1)S(1)} %get-tuple-element.117), channel_id=1, source_target_pairs={{0,24},{4,28},{8,16},{12,20},{16,8},{20,12},{24,0},{28,4},{1,25},{... | collective-permute-start | bytes 393224 | tf_op jit(solution)/shard_map/ppermute | solution.py:15
  117.3 13.1 %collective-permute-start.40 = (bf16[64,1024]{1,0:T(8,128)(2,1)S(1)}, bf16[64,1024]{1,0:T(8,128)(2,1)S(1)}, u32[]{:S(2)}, u32[]{:S(2)}) collective-permute-start(bf16[64,1024]{1,0:T(8,128)(2,1)S(1)} %get-tuple-element.118), channel_id=1, source_target_pairs={{0,28},{4,24},{8,20},{12,16},{16,12},{20,8},{24,4},{28,0},{1,29},{... | collective-permute-start | bytes 393224 | tf_op jit(solution)/shard_map/ppermute | solution.py:15
  119.2 11.1 %collective-permute-start.18 = (bf16[64,1024]{1,0:T(8,128)(2,1)S(1)}, bf16[64,1024]{1,0:T(8,128)(2,1)S(1)}, u32[]{:S(2)}, u32[]{:S(2)}) collective-permute-start(bf16[64,1024]{1,0:T(8,128)(2,1)S(1)} %get-tuple-element.96), channel_id=1, source_target_pairs={{0,4},{4,0},{8,12},{12,8},{16,20},{20,16},{24,28},{28,24},{1,5},{5... | collective-permute-start | bytes 393224 | tf_op jit(solution)/shard_map/ppermute | solution.py:15
  126.2 5.5 %collective-permute-start.19 = (bf16[64,1024]{1,0:T(8,128)(2,1)S(1)}, bf16[64,1024]{1,0:T(8,128)(2,1)S(1)}, u32[]{:S(2)}, u32[]{:S(2)}) collective-permute-start(bf16[64,1024]{1,0:T(8,128)(2,1)S(1)} %get-tuple-element.97), channel_id=1, source_target_pairs={{0,8},{4,12},{8,0},{12,4},{16,24},{20,28},{24,16},{28,20},{1,9},{5... | collective-permute-start | bytes 393224 | tf_op jit(solution)/shard_map/ppermute | solution.py:15
  130.3 5.9 %collective-permute-start.20 = (bf16[64,1024]{1,0:T(8,128)(2,1)S(1)}, bf16[64,1024]{1,0:T(8,128)(2,1)S(1)}, u32[]{:S(2)}, u32[]{:S(2)}) collective-permute-start(bf16[64,1024]{1,0:T(8,128)(2,1)S(1)} %get-tuple-element.98), channel_id=1, source_target_pairs={{0,12},{4,8},{8,4},{12,0},{16,28},{20,24},{24,20},{28,16},{1,13},{... | collective-permute-start | bytes 393224 | tf_op jit(solution)/shard_map/ppermute | solution.py:15
